TPU v7x, 512 devices: a whole 4x8x8 slice. The times are simulated.
512 devices in a mesh: row: 64 (over z, y), col: 8 (over x, core).
Axes of the slice: x: 4, y: 8, z: 8, core: 2. Of those that a mesh axis runs over, the one named last changes fastest.
Arguments:
- tokens: bfloat16 [2, 8192, 2048], P(None, 'row'), may hold values from -6 to 6
- w_value: bfloat16 [2048, 1024], P(None, 'col'), may hold values from -0.125 to 0.125
- w_first: bfloat16 [2048, 1024], P(None, 'col'), may hold values from -0.125 to 0.125
- w_second: bfloat16 [2048, 1024], P(None, 'col'), may hold values from -0.125 to 0.125
- short_taps: float32 [3, 3, 1024], P(None, None, 'col'), may hold values from -3.5 to 3.5
- filter_in: float32 [33, 64], replicated, may hold values from -2 to 2
- filter_mid: float32 [64, 64], replicated, may hold values from -1.5 to 1.5
- filter_out: float32 [64, 2, 2, 1024], P(None, None, None, 'col'), may hold values from -0.75 to 0.75
- decay_rate: float32 [1024], P('col'), may hold values from 0 to 1, as said below
- skip_gain: float32 [2, 1024], P(None, 'col'), may hold values from -4 to 4
- w_output: bfloat16 [1024, 2048], P(None, 'col'), may hold values from -0.1875 to 0.1875
Outputs:
- mixed_out: bfloat16 [2, 8192, 2048], P(None, 'row', 'col')
Inputs may be any that keep to these rules, and one draw needn't show every extreme that they name: `decay_rate`: Per-position decay rates of the channels' filters; all positive.
All inputs are finite; a program needn't handle non-finite values.
Results may differ from a plain program's by a relative error of at most 0.007.
Values may be sent and summed in bfloat16 or wider, within the bound.
No kernel may reach another device: no remote copies, remote signals or barrier semaphores. Data moves between devices by JAX's collectives and lax.ppermute only.
A program may use at most 64 MiB of HBM per device.

v0:
```python
import math

import jax
import jax.numpy as jnp
from jax import lax
from jax.sharding import Mesh
from jax.sharding import PartitionSpec as P

ROW = ("row_0", "row_1")


highest = lax.Precision.HIGHEST


def split_up(array, dim, devices):
    before, after = (array.shape[:dim], array.shape[dim + 1 :])
    return jnp.moveaxis(array.reshape(*before, devices, -1, *after), dim, 0)


def laid_out(parts, dim):
    dims = list(parts.shape[1:])
    dims[dim] *= parts.shape[0]
    return jnp.moveaxis(parts, 0, dim).reshape(dims)


def turned_blocks(parts, axes, turns):
    dims = [lax.axis_size(a) for a in axes]
    parts = parts.reshape(*dims, *parts.shape[1:])
    for k in turns:
        parts = lax.all_to_all(parts, axes[k], split_axis=k, concat_axis=k, tiled=True)
    return parts.reshape(-1, *parts.shape[len(axes) :])


def stepwise_exchange(array, axes, turns, split_dim, concat_dim):
    parts = split_up(array, split_dim, lax.axis_size(axes))
    return laid_out(turned_blocks(parts, axes, turns), concat_dim)


def from_everyone(array, axis):
    devices = lax.axis_size(axis)
    return lax.all_to_all(
        jnp.broadcast_to(array[None], (devices, *array.shape)), axis, 0, 0, tiled=True
    )


def collect(array, axis, dim):
    parts = from_everyone(array, axis)
    return laid_out(parts, dim)


def position_features(length, band_count):
    lag_index = jnp.arange(length, dtype=jnp.float32)
    ramp_line = lag_index / (length - 1)
    omega_step = 2.0 * math.pi / length * lag_index
    band_freq = jnp.linspace(0.0001, band_count - 1, band_count, dtype=jnp.float32)
    angle = omega_step[:, None] * band_freq[None, :]
    return jnp.concatenate([ramp_line[:, None], jnp.cos(angle), -jnp.sin(angle)], axis=1)


def implicit_kernel(length, filter_in, filter_mid, out_cut, rate_cut):
    band_count = (filter_in.shape[0] - 1) // 2
    features = position_features(length, band_count)
    hidden = jnp.sin(jnp.dot(features, filter_in, precision=highest))
    hidden = jnp.sin(jnp.dot(hidden, filter_mid, precision=highest))
    shaped = jnp.einsum("lh,hsoc->socl", hidden, out_cut, precision=highest)
    lag_index = jnp.arange(length, dtype=jnp.float32)
    shaped = shaped * jnp.exp(-rate_cut[:, None] * lag_index[None, :])
    ahead_half = shaped[0]
    behind_half = shaped[1]
    zero_col = jnp.zeros(ahead_half.shape[:-1] + (1,), jnp.float32)
    kernel = jnp.concatenate([ahead_half, zero_col, behind_half[..., 1:][..., ::-1]], axis=-1)
    return kernel * lax.rsqrt(jnp.sum(kernel * kernel, axis=-1, keepdims=True) + 1e-06)


def transform_tables(factor_one, factor_two):
    full_length = factor_one * factor_two
    row_index = jnp.arange(factor_one, dtype=jnp.int32)
    col_index = jnp.arange(factor_two, dtype=jnp.int32)
    angle_rows = (row_index[:, None] * row_index[None, :] % factor_one).astype(jnp.float32) * (
        2.0 * math.pi / factor_one
    )
    angle_cols = (col_index[:, None] * col_index[None, :] % factor_two).astype(jnp.float32) * (
        2.0 * math.pi / factor_two
    )
    angle_turn = (row_index[:, None] * col_index[None, :] % full_length).astype(jnp.float32) * (
        2.0 * math.pi / full_length
    )
    return (
        jnp.cos(angle_rows),
        jnp.sin(angle_rows),
        jnp.cos(angle_cols),
        jnp.sin(angle_cols),
        jnp.cos(angle_turn),
        jnp.sin(angle_turn),
    )


def forward_transform(signal, tables):
    cosine_rows, sine_rows, cosine_cols, sine_cols, cosine_turn, sine_turn = tables
    used_rows = signal.shape[-2]
    first_real = jnp.einsum(
        "kn,...nq->...kq", cosine_rows[:, :used_rows], signal, precision=highest
    )
    first_imag = -jnp.einsum("kn,...nq->...kq", sine_rows[:, :used_rows], signal, precision=highest)
    turned_real = first_real * cosine_turn + first_imag * sine_turn
    turned_imag = first_imag * cosine_turn - first_real * sine_turn
    spec_real = jnp.matmul(turned_real, cosine_cols, precision=highest) + jnp.matmul(
        turned_imag, sine_cols, precision=highest
    )
    spec_imag = jnp.matmul(turned_imag, cosine_cols, precision=highest) - jnp.matmul(
        turned_real, sine_cols, precision=highest
    )
    return (spec_real, spec_imag)


def inverse_transform(spec_real, spec_imag, tables):
    cosine_rows, sine_rows, cosine_cols, sine_cols, cosine_turn, sine_turn = tables
    mid_real = jnp.matmul(spec_real, cosine_cols, precision=highest) - jnp.matmul(
        spec_imag, sine_cols, precision=highest
    )
    mid_imag = jnp.matmul(spec_imag, cosine_cols, precision=highest) + jnp.matmul(
        spec_real, sine_cols, precision=highest
    )
    turned_real = mid_real * cosine_turn - mid_imag * sine_turn
    turned_imag = mid_imag * cosine_turn + mid_real * sine_turn
    half_rows = cosine_rows.shape[0] // 2
    restored = jnp.einsum(
        "nk,...kq->...nq", cosine_rows[:half_rows], turned_real, precision=highest
    )
    restored = restored - jnp.einsum(
        "nk,...kq->...nq", sine_rows[:half_rows], turned_imag, precision=highest
    )
    return restored / (cosine_rows.shape[0] * cosine_cols.shape[0])


def on_device(
    tokens,
    w_value,
    w_first,
    w_second,
    short_taps,
    filter_in,
    filter_mid,
    filter_out,
    decay_rate,
    skip_gain,
    w_output,
):
    seq_count = tokens.shape[0]
    tok_rows = tokens.shape[1]
    local_width = w_value.shape[1]
    groups = lax.axis_size(ROW)
    narrow = local_width // groups
    length = tok_rows * groups
    offset = lax.axis_index(ROW) * narrow
    projected = jnp.stack(
        [
            jnp.einsum("std,dc->sct", tokens, weight, preferred_element_type=jnp.float32).astype(
                jnp.bfloat16
            )
            for weight in (w_value, w_first, w_second)
        ]
    )
    arrived = lax.all_to_all(projected, ROW, split_axis=2, concat_axis=3, tiled=True)
    arrived = arrived.astype(jnp.float32)
    tap_cut = lax.dynamic_slice_in_dim(short_taps, offset, narrow, 2)
    padded_span = jnp.pad(arrived, ((0, 0), (0, 0), (0, 0), (1, 1)))
    spread = (
        tap_cut[0][:, None, :, None] * padded_span[..., :length]
        + tap_cut[1][:, None, :, None] * padded_span[..., 1 : length + 1]
        + tap_cut[2][:, None, :, None] * padded_span[..., 2:]
    )
    rate_cut = lax.dynamic_slice_in_dim(decay_rate, offset, narrow, 0)
    gain_cut = lax.dynamic_slice_in_dim(skip_gain, offset, narrow, 1)
    out_cut = lax.dynamic_slice_in_dim(filter_out, offset, narrow, 3)
    kernel = implicit_kernel(length, filter_in, filter_mid, out_cut, rate_cut)
    factor_one = 256
    factor_two = 2 * length // factor_one
    tables = transform_tables(factor_one, factor_two)
    kernel_real, kernel_imag = forward_transform(
        kernel.reshape(2, narrow, factor_one, factor_two), tables
    )
    carried = spread[0]
    for order_idx in range(2):
        state_real, state_imag = forward_transform(
            carried.reshape(seq_count, narrow, factor_one // 2, factor_two), tables
        )
        prod_real = state_real * kernel_real[order_idx] - state_imag * kernel_imag[order_idx]
        prod_imag = state_real * kernel_imag[order_idx] + state_imag * kernel_real[order_idx]
        reach_term = inverse_transform(prod_real, prod_imag, tables).reshape(
            seq_count, narrow, length
        )
        carried = spread[order_idx + 1] * (
            reach_term + gain_cut[order_idx][None, :, None] * carried
        )
    gated_out = carried.astype(jnp.bfloat16)
    returned = stepwise_exchange(gated_out, ROW, (0, 1), 2, 1)
    result = jnp.einsum(
        "sct,cd->std", collect(returned, "col", 1), w_output, preferred_element_type=jnp.float32
    )
    return result.astype(jnp.bfloat16)


def solution(mesh):
    torus = Mesh(mesh.devices.reshape(8, 8, mesh.shape["col"]), ("row_0", "row_1", "col"))
    in_specs = (
        P(None, ROW, None),
        P(None, "col"),
        P(None, "col"),
        P(None, "col"),
        P(None, None, "col"),
        P(),
        P(),
        P(None, None, None, "col"),
        P("col"),
        P(None, "col"),
        P(None, "col"),
    )
    out_specs = P(None, ROW, "col")
    return jax.shard_map(
        on_device, mesh=torus, in_specs=in_specs, out_specs=out_specs, check_vma=False
    )
```

profile of v0, /device:TPU:1, one launch (start us, length us, event | category | flops | bytes accessed | tf_op | source)
XLA Modules:
  0.0 130.3 jit_solution(11389962554042009182)
XLA Ops:
  0.0 1.2 copy-done
  1.2 1.5 %fusion.13 = bf16[1,2,128,128]{3,2,1,0:T(8,128)(2,1)S(1)} fusion(bf16[2,128,2048]{2,1,0:T(8,128)(2,1)S(1)} %copy-done, bf16[2048,128]{1,0:T(8,128)(2,1)} %param.12), kind=kOutput, calls=%fused_computation.38 | convolution fusion | flops 134250496 | bytes 1638400 | tf_op jit(solution)/shard_map/std,dc->sct/dot_general | solution.py:158
  2.8 1.6 %fusion.14 = bf16[1,2,128,128]{3,2,1,0:T(8,128)(2,1)S(1)} fusion(bf16[2,128,2048]{2,1,0:T(8,128)(2,1)S(1)} %copy-done, bf16[2048,128]{1,0:T(8,128)(2,1)} %param.13), kind=kOutput, calls=%fused_computation.39 | convolution fusion | flops 134250496 | bytes 1638400 | tf_op jit(solution)/shard_map/std,dc->sct/dot_general | solution.py:158
  4.9 0.9 copy.72
  5.8 17.1 %all-to-all-start = ((bf16[3,2,128,128]{3,1,0,2:T(2,128)(2,1)}), bf16[3,2,128,128]{3,1,0,2:T(2,128)(2,1)S(1)}, u32[]{:S(2)}, u32[]{:S(2)}) async-start(bf16[3,2,128,128]{3,1,0,2:T(2,128)(2,1)} %copy.72), calls=%async_computation | async-start | bytes 393216 | tf_op jit(solution)/shard_map/all_to_all | solution.py:164
  23.5 1.9 %multiply_cosine_fusion = (f32[8192,16]{0,1:T(8,128)S(1)}, f32[8192,16]{0,1:T(8,128)S(1)}) fusion(f32[16]{0:T(128)S(1)} %pad_maximum_fusion.1, f32[8192]{0:T(1024)S(1)} %iota_multiply_fusion), kind=kLoop, calls=%fused_computation.42 | loop fusion | flops 262144 | bytes 1081408 | tf_op jit(solution)/shard_map/cos | solution.py:57
  25.5 12.0 %convolution_sine_fusion.1 = f32[8192,64]{0,1:T(8,128)S(1)} fusion(f32[33,64]{1,0:T(8,128)S(1)} %copy-done.6, f32[8192,16]{0,1:T(8,128)S(1)} %get-tuple-element.15, f32[8192,16]{0,1:T(8,128)S(1)} %get-tuple-element.14, f32[8192,1]{0,1:T(1,128)S(1)} %iota_multiply_fusion.1), kind=kOutput, calls=%fused_computation.2 | convolution fusion | flops 208158720 | bytes 3186944 | tf_op jit(solution)/shard_map/dot_general | solution.py:63
  37.5 10.1 %fusion = f32[8192,64,1,1]{0,1,3,2:T(8,128)S(1)} fusion(f32[8192,64]{0,1:T(8,128)S(1)} %convolution_sine_fusion.1, f32[64,64]{1,0:T(8,128)S(1)} %copy-done.5), kind=kOutput, calls=%fused_computation.1 | convolution fusion | flops 402653184 | bytes 4210688 | tf_op jit(solution)/shard_map/dot_general | solution.py:64
  47.5 1.1 convolution_multiply_fusion
  48.9 5.7 %reverse = f32[2,2,8192]{2,1,0:T(2,128)S(1)} reverse(f32[2,2,8192]{2,1,0:T(2,128)S(1)} %bitcast.189), dimensions={2} | reverse | bytes 262144
  54.9 0.7 concatenate.14
  56.1 1.8 %fusion.6 = f32[2,2,256,64]{2,3,1,0:T(8,128)S(1)} fusion(f32[2,2,256,64]{3,2,1,0:T(8,128)S(1)} %concatenate.15, f32[2,2]{1,0:T(2,128)S(1)} %add_rsqrt_fusion), kind=kOutput, calls=%fused_computation.19 | convolution fusion | flops 202375168 | bytes 524304 | tf_op jit(solution)/shard_map/kn,...nq->...kq/dot_general | solution.py:104
  58.0 1.8 %convolution_bitcast_fusion = f32[2,2,256,64]{2,3,1,0:T(8,128)S(1)} fusion(f32[2,2,256,64]{3,2,1,0:T(8,128)S(1)} %concatenate.15, f32[2,2]{1,0:T(2,128)S(1)} %add_rsqrt_fusion), kind=kOutput, calls=%fused_computation.20 | convolution fusion | flops 202309632 | bytes 524304 | tf_op jit(solution)/shard_map/kn,...nq->...kq/dot_general | solution.py:101
  61.2 1.0 fusion.59
  62.2 0.6 convolution_add_fusion.3
  63.5 1.0 fusion.58
  64.9 0.9 multiply_add_fusion
  65.8 0.7 fusion.220
  66.7 0.6 convolution_bitcast_fusion.1
  67.3 0.6 fusion.7
  69.6 0.8 convolution_subtract_fusion.4
  71.0 1.2 fusion.90
  72.2 0.8 copy.83
  73.0 0.6 convolution_subtract_fusion.2
  73.5 1.5 %convolution_add_fusion.2 = f32[2,2,256,64]{2,3,1,0:T(8,128)S(1)} fusion(f32[2,2,256,64]{2,3,1,0:T(8,128)} %fusion.90, f32[2,2,256,64]{2,3,1,0:T(8,128)S(1)} %convolution_subtract_fusion.4, f32[2,2,256,64]{2,3,1,0:T(8,128)S(1)} %convolution_add_fusion.4, f32[2,256,64]{1,2,0:T(8,128)S(1)} %get-tuple-element.11, f32[2,256,64]{1,2,0:T(8,128)S(1)} %get-tuple-element.9), kind=kOutput, calls=%fused_computation.13 | convolution fusion | flops 50651136 | bytes 1310720 | tf_op jit(solution)/shard_map/dot_general | solution.py:121
  75.8 1.9 %add_multiply_fusion = (f32[2,2,128,64]{2,3,1,0:T(8,128)S(1)}, f32[2,2,128,64]{2,3,1,0:T(8,128)}) fusion(f32[2,2,128,64]{2,3,1,0:T(8,128)S(1)} %copy.84, f32[2,2,128,64]{2,3,1,0:T(8,128)} %copy.83, f32[2]{0:T(128)S(1)} %get-tuple-element.20, f32[2,2,64,128]{3,2,1,0:T(8,128)S(1)} %fusion.40, f32[256,256]{1,0:T(8,128)S(1)} %fusion.58, ...), kind=kOutput, calls=%fused_computation.105 | convolution fusion | flops 101023744 | bytes 1442304 | tf_op jit(solution)/shard_map/nk,...kq->...nq/dot_general | solution.py:130
  82.0 0.6 convolution_subtract_fusion
  82.6 0.6 convolution_add_fusion
  84.7 13.3 %all_to_all.24 = bf16[8,8,2,2,128]{4,1,3,2,0:T(8,128)(2,1)S(1)} all-to-all(bf16[8,8,2,2,128]{4,1,3,2,0:T(8,128)(2,1)S(1)} %copy.87), channel_id=1, replica_groups=mesh['row_0'=8,'row_1'=8,'col'=8] {'row_0'}, dimensions={0} | all-to-all | bytes 131072 | tf_op jit(solution)/shard_map/all_to_all | solution.py:30
  98.1 13.4 %all_to_all.25 = bf16[8,8,2,2,128]{4,0,3,2,1:T(8,128)(2,1)S(1)} all-to-all(bf16[8,8,2,2,128]{4,0,3,2,1:T(8,128)(2,1)S(1)} %copy.88), channel_id=1, replica_groups=mesh['row_0'=8,'row_1'=8,'col'=8] {'row_1'}, dimensions={1} | all-to-all | bytes 131072 | tf_op jit(solution)/shard_map/all_to_all | solution.py:30
  111.9 17.5 %all_to_all.26 = bf16[8,2,128,128]{2,3,1,0:T(8,128)(2,1)S(1)} all-to-all(bf16[8,2,128,128]{2,3,1,0:T(8,128)(2,1)S(1)} %broadcast_in_dim.7), channel_id=1, replica_groups=mesh['row_0'=8,'row_1'=8,'col'=8] {'col'}, dimensions={0} | all-to-all | bytes 1048576 | tf_op jit(solution)/shard_map/all_to_all | solution.py:41
  129.4 1.0 convolution_convert_fusion
  (82 shorter events, 13.8 us)
Async XLA Ops:
  0.0 1.2 copy-start
  0.0 4.4 %copy-start.1 = (bf16[2048,128]{1,0:T(8,128)(2,1)S(1)}, bf16[2048,128]{1,0:T(8,128)(2,1)}, u32[]{:S(2)}) copy-start(bf16[2048,128]{1,0:T(8,128)(2,1)} %param.14) | copy-start | bytes 1572868
  2.8 20.3 %copy-start.4 = (f32[64,2,2,128]{3,2,1,0:T(2,128)S(1)}, f32[64,2,2,128]{3,2,1,0:T(2,128)}, u32[]{:S(2)}) copy-start(f32[64,2,2,128]{3,2,1,0:T(2,128)} %param.18) | copy-start | bytes 393220
  2.8 20.5 %copy-start.10 = (f32[128]{0:T(128)S(1)}, f32[128]{0:T(128)}, u32[]{:S(2)}) copy-start(f32[128]{0:T(128)} %param.19) | copy-start | bytes 1540
  4.4 21.1 %copy-start.6 = (f32[33,64]{1,0:T(8,128)S(1)}, f32[33,64]{1,0:T(8,128)}, u32[]{:S(2)}) copy-start(f32[33,64]{1,0:T(8,128)} %param.16) | copy-start | bytes 25348
  5.8 58.7 %all-to-all-start = ((bf16[3,2,128,128]{3,1,0,2:T(2,128)(2,1)}), bf16[3,2,128,128]{3,1,0,2:T(2,128)(2,1)S(1)}, u32[]{:S(2)}, u32[]{:S(2)}) async-start(bf16[3,2,128,128]{3,1,0,2:T(2,128)(2,1)} %copy.72), calls=%async_computation | async-start | bytes 393216 | tf_op jit(solution)/shard_map/all_to_all | solution.py:164
  23.5 13.9 %copy-start.5 = (f32[64,64]{1,0:T(8,128)S(1)}, f32[64,64]{1,0:T(8,128)}, u32[]{:S(2)}) copy-start(f32[64,64]{1,0:T(8,128)} %param.17) | copy-start | bytes 49156
  60.6 2.7 %copy-start.8 = (f32[2,128]{1,0:T(2,128)S(1)}, f32[2,128]{1,0:T(2,128)}, u32[]{:S(2)}) copy-start(f32[2,128]{1,0:T(2,128)} %param.20) | copy-start | bytes 3076
  60.6 2.8 %copy-start.7 = (f32[3,3,128]{2,1,0:T(4,128)S(1)}, f32[3,3,128]{2,1,0:T(4,128)}, u32[]{:S(2)}) copy-start(f32[3,3,128]{2,1,0:T(4,128)} %param.15) | copy-start | bytes 13828
  82.6 1.6 %copy-start.3 = (f32[2,2,128,64]{2,3,1,0:T(8,128)S(1)}, f32[2,2,128,64]{2,3,1,0:T(8,128)}, u32[]{:S(2)}) copy-start(f32[2,2,128,64]{2,3,1,0:T(8,128)} %get-tuple-element.22) | copy-start | bytes 393220
  83.2 1.3 copy-start.2
  84.2 45.1 %copy-start.9 = (bf16[1024,256]{1,0:T(8,128)(2,1)S(1)}, bf16[1024,256]{1,0:T(8,128)(2,1)}, u32[]{:S(2)}) copy-start(bf16[1024,256]{1,0:T(8,128)(2,1)} %param.21) | copy-start | bytes 1572868
where the time goes:
time: 131 us; the launch traced here: 130 us
  matrix products  49.3 us (38%)
  blocking collectives  44.3 us (34%)
  starting transfers between devices  17.1 us (13%)
  local copies, waits for them, and re-layouts  13.1 us (10%)
  other arithmetic  5.9 us (5%)
    all_to_all x2, blocking collectives, turned_blocks(): lax.all_to_all(parts, axes[k], split_axis=k, concat_axis=k, tiled=True)  26.7 us
    all_to_all x1, blocking collectives, from_everyone(): lax.all_to_all(jnp.broadcast_to(array[None], (devices, *array.shape)), ax...  17.5 us
    all_to_all x1, starting transfers between devices, on_device(): lax.all_to_all(projected, ROW, split_axis=2, concat_axis=3, tiled=True)  17.1 us
    dot_general x1, matrix products, implicit_kernel(): hidden = jnp.sin(jnp.dot(features, filter_in, precision=highest))  12 us
    dot_general x1, matrix products, implicit_kernel(): hidden = jnp.sin(jnp.dot(hidden, filter_mid, precision=highest))  10.1 us
    unnamed x24, local copies, waits for them, and re-layouts  7.23 us
    dot_general x3, matrix products, on_device(): jnp.einsum('std,dc->sct', tokens, weight, preferred_element_type=jnp.floa...  3.58 us
    dot_general x3, matrix products, forward_transform(): jnp.einsum('kn,...nq->...kq', sine_rows[:, :used_rows], signal, precision...  2.82 us
  transfers between devices with their start and end apart: 1, of which 0 were waited for; matrix products, arithmetic and copies ran while one was open for 32% of the time, Pallas kernels for 0%

commit v1 on v0

v1 whole, which is shorter than its diff:
```python
import functools
import math

import jax
import jax.numpy as jnp
import numpy as np
from jax import lax
from jax.experimental import pallas as pl
from jax.experimental.pallas import tpu as pltpu
from jax.sharding import Mesh
from jax.sharding import PartitionSpec as P

ROW = ("row_0", "row_1")
COL = ("x", "core")
SIDE = 128
HALF = SIDE // 2
BF = jnp.bfloat16
F32 = jnp.float32


def halves(table):
    table = np.asarray(table, np.float32)
    top = table.astype(jnp.bfloat16)
    return top, (table - top.astype(np.float32)).astype(jnp.bfloat16)


@functools.lru_cache(None)
def tables(length, feats):
    bands = (feats - 1) // 2
    lag = np.arange(length, dtype=np.float64)
    freq = np.linspace(0.0001, bands - 1, bands)
    angle = (2.0 * math.pi / length) * lag[None, :] * freq[:, None]
    features = np.concatenate(
        [lag[None, :] / (length - 1), np.cos(angle), -np.sin(angle), np.zeros((40 - feats, length))]
    )
    index = np.arange(SIDE)
    turn = 2.0 * math.pi / SIDE * (index[:, None] * index[None, :] % SIDE)
    cos, sin = np.cos(turn), np.sin(turn)
    fine = 2.0 * math.pi / (SIDE * SIDE) * (index[:, None] * index[None, :])
    real_in = np.concatenate([cos[:, :HALF], -sin[:, :HALF]])
    pair_in = np.block([[cos[:, :HALF], sin[:, :HALF]], [-sin[:, :HALF], cos[:, :HALF]]])
    right = np.block([[cos, -sin], [sin, cos]])
    split = {}
    split["real_in"] = halves(real_in)
    split["pair_in"] = halves(pair_in)
    split["pair_out"] = halves(pair_in.T)
    split["right"] = halves(right)
    split["back"] = halves(right.T)
    split["spec_re"] = halves(np.concatenate([cos, sin]))
    split["spec_im"] = halves(np.concatenate([-sin, cos]))
    return np.asarray(features, np.float32), np.stack([np.cos(fine), np.sin(fine)]).astype(
        np.float32
    ), split


def hi_lo(value):
    top = value.astype(BF)
    return top, (value - top.astype(F32)).astype(BF)


def mm(a, b, dims=(((1,), (0,)), ((), ()))):
    return lax.dot_general(a, b, dims, preferred_element_type=F32)


def left_const(const_hi, const_lo, value):
    top, low = hi_lo(value)
    return mm(const_hi, top) + mm(const_lo, top) + mm(const_hi, low)


def right_const(value, const_hi, const_lo):
    top, low = hi_lo(value)
    return mm(top, const_hi) + mm(low, const_hi) + mm(top, const_lo)


def sine_of_turns(turns):
    big = 12582912.0
    moved = turns - 0.25
    moved = moved - ((moved + big) - big)
    quarter = 0.25 - jnp.abs(moved)
    square = quarter * quarter
    poly = -70.98993302 * square + 81.34038614
    poly = poly * square - 41.33713041
    poly = poly * square + 6.28316395
    return poly * quarter


def filter_kernel(
    features_ref, in_ref, mid_ref, out_ref, rate_ref, fine_ref,
    real_hi, real_lo, re_hi, re_lo, im_hi, im_lo,
    spec_re_ref, spec_im_ref, rows_ref,
):
    length = features_ref.shape[1]
    device = lax.axis_index("row_0") * lax.axis_size("row_1") + lax.axis_index("row_1")
    lane = lax.broadcasted_iota(jnp.int32, (8, SIDE), 1)
    row = lax.broadcasted_iota(jnp.int32, (8, SIDE), 0)
    mine = lane == 2 * device + row % 2
    last = (((1,), (1,)), ((), ()))
    first = (((0,), (0,)), ((), ()))
    out_hi = jnp.zeros((8, out_ref.shape[0]), F32)
    out_lo = jnp.zeros((8, out_ref.shape[0]), F32)
    for pair in range(4):
        pick = jnp.where(mine & (row // 2 == pair), 1.0, 0.0).astype(BF)
        top, low = hi_lo(out_ref[:, pair * SIDE : (pair + 1) * SIDE])
        out_hi += mm(pick, top, last)
        out_lo += mm(pick, low, last)
    out_hi, out_lo = out_hi.astype(BF), out_lo.astype(BF)
    rate = jnp.sum(jnp.where(mine, rate_ref[...], 0.0), axis=1, keepdims=True)
    scale = 1.0 / (2.0 * math.pi)
    in_hi, in_lo = hi_lo(in_ref[...] * scale)
    mid_hi, mid_lo = hi_lo(mid_ref[...] * scale)
    out_all = jnp.concatenate([out_hi, out_lo, out_hi], axis=1)
    mid_all = jnp.concatenate([mid_hi, mid_lo, mid_hi], axis=1)
    chunk = 1024
    squares = jnp.zeros((8, SIDE), F32)
    sign = jnp.where(lax.broadcasted_iota(jnp.int32, (8, SIDE), 0) < 4, 1.0, -1.0)
    for start in range(0, length, chunk):
        top, low = hi_lo(features_ref[:, start : start + chunk])
        turns = mm(in_hi, top) + mm(in_lo, top) + mm(in_hi, low)
        top, low = hi_lo(sine_of_turns(turns))
        turns = mm(mid_all, jnp.concatenate([top, top, low], axis=0))
        top, low = hi_lo(sine_of_turns(turns))
        shaped = mm(out_all, jnp.concatenate([top, top, low], axis=0))
        for piece in range(chunk // SIDE):
            base = start + piece * SIDE
            lag = (lane + base).astype(F32)
            part = shaped[:, piece * SIDE : (piece + 1) * SIDE] * jnp.exp(-rate * lag)
            if base == 0:
                part = jnp.where((row >= 4) & (lane == 0), 0.0, part)
            squares += part * part
            other = pltpu.roll(part, 4, 0)
            rows_ref[base // SIDE] = other + part * sign
    total = jnp.sum(squares + pltpu.roll(squares, 4, 0), axis=1, keepdims=True)
    factor = lax.rsqrt(total + 1e-06) * (1.0 / (SIDE * SIDE))
    grid = jnp.concatenate([rows_ref[:, j, :] * factor[j : j + 1, :] for j in range(8)], axis=1)
    grid = left_const(real_hi[...], real_lo[...], grid)
    cos, sin = fine_ref[0], fine_ref[1]

    def turned(j):
        real = grid[:SIDE, j * SIDE : (j + 1) * SIDE]
        imag = grid[SIDE:, j * SIDE : (j + 1) * SIDE]
        return jnp.concatenate([real * cos + imag * sin, imag * cos - real * sin], axis=1)

    for order in range(2):
        for channel in range(2):
            j = order * 2 + channel
            rows = pl.ds(channel * SIDE, SIDE)
            spec_re_ref[order, rows, :] = right_const(turned(j), re_hi[...], re_lo[...])
            spec_im_ref[order, rows, :] = right_const(turned(j + 4), im_hi[...], im_lo[...])


def conv_kernel(
    x_ref, taps_ref, gain_ref, spec_re_ref, spec_im_ref, fine_ref,
    in_hi, in_lo, out_hi, out_lo, right_hi, right_lo, back_hi, back_lo,
    o_ref, wide_ref, rows_ref,
):
    device = lax.axis_index("row_0") * lax.axis_size("row_1") + lax.axis_index("row_1")
    wide_ref[...] = x_ref[...].astype(F32)
    row = lax.broadcasted_iota(jnp.int32, (HALF, SIDE), 0)
    lane = lax.broadcasted_iota(jnp.int32, (HALF, SIDE), 1)

    def smoothed(p):
        seqs = []
        for s in range(2):
            chans = []
            for c in range(2):
                here = wide_ref[:, (p * 2 + s) * 2 + c, :]
                moved = pltpu.roll(here, 1, 1)
                prev = jnp.where(lane == 0, pltpu.roll(moved, 1, 0), moved)
                prev = jnp.where((lane == 0) & (row == 0), 0.0, prev)
                moved = pltpu.roll(here, SIDE - 1, 1)
                after = jnp.where(lane == SIDE - 1, pltpu.roll(moved, HALF - 1, 0), moved)
                after = jnp.where((lane == SIDE - 1) & (row == HALF - 1), 0.0, after)
                at = 2 * device + c
                chans.append(
                    taps_ref[p, at] * prev + taps_ref[3 + p, at] * here + taps_ref[6 + p, at] * after
                )
            seqs.append(jnp.concatenate(chans, axis=1))
        return jnp.concatenate(seqs, axis=0)

    cos, sin = fine_ref[0], fine_ref[1]
    cos2, sin2 = jnp.concatenate([cos, cos], axis=1), jnp.concatenate([sin, sin], axis=1)
    lane2 = lax.broadcasted_iota(jnp.int32, (1, 2 * SIDE), 1)
    state = smoothed(0)
    for order in range(2):
        grid = left_const(in_hi[...], in_lo[...], state)
        real, imag = grid[:SIDE], grid[SIDE:]
        real, imag = real * cos2 + imag * sin2, imag * cos2 - real * sin2
        grid = jnp.concatenate(
            [
                jnp.concatenate([real[:, :SIDE], imag[:, :SIDE]], axis=1),
                jnp.concatenate([real[:, SIDE:], imag[:, SIDE:]], axis=1),
            ],
            axis=0,
        )
        grid = right_const(grid, right_hi[...], right_lo[...])
        real, imag = grid[:, :SIDE], grid[:, SIDE:]
        k_re, k_im = spec_re_ref[order], spec_im_ref[order]
        grid = jnp.concatenate([real * k_re - imag * k_im, real * k_im + imag * k_re], axis=1)
        grid = right_const(grid, back_hi[...], back_lo[...])
        real = jnp.concatenate([grid[:SIDE, :SIDE], grid[SIDE:, :SIDE]], axis=1)
        imag = jnp.concatenate([grid[:SIDE, SIDE:], grid[SIDE:, SIDE:]], axis=1)
        grid = jnp.concatenate([real * cos2 - imag * sin2, real * sin2 + imag * cos2], axis=0)
        reach = left_const(out_hi[...], out_lo[...], grid)
        gain = jnp.where(lane2 < SIDE, gain_ref[order, 2 * device], gain_ref[order, 2 * device + 1])
        state = smoothed(order + 1) * (reach + gain * state)
    for s in range(2):
        for c in range(2):
            rows_ref[s, pl.ds(c, HALF, stride=2), :] = state[
                s * HALF : (s + 1) * HALF, c * SIDE : (c + 1) * SIDE
            ]
        o_ref[:, pl.ds(s * SIDE, SIDE)] = rows_ref[s].astype(BF)


def on_device(
    tokens,
    w_value,
    w_first,
    w_second,
    short_taps,
    filter_in,
    filter_mid,
    filter_out,
    decay_rate,
    skip_gain,
    w_output,
):
    seqs, tok_rows, _ = tokens.shape
    blocks = lax.axis_size(ROW)
    length = tok_rows * blocks
    feats = filter_in.shape[0]
    features, fine, split = tables(length, feats)
    projected = jnp.stack(
        [
            jnp.einsum("std,dc->sct", tokens, weight, preferred_element_type=F32).astype(BF)
            for weight in (w_value, w_first, w_second)
        ]
    )
    pieces = projected.reshape(3, seqs, blocks, 2, tok_rows).transpose(2, 0, 1, 3, 4)
    pieces = pieces.reshape(blocks, 12, tok_rows)
    arrived = lax.all_to_all(pieces, ROW, 0, 0, tiled=True)

    vmem = pl.BlockSpec(memory_space=pltpu.VMEM)
    smem = pl.BlockSpec(memory_space=pltpu.SMEM)
    fine = jnp.asarray(fine)
    spec = jax.ShapeDtypeStruct((2, 2 * SIDE, SIDE), F32)
    const = {k: tuple(jnp.asarray(h) for h in v) for k, v in split.items()}
    spec_re, spec_im = pl.pallas_call(
        filter_kernel,
        out_shape=(spec, spec),
        in_specs=[vmem] * 12,
        out_specs=(vmem, vmem),
        scratch_shapes=[pltpu.VMEM((HALF, 8, SIDE), F32)],
        cost_estimate=pl.CostEstimate(
            flops=4_000_000_000, bytes_accessed=3_000_000, transcendentals=0
        ),
        name="filter_spectra",
    )(
        jnp.asarray(features),
        jnp.pad(filter_in.T, ((0, 0), (0, 40 - feats))),
        filter_mid.T,
        filter_out.reshape(filter_out.shape[0], -1),
        decay_rate.reshape(1, -1),
        fine,
        *const["real_in"],
        *const["spec_re"],
        *const["spec_im"],
    )
    gated = pl.pallas_call(
        conv_kernel,
        out_shape=jax.ShapeDtypeStruct((2 * blocks, seqs * tok_rows), BF),
        in_specs=[vmem, smem, smem] + [vmem] * 11,
        out_specs=vmem,
        scratch_shapes=[
            pltpu.VMEM((HALF, 12, SIDE), F32),
            pltpu.VMEM((2, SIDE, SIDE), F32),
        ],
        cost_estimate=pl.CostEstimate(
            flops=4_000_000_000, bytes_accessed=2_000_000, transcendentals=0
        ),
        name="gated_conv",
    )(
        arrived,
        short_taps.reshape(9, -1),
        skip_gain,
        spec_re,
        spec_im,
        fine,
        *const["pair_in"],
        *const["pair_out"],
        *const["right"],
        *const["back"],
    )
    returned = lax.all_to_all(gated, ROW, 0, 0, tiled=True)
    everyone = lax.all_to_all(
        jnp.broadcast_to(returned[None], (lax.axis_size("x"), *returned.shape)), "x", 0, 0, tiled=True
    )
    everyone = lax.all_gather(everyone, "core", axis=1)
    everyone = everyone.reshape(-1, seqs * tok_rows)
    result = jnp.einsum("ct,cd->td", everyone, w_output, preferred_element_type=F32)
    return result.astype(BF).reshape(seqs, tok_rows, -1)


def solution(mesh):
    torus = Mesh(mesh.devices.reshape(8, 8, 4, 2), ("row_0", "row_1", "x", "core"))
    in_specs = (
        P(None, ROW, None),
        P(None, COL),
        P(None, COL),
        P(None, COL),
        P(None, None, COL),
        P(),
        P(),
        P(None, None, None, COL),
        P(COL),
        P(None, COL),
        P(None, COL),
    )
    out_specs = P(None, ROW, COL)
    return jax.shard_map(
        on_device, mesh=torus, in_specs=in_specs, out_specs=out_specs, check_vma=False
    )
```

time: 131 us -> 80 us (0.61)
  matrix products: 49.3 us -> 3.5 us
  Pallas kernels: 0 us -> 13.5 us
  blocking collectives: 44.3 us -> 37 us
  local copies, waits for them, and re-layouts: 13.1 us -> 7.06 us
  other arithmetic: 5.9 us -> 0.03 us
    dot_general x37 -> x4, matrix products: 49.3 us -> 3.5 us  [the longest x3 2.5 us: on_device(): jnp.einsum('std,dc->sct', tokens, weight, preferred_element_type=F32)]
    pallas_call x0 -> x2, Pallas kernels: none -> 13.5 us  [the longest x1 8.81 us: on_device(): pl.pallas_call(filter_kernel, out_shape=(spec, spec), in_specs=[vmem] * 1...]
    all_to_all x3 -> x2, blocking collectives: 44.3 us -> 31.1 us  [the longest x1 21.8 us: on_device(): returned = lax.all_to_all(gated, ROW, 0, 0, tiled=True)]
    all_gather x0 -> x1, blocking collectives: none -> 5.89 us  [on_device(): everyone = lax.all_gather(everyone, 'core', axis=1)]
    unnamed x24 -> x20, local copies, waits for them, and re-layouts: 7.23 us -> 3.22 us
    cos x2 -> x0, other arithmetic: 2.86 us -> none  [the longest x1 1.9 us: position_features(): jnp.cos(angle)]
    reshape x3, local copies, waits for them, and re-layouts: 0.2 us -> 2.2 us  [the longest x1 0.84 us: on_device(): pieces = pieces.reshape(blocks, 12, tok_rows)]
  transfers between devices with their start and end apart: 1 -> 1, of which waited for: 0 -> 1; matrix products, arithmetic and copies ran while one was open for 32% -> 3% of each run, Pallas kernels for 0% -> 11%
where the time goes in v1:
time: 80 us; the launch traced here: 79.6 us
  blocking collectives  37 us (46%)
  starting transfers between devices  17.1 us (21%)
  Pallas kernels  13.5 us (17%)
  local copies, waits for them, and re-layouts  7.06 us (9%)
  matrix products  3.5 us (4%)
  waiting for transfers between devices  1.25 us (2%)
    all_to_all x1, blocking collectives, on_device(): returned = lax.all_to_all(gated, ROW, 0, 0, tiled=True)  21.8 us
    all_to_all x1, starting transfers between devices, on_device(): arrived = lax.all_to_all(pieces, ROW, 0, 0, tiled=True)  17.1 us
    all_to_all x1, blocking collectives, on_device(): lax.all_to_all(jnp.broadcast_to(returned[None], (lax.axis_size('x'), *ret...  9.34 us
    pallas_call x1, Pallas kernels, on_device(): pl.pallas_call(filter_kernel, out_shape=(spec, spec), in_specs=[vmem] * 1...  8.81 us
    all_gather x1, blocking collectives, on_device(): everyone = lax.all_gather(everyone, 'core', axis=1)  5.89 us
    pallas_call x1, Pallas kernels, on_device(): pl.pallas_call(conv_kernel, out_shape=jax.ShapeDtypeStruct((2 * blocks, s...  4.71 us
    unnamed x20, local copies, waits for them, and re-layouts  3.22 us
    dot_general x3, matrix products, on_device(): jnp.einsum('std,dc->sct', tokens, weight, preferred_element_type=F32)  2.5 us
  transfers between devices with their start and end apart: 1, of which 1 were waited for; matrix products, arithmetic and copies ran while one was open for 3% of the time, Pallas kernels for 11%

profile of v1, /device:TPU:1, one launch (start us, length us, event | category | flops | bytes accessed | tf_op | source)
XLA Modules:
  0.0 79.6 jit_solution(8048407262976400210)
XLA Ops:
  0.0 0.0 copy-start
  0.0 1.2 %copy-done = bf16[2,128,2048]{2,1,0:T(8,128)(2,1)S(1)} copy-done((bf16[2,128,2048]{2,1,0:T(8,128)(2,1)S(1)}, bf16[2,128,2048]{2,1,0:T(8,128)(2,1)}, u32[]{:S(2)}) %copy-start) | copy-done | bytes 1048600
  1.2 1.5 %convolution_convert_fusion.3 = bf16[128,2,128]{2,0,1:T(8,128)(2,1)S(1)} fusion(bf16[2,128,2048]{2,1,0:T(8,128)(2,1)S(1)} %copy-done, bf16[2048,128]{1,0:T(8,128)(2,1)} %param.28), kind=kOutput, calls=%fused_computation.3 | convolution fusion | flops 134250496 | bytes 1638400 | tf_op jit(solution)/shard_map/std,dc->sct/dot_general | solution.py:234
  2.8 0.0 copy-start.2
  2.8 0.0 copy-done.1
  2.8 0.5 convolution_convert_fusion.2
  3.3 0.5 copy-done.2
  3.8 0.0 copy-start.7
  3.8 0.0 copy-start.6
  3.8 0.0 copy-start.5
  3.8 0.5 convolution_convert_fusion.1
  4.4 0.8 %copy.42 = bf16[64,12,128]{2,1,0:T(8,128)(2,1)} copy(bf16[64,12,128]{2,0,1:T(8,128)(2,1)S(1)} %bitcast.31) | data formatting | bytes 393216 | tf_op jit(solution)/shard_map/reshape | solution.py:239
  5.2 17.1 %all-to-all-start = ((bf16[64,12,128]{2,1,0:T(8,128)(2,1)}), bf16[64,12,128]{2,1,0:T(8,128)(2,1)S(1)}, u32[]{:S(2)}, u32[]{:S(2)}) async-start(bf16[64,12,128]{2,1,0:T(8,128)(2,1)} %copy.42), calls=%async_computation | async-start | bytes 524288 | tf_op jit(solution)/shard_map/all_to_all | solution.py:240
  22.3 0.0 copy-done.7
  22.4 0.6 reshape.30.taps_ref
  23.0 0.0 copy-done.6
  23.0 0.1 copy.43
  23.0 0.0 copy-done.5
  23.0 0.7 copy.44
  23.7 0.0 copy-done.4
  23.7 0.8 reshape.31.out_ref
  24.5 0.6 pad.4.in_ref
  25.1 8.8 %filter_spectra.1 = (f32[2,256,128]{2,1,0:T(8,128)}, f32[2,256,128]{2,1,0:T(8,128)}) custom-call(f32[40,8192]{1,0:T(8,128)} %constant.50.clone.features_ref, f32[64,40]{1,0:T(8,128)} %pad.4.in_ref, f32[64,64]{1,0:T(8,128)} %bitcast.37, f32[64,512]{1,0:T(8,128)} %reshape.31.out_ref, f32[1,128]{1,0:T(1,128)} %bitcast.38, ...), custom_call_target="tpu_custom_call" | custom-call | flops 4000000000 | bytes 3000000 | tf_op jit(solution)/shard_map/filter_spectra/pallas_call | solution.py:247
  33.9 1.3 %all-to-all-done.x_ref = bf16[64,12,128]{2,1,0:T(8,128)(2,1)S(1)} async-done(((bf16[64,12,128]{2,1,0:T(8,128)(2,1)}), bf16[64,12,128]{2,1,0:T(8,128)(2,1)S(1)}, u32[]{:S(2)}, u32[]{:S(2)}) %all-to-all-start) | async-done | bytes 196640 | tf_op jit(solution)/shard_map/all_to_all | solution.py:240
  35.2 0.7 copy-done.3
  35.9 4.7 %gated_conv.1 = bf16[128,256]{1,0:T(8,128)(2,1)} custom-call(bf16[64,12,128]{2,1,0:T(8,128)(2,1)} %copy-done.3, f32[9,128]{1,0:T(8,128)} %reshape.30.taps_ref, f32[2,128]{1,0:T(2,128)} %gain_ref.1, f32[2,256,128]{2,1,0:T(8,128)} %get-tuple-element.7.spec_re_ref, f32[2,256,128]{2,1,0:T(8,128)} %get-tuple-element.8.spec_im_ref, ...), custom_call_target="tpu_custom_call" | custom-call | flops 4000000000 | bytes 2000000 | tf_op jit(solution)/shard_map/gated_conv/pallas_call | solution.py:268
  40.6 0.9 %all_to_all.13 = bf16[64,2,256]{2,1,0:T(2,128)(2,1)S(1)} reshape(bf16[128,256]{1,0:T(8,128)(2,1)} %gated_conv.1) | data formatting | bytes 131072 | tf_op jit(solution)/shard_map/all_to_all | solution.py:293
  41.5 21.8 %all_to_all.19 = bf16[64,2,256]{2,1,0:T(2,128)(2,1)S(1)} all-to-all(bf16[64,2,256]{2,1,0:T(2,128)(2,1)S(1)} %all_to_all.13), channel_id=1, replica_groups=mesh['row_0'=8,'row_1'=8,'x'=4,'core'=2] {'row_0','row_1'}, dimensions={0} | all-to-all | bytes 131072 | tf_op jit(solution)/shard_map/all_to_all | solution.py:293
  63.4 9.3 %all_to_all.20 = bf16[4,128,256]{2,1,0:T(8,128)(2,1)S(1)} all-to-all(bf16[4,128,256]{2,1,0:T(8,128)(2,1)S(1)} %broadcast_in_dim.9), channel_id=1, replica_groups=mesh['row_0'=8,'row_1'=8,'x'=4,'core'=2] {'x'}, dimensions={0} | all-to-all | bytes 524288 | tf_op jit(solution)/shard_map/all_to_all | solution.py:294
  72.7 5.9 %all-gather = bf16[4,256,256]{2,1,0:T(8,128)(2,1)S(1)} all-gather(bf16[4,128,256]{2,1,0:T(8,128)(2,1)S(1)} %all_to_all.20), channel_id=2, replica_groups=mesh['row_0'=8,'row_1'=8,'x'=4,'core'=2] {'core'}, dimensions={1}, use_global_device_ids=true | all-gather | bytes 786432 | tf_op jit(solution)/shard_map/all_gather | solution.py:297
  78.6 0.0 copy-done.8
  78.6 1.0 %convolution_convert_fusion = bf16[256,256]{1,0:T(8,128)(2,1)} fusion(bf16[1024,256]{1,0:T(8,128)(2,1)S(1)} %bitcast.32, bf16[1024,256]{1,0:T(8,128)(2,1)S(1)} %copy-done.8), kind=kOutput, calls=%fused_computation | convolution fusion | flops 134283264 | bytes 1179648 | tf_op jit(solution)/shard_map/ct,cd->td/dot_general | solution.py:299
  (10 shorter events, 0.1 us)
Async XLA Ops:
  0.0 1.2 %copy-start = (bf16[2,128,2048]{2,1,0:T(8,128)(2,1)S(1)}, bf16[2,128,2048]{2,1,0:T(8,128)(2,1)}, u32[]{:S(2)}) copy-start(bf16[2,128,2048]{2,1,0:T(8,128)(2,1)} %param.27) | copy-start | bytes 3145732
  0.0 2.8 %copy-start.1 = (bf16[2048,128]{1,0:T(8,128)(2,1)S(1)}, bf16[2048,128]{1,0:T(8,128)(2,1)}, u32[]{:S(2)}) copy-start(bf16[2048,128]{1,0:T(8,128)(2,1)} %param.29) | copy-start | bytes 1572868
  2.8 1.0 %copy-start.2 = (bf16[2048,128]{1,0:T(8,128)(2,1)S(1)}, bf16[2048,128]{1,0:T(8,128)(2,1)}, u32[]{:S(2)}) copy-start(bf16[2048,128]{1,0:T(8,128)(2,1)} %param.30) | copy-start | bytes 1572868
  3.8 18.5 %copy-start.7 = (f32[3,3,128]{2,1,0:T(4,128)S(1)}, f32[3,3,128]{2,1,0:T(4,128)}, u32[]{:S(2)}) copy-start(f32[3,3,128]{2,1,0:T(4,128)} %param.31) | copy-start | bytes 13828
  3.8 19.1 %copy-start.6 = (f32[33,64]{1,0:T(8,128)S(1)}, f32[33,64]{1,0:T(8,128)}, u32[]{:S(2)}) copy-start(f32[33,64]{1,0:T(8,128)} %param.32) | copy-start | bytes 25348
  3.8 19.2 %copy-start.5 = (f32[64,64]{1,0:T(8,128)S(1)}, f32[64,64]{1,0:T(8,128)}, u32[]{:S(2)}) copy-start(f32[64,64]{1,0:T(8,128)} %param.33) | copy-start | bytes 49156
  3.8 19.9 %copy-start.4 = (f32[64,2,2,128]{3,2,1,0:T(2,128)S(1)}, f32[64,2,2,128]{3,2,1,0:T(2,128)}, u32[]{:S(2)}) copy-start(f32[64,2,2,128]{3,2,1,0:T(2,128)} %param.34) | copy-start | bytes 393220
  5.2 30.0 %all-to-all-start = ((bf16[64,12,128]{2,1,0:T(8,128)(2,1)}), bf16[64,12,128]{2,1,0:T(8,128)(2,1)S(1)}, u32[]{:S(2)}, u32[]{:S(2)}) async-start(bf16[64,12,128]{2,1,0:T(8,128)(2,1)} %copy.42), calls=%async_computation | async-start | bytes 524288 | tf_op jit(solution)/shard_map/all_to_all | solution.py:240
  35.2 0.7 copy-start.3
  40.6 38.0 %copy-start.8 = (bf16[1024,256]{1,0:T(8,128)(2,1)S(1)}, bf16[1024,256]{1,0:T(8,128)(2,1)}, u32[]{:S(2)}) copy-start(bf16[1024,256]{1,0:T(8,128)(2,1)} %param.37) | copy-start | bytes 1572868

commit v2 on v1

--- a/solution.py
+++ b/solution.py
@@ -27,30 +27,22 @@
 @functools.lru_cache(None)
 def tables(length, feats):
     bands = (feats - 1) // 2
-    lag = np.arange(length, dtype=np.float64)
-    freq = np.linspace(0.0001, bands - 1, bands)
-    angle = (2.0 * math.pi / length) * lag[None, :] * freq[:, None]
-    features = np.concatenate(
-        [lag[None, :] / (length - 1), np.cos(angle), -np.sin(angle), np.zeros((40 - feats, length))]
-    )
+    freq = np.linspace(0.0001, bands - 1, bands)[:, None] * (2.0 * math.pi / length)
+    coarse, near = freq * np.arange(SIDE) * SIDE, freq * np.arange(SIDE)
+    waves = np.stack([np.cos(coarse), np.sin(coarse), np.cos(near), np.sin(near)])
     index = np.arange(SIDE)
     turn = 2.0 * math.pi / SIDE * (index[:, None] * index[None, :] % SIDE)
     cos, sin = np.cos(turn), np.sin(turn)
     fine = 2.0 * math.pi / (SIDE * SIDE) * (index[:, None] * index[None, :])
-    real_in = np.concatenate([cos[:, :HALF], -sin[:, :HALF]])
     pair_in = np.block([[cos[:, :HALF], sin[:, :HALF]], [-sin[:, :HALF], cos[:, :HALF]]])
     right = np.block([[cos, -sin], [sin, cos]])
     split = {}
-    split["real_in"] = halves(real_in)
     split["pair_in"] = halves(pair_in)
     split["pair_out"] = halves(pair_in.T)
     split["right"] = halves(right)
     split["back"] = halves(right.T)
-    split["spec_re"] = halves(np.concatenate([cos, sin]))
-    split["spec_im"] = halves(np.concatenate([-sin, cos]))
-    return np.asarray(features, np.float32), np.stack([np.cos(fine), np.sin(fine)]).astype(
-        np.float32
-    ), split
+    fine = np.stack([np.cos(fine), np.sin(fine)])
+    return waves.astype(np.float32), fine.astype(np.float32), split
 
 
 def hi_lo(value):
@@ -84,12 +76,42 @@
     return poly * quarter
 
 
+def project_kernel(steps, tok_hbm, a_hbm, b_hbm, c_hbm, o_ref, tok, weights, flat_ref, wide_ref, sems):
+    depth = tok.shape[2] // steps
+    copies = []
+    for step in range(steps):
+        cut = pl.ds(step * depth, depth)
+        group = [pltpu.make_async_copy(tok_hbm.at[:, :, cut], tok.at[:, :, cut], sems.at[step, 3])]
+        for p, source in enumerate((a_hbm, b_hbm, c_hbm)):
+            group.append(
+                pltpu.make_async_copy(source.at[cut, :], weights.at[p, cut, :], sems.at[step, p])
+            )
+        for copy in group:
+            copy.start()
+        copies.append(group)
+    sums = [[None] * 3, [None] * 3]
+    for step in range(steps):
+        for copy in copies[step]:
+            copy.wait()
+        cut = slice(step * depth, (step + 1) * depth)
+        for s in range(2):
+            for p in range(3):
+                part = mm(tok[s, :, cut], weights[p, cut, :])
+                sums[s][p] = part if step == 0 else sums[s][p] + part
+    for s in range(2):
+        for p in range(3):
+            flat_ref[s * 3 + p] = sums[s][p].T
+            for c in range(2):
+                wide_ref[:, (p * 2 + s) * 2 + c, :] = flat_ref[s * 3 + p, pl.ds(c, HALF, stride=2), :]
+    o_ref[...] = wide_ref[...].astype(BF)
+
+
 def filter_kernel(
-    features_ref, in_ref, mid_ref, out_ref, rate_ref, fine_ref,
-    real_hi, real_lo, re_hi, re_lo, im_hi, im_lo,
-    spec_re_ref, spec_im_ref, rows_ref,
+    waves_ref, in_ref, mid_ref, out_ref, rate_ref, fine_ref,
+    in_hi_ref, in_lo_ref, right_hi, right_lo,
+    spec_re_ref, spec_im_ref, rows_ref, pad_ref,
 ):
-    length = features_ref.shape[1]
+    length = HALF * SIDE
     device = lax.axis_index("row_0") * lax.axis_size("row_1") + lax.axis_index("row_1")
     lane = lax.broadcasted_iota(jnp.int32, (8, SIDE), 1)
     row = lax.broadcasted_iota(jnp.int32, (8, SIDE), 0)
@@ -100,24 +122,50 @@
     out_lo = jnp.zeros((8, out_ref.shape[0]), F32)
     for pair in range(4):
         pick = jnp.where(mine & (row // 2 == pair), 1.0, 0.0).astype(BF)
-        top, low = hi_lo(out_ref[:, pair * SIDE : (pair + 1) * SIDE])
+        top, low = hi_lo(out_ref[:, pair // 2, pair % 2, :])
         out_hi += mm(pick, top, last)
         out_lo += mm(pick, low, last)
     out_hi, out_lo = out_hi.astype(BF), out_lo.astype(BF)
     rate = jnp.sum(jnp.where(mine, rate_ref[...], 0.0), axis=1, keepdims=True)
     scale = 1.0 / (2.0 * math.pi)
-    in_hi, in_lo = hi_lo(in_ref[...] * scale)
+    pad_ref[...] = jnp.zeros_like(pad_ref)
+    pad_ref[:32, :] = in_ref[1:33, :] * scale
+    pad_ref[32:33, :] = in_ref[0:1, :] * scale
+    in_hi, in_lo = hi_lo(pad_ref[...])
+    in_all = jnp.concatenate([in_hi, in_lo, in_hi], axis=0)
     mid_hi, mid_lo = hi_lo(mid_ref[...] * scale)
     out_all = jnp.concatenate([out_hi, out_lo, out_hi], axis=1)
-    mid_all = jnp.concatenate([mid_hi, mid_lo, mid_hi], axis=1)
+    mid_all = jnp.concatenate([mid_hi, mid_lo, mid_hi], axis=0)
     chunk = 1024
+    cos_near, sin_near = waves_ref[2], waves_ref[3]
+    wide_lane = lax.broadcasted_iota(jnp.int32, (16, SIDE), 1)
+    top_row = lax.broadcasted_iota(jnp.int32, (16, SIDE), 0) == 0
+    ramp_step = 1.0 / (length - 1)
+
+    def features(block):
+        cos_far = waves_ref[0, :, block : block + 1]
+        sin_far = waves_ref[1, :, block : block + 1]
+        ramp = jnp.where(top_row, (wide_lane + block * SIDE).astype(F32) * ramp_step, 0.0)
+        return jnp.concatenate(
+            [
+                cos_far * cos_near - sin_far * sin_near,
+                -(sin_far * cos_near + cos_far * sin_near),
+                ramp,
+            ],
+            axis=0,
+        )
+
     squares = jnp.zeros((8, SIDE), F32)
     sign = jnp.where(lax.broadcasted_iota(jnp.int32, (8, SIDE), 0) < 4, 1.0, -1.0)
     for start in range(0, length, chunk):
-        top, low = hi_lo(features_ref[:, start : start + chunk])
-        turns = mm(in_hi, top) + mm(in_lo, top) + mm(in_hi, low)
+        top, low = hi_lo(
+            jnp.concatenate(
+                [features(b) for b in range(start // SIDE, (start + chunk) // SIDE)], axis=1
+            )
+        )
+        turns = mm(in_all, jnp.concatenate([top, top, low], axis=0), first)
         top, low = hi_lo(sine_of_turns(turns))
-        turns = mm(mid_all, jnp.concatenate([top, top, low], axis=0))
+        turns = mm(mid_all, jnp.concatenate([top, top, low], axis=0), first)
         top, low = hi_lo(sine_of_turns(turns))
         shaped = mm(out_all, jnp.concatenate([top, top, low], axis=0))
         for piece in range(chunk // SIDE):
@@ -132,7 +180,7 @@
     total = jnp.sum(squares + pltpu.roll(squares, 4, 0), axis=1, keepdims=True)
     factor = lax.rsqrt(total + 1e-06) * (1.0 / (SIDE * SIDE))
     grid = jnp.concatenate([rows_ref[:, j, :] * factor[j : j + 1, :] for j in range(8)], axis=1)
-    grid = left_const(real_hi[...], real_lo[...], grid)
+    grid = left_const(in_hi_ref[:, :HALF], in_lo_ref[:, :HALF], grid)
     cos, sin = fine_ref[0], fine_ref[1]
 
     def turned(j):
@@ -144,8 +192,12 @@
         for channel in range(2):
             j = order * 2 + channel
             rows = pl.ds(channel * SIDE, SIDE)
-            spec_re_ref[order, rows, :] = right_const(turned(j), re_hi[...], re_lo[...])
-            spec_im_ref[order, rows, :] = right_const(turned(j + 4), im_hi[...], im_lo[...])
+            spec_re_ref[order, rows, :] = right_const(
+                turned(j), right_hi[:, :SIDE], right_lo[:, :SIDE]
+            )
+            spec_im_ref[order, rows, :] = right_const(
+                turned(j + 4), right_hi[:, SIDE:], right_lo[:, SIDE:]
+            )
 
 
 def conv_kernel(
@@ -172,7 +224,7 @@
                 after = jnp.where((lane == SIDE - 1) & (row == HALF - 1), 0.0, after)
                 at = 2 * device + c
                 chans.append(
-                    taps_ref[p, at] * prev + taps_ref[3 + p, at] * here + taps_ref[6 + p, at] * after
+                    taps_ref[0, p, at] * prev + taps_ref[1, p, at] * here + taps_ref[2, p, at] * after
                 )
             seqs.append(jnp.concatenate(chans, axis=1))
         return jnp.concatenate(seqs, axis=0)
@@ -205,10 +257,10 @@
         state = smoothed(order + 1) * (reach + gain * state)
     for s in range(2):
         for c in range(2):
-            rows_ref[s, pl.ds(c, HALF, stride=2), :] = state[
+            rows_ref[:, c, pl.ds(s * SIDE, SIDE)] = state[
                 s * HALF : (s + 1) * HALF, c * SIDE : (c + 1) * SIDE
             ]
-        o_ref[:, pl.ds(s * SIDE, SIDE)] = rows_ref[s].astype(BF)
+    o_ref[...] = rows_ref[...].astype(BF)
 
 
 def on_device(
@@ -228,59 +280,72 @@
     blocks = lax.axis_size(ROW)
     length = tok_rows * blocks
     feats = filter_in.shape[0]
-    features, fine, split = tables(length, feats)
-    projected = jnp.stack(
-        [
-            jnp.einsum("std,dc->sct", tokens, weight, preferred_element_type=F32).astype(BF)
-            for weight in (w_value, w_first, w_second)
-        ]
-    )
-    pieces = projected.reshape(3, seqs, blocks, 2, tok_rows).transpose(2, 0, 1, 3, 4)
-    pieces = pieces.reshape(blocks, 12, tok_rows)
-    arrived = lax.all_to_all(pieces, ROW, 0, 0, tiled=True)
-
+    waves, fine, split = tables(length, feats)
+    far = pl.BlockSpec(memory_space=pltpu.HBM)
     vmem = pl.BlockSpec(memory_space=pltpu.VMEM)
     smem = pl.BlockSpec(memory_space=pltpu.SMEM)
+    steps = 4
+    pieces = pl.pallas_call(
+        functools.partial(project_kernel, steps),
+        out_shape=jax.ShapeDtypeStruct((blocks, 12, tok_rows), BF),
+        in_specs=[far] * 4,
+        out_specs=vmem,
+        scratch_shapes=[
+            pltpu.VMEM(tokens.shape, BF),
+            pltpu.VMEM((3, *w_value.shape), BF),
+            pltpu.VMEM((6, SIDE, SIDE), F32),
+            pltpu.VMEM((HALF, 12, SIDE), F32),
+            pltpu.SemaphoreType.DMA((steps, 4)),
+        ],
+        compiler_params=pltpu.CompilerParams(vmem_limit_bytes=66_700_000),
+        name="project",
+    )(tokens, w_value, w_first, w_second)
+    arrived = lax.all_to_all(pieces, ROW, 0, 0, tiled=True)
+
     fine = jnp.asarray(fine)
     spec = jax.ShapeDtypeStruct((2, 2 * SIDE, SIDE), F32)
     const = {k: tuple(jnp.asarray(h) for h in v) for k, v in split.items()}
     spec_re, spec_im = pl.pallas_call(
         filter_kernel,
         out_shape=(spec, spec),
-        in_specs=[vmem] * 12,
+        in_specs=[vmem] * 10,
         out_specs=(vmem, vmem),
-        scratch_shapes=[pltpu.VMEM((HALF, 8, SIDE), F32)],
+        scratch_shapes=[
+            pltpu.VMEM((HALF, 8, SIDE), F32),
+            pltpu.VMEM((48, filter_in.shape[1]), F32),
+        ],
+        compiler_params=pltpu.CompilerParams(vmem_limit_bytes=16 * 2**20),
         cost_estimate=pl.CostEstimate(
             flops=4_000_000_000, bytes_accessed=3_000_000, transcendentals=0
         ),
         name="filter_spectra",
     )(
-        jnp.asarray(features),
-        jnp.pad(filter_in.T, ((0, 0), (0, 40 - feats))),
-        filter_mid.T,
-        filter_out.reshape(filter_out.shape[0], -1),
+        jnp.asarray(waves),
+        filter_in,
+        filter_mid,
+        filter_out,
         decay_rate.reshape(1, -1),
         fine,
-        *const["real_in"],
-        *const["spec_re"],
-        *const["spec_im"],
+        *const["pair_in"],
+        *const["right"],
     )
     gated = pl.pallas_call(
         conv_kernel,
-        out_shape=jax.ShapeDtypeStruct((2 * blocks, seqs * tok_rows), BF),
+        out_shape=jax.ShapeDtypeStruct((blocks, 2, seqs * tok_rows), BF),
         in_specs=[vmem, smem, smem] + [vmem] * 11,
         out_specs=vmem,
         scratch_shapes=[
             pltpu.VMEM((HALF, 12, SIDE), F32),
-            pltpu.VMEM((2, SIDE, SIDE), F32),
+            pltpu.VMEM((HALF, 2, 2 * SIDE), F32),
         ],
+        compiler_params=pltpu.CompilerParams(vmem_limit_bytes=16 * 2**20),
         cost_estimate=pl.CostEstimate(
             flops=4_000_000_000, bytes_accessed=2_000_000, transcendentals=0
         ),
         name="gated_conv",
     )(
         arrived,
-        short_taps.reshape(9, -1),
+        short_taps,
         skip_gain,
         spec_re,
         spec_im,
@@ -291,6 +356,7 @@
         *const["back"],
     )
     returned = lax.all_to_all(gated, ROW, 0, 0, tiled=True)
+    returned = returned.reshape(2 * blocks, seqs * tok_rows)
     everyone = lax.all_to_all(
         jnp.broadcast_to(returned[None], (lax.axis_size("x"), *returned.shape)), "x", 0, 0, tiled=True
     )

time: 80 us -> 71.9 us (0.90)
  local copies, waits for them, and re-layouts: 7.06 us -> 1.34 us
  waiting for transfers between devices: 1.25 us -> 5.83 us
  blocking collectives: 37 us -> 32.6 us
  matrix products: 3.5 us -> 1 us
    all_to_all x1, waiting for transfers between devices: 1.25 us -> 5.83 us  [on_device(): arrived = lax.all_to_all(pieces, ROW, 0, 0, tiled=True)]
    all_to_all x1, blocking collectives: 21.8 us -> 17.2 us  [on_device(): returned = lax.all_to_all(gated, ROW, 0, 0, tiled=True)]
    dot_general x3 -> x0, matrix products: 2.5 us -> none  [on_device(): jnp.einsum('std,dc->sct', tokens, weight, preferred_element_type=F32)]
    pallas_call x1, Pallas kernels: 8.81 us -> 6.32 us  [on_device(): pl.pallas_call(filter_kernel, out_shape=(spec, spec), in_specs=[vmem] * 1...]
    pallas_call x1 -> x2, Pallas kernels: 4.71 us -> 7.07 us  [the longest x1 3.69 us: on_device(): pl.pallas_call(functools.partial(project_kernel, steps), out_shape=jax.Sh...]
    reshape x3 -> x0, local copies, waits for them, and re-layouts: 2.2 us -> none  [the longest x1 0.84 us: on_device(): pieces = pieces.reshape(blocks, 12, tok_rows)]
    unnamed x20 -> x34, local copies, waits for them, and re-layouts: 3.22 us -> 1.28 us
    all_to_all x1 -> x0, local copies, waits for them, and re-layouts: 0.93 us -> none  [on_device(): returned = lax.all_to_all(gated, ROW, 0, 0, tiled=True)]
  transfers between devices with their start and end apart: 1 -> 1, of which waited for: 1 -> 1; matrix products, arithmetic and copies ran while one was open for 3% -> 0% of each run, Pallas kernels for 11% -> 9%
where the time goes in v2:
time: 71.9 us; the launch traced here: 71.6 us
  blocking collectives  32.6 us (45%)
  starting transfers between devices  17.3 us (24%)
  Pallas kernels  13.4 us (19%)
  waiting for transfers between devices  5.83 us (8%)
  local copies, waits for them, and re-layouts  1.34 us (2%)
  matrix products  1 us (1%)
    all_to_all x1, starting transfers between devices, on_device(): arrived = lax.all_to_all(pieces, ROW, 0, 0, tiled=True)  17.3 us
    all_to_all x1, blocking collectives, on_device(): returned = lax.all_to_all(gated, ROW, 0, 0, tiled=True)  17.2 us
    all_to_all x1, blocking collectives, on_device(): lax.all_to_all(jnp.broadcast_to(returned[None], (lax.axis_size('x'), *ret...  9.34 us
    pallas_call x1, Pallas kernels, on_device(): pl.pallas_call(filter_kernel, out_shape=(spec, spec), in_specs=[vmem] * 1...  6.32 us
    all_gather x1, blocking collectives, on_device(): everyone = lax.all_gather(everyone, 'core', axis=1)  6.03 us
    all_to_all x1, waiting for transfers between devices, on_device(): arrived = lax.all_to_all(pieces, ROW, 0, 0, tiled=True)  5.83 us
    pallas_call x1, Pallas kernels, on_device(): pl.pallas_call(functools.partial(project_kernel, steps), out_shape=jax.Sh...  3.69 us
    pallas_call x1, Pallas kernels, on_device(): pl.pallas_call(conv_kernel, out_shape=jax.ShapeDtypeStruct((blocks, 2, se...  3.38 us
  transfers between devices with their start and end apart: 1, of which 1 were waited for; matrix products, arithmetic and copies ran while one was open for 0% of the time, Pallas kernels for 9%

profile of v2, /device:TPU:1, one launch (start us, length us, event | category | flops | bytes accessed | tf_op | source)
XLA Modules:
  0.0 71.6 jit_solution(4892848369295445512)
XLA Ops:
  0.0 3.7 %project.1 = bf16[64,12,128]{2,1,0:T(8,128)(2,1)} custom-call(bf16[2,128,2048]{2,1,0:T(8,128)(2,1)} %tok_hbm.1, bf16[2048,128]{1,0:T(8,128)(2,1)} %a_hbm.1, bf16[2048,128]{1,0:T(8,128)(2,1)} %b_hbm.1, bf16[2048,128]{1,0:T(8,128)(2,1)} %c_hbm.1), custom_call_target="tpu_custom_call" | custom-call | tf_op jit(solution)/shard_map/project/pallas_call | solution.py:288
  3.7 0.0 copy-start
  3.7 0.0 copy-start.1
  3.7 0.0 copy-start.2
  3.7 0.0 copy-start.6
  3.8 0.0 copy-start.7
  3.8 0.0 copy-start.11
  3.8 17.3 %all-to-all-start = ((bf16[64,12,128]{2,1,0:T(8,128)(2,1)}), bf16[64,12,128]{2,1,0:T(8,128)(2,1)S(1)}, u32[]{:S(2)}, u32[]{:S(2)}) async-start(bf16[64,12,128]{2,1,0:T(8,128)(2,1)} %project.1), calls=%async_computation | async-start | bytes 524288 | tf_op jit(solution)/shard_map/all_to_all | solution.py:303
  21.1 0.0 copy-start.5
  21.1 0.0 copy-done.8
  21.1 0.0 copy-done.12
  21.1 0.0 copy-done.15
  21.1 0.0 copy-done
  21.1 0.0 copy-done.1
  21.1 0.0 copy-done.2
  21.1 0.0 copy-done.6
  21.1 0.0 copy-done.7
  21.1 0.0 copy-done.11
  21.2 0.6 copy-done.5
  21.7 0.0 copy-start.14
  21.7 6.3 %filter_spectra.1 = (f32[2,256,128]{2,1,0:T(8,128)S(1)}, f32[2,256,128]{2,1,0:T(8,128)S(1)}) custom-call(f32[4,16,128]{2,1,0:T(8,128)S(1)} %copy-done.15, f32[33,64]{1,0:T(8,128)S(1)} %copy-done.2, f32[64,64]{1,0:T(8,128)S(1)} %copy-done.1, f32[64,2,2,128]{3,2,1,0:T(2,128)S(1)} %copy-done, f32[1,128]{1,0:T(1,128)S(1)} %bitcast.5, ...), custom_call_target="tpu_custom_call" | custom-call | flops 4000000000 | bytes 3000000 | tf_op jit(solution)/shard_map/filter_spectra/pallas_call | solution.py:308
  28.1 5.8 %all-to-all-done.x_ref = bf16[64,12,128]{2,1,0:T(8,128)(2,1)S(1)} async-done(((bf16[64,12,128]{2,1,0:T(8,128)(2,1)}), bf16[64,12,128]{2,1,0:T(8,128)(2,1)S(1)}, u32[]{:S(2)}, u32[]{:S(2)}) %all-to-all-start) | async-done | bytes 196640 | tf_op jit(solution)/shard_map/all_to_all | solution.py:303
  33.9 0.0 copy-done.3
  33.9 0.0 copy-done.9
  33.9 0.0 copy-done.10
  33.9 0.6 copy-done.4
  34.6 3.4 %gated_conv.1 = bf16[64,2,256]{2,1,0:T(2,128)(2,1)S(1)} custom-call(bf16[64,12,128]{2,1,0:T(8,128)(2,1)S(1)} %all-to-all-done.x_ref, f32[3,3,128]{2,1,0:T(4,128)S(1)} %copy-done.3, f32[2,128]{1,0:T(2,128)S(1)} %copy-done.4, f32[2,256,128]{2,1,0:T(8,128)S(1)} %get-tuple-element.7.spec_re_ref, f32[2,256,128]{2,1,0:T(8,128)S(1)} %get-tuple-element.8.spec_im_ref, ...), custom_call_target="tpu_custom_call" | custom-call | flops 4000000000 | bytes 2000000 | tf_op jit(solution)/shard_map/gated_conv/pallas_call | solution.py:332
  38.0 17.2 %all_to_all.15 = bf16[64,2,256]{2,1,0:T(2,128)(2,1)S(1)} all-to-all(bf16[64,2,256]{2,1,0:T(2,128)(2,1)S(1)} %gated_conv.1), channel_id=1, replica_groups=mesh['row_0'=8,'row_1'=8,'x'=4,'core'=2] {'row_0','row_1'}, dimensions={0} | all-to-all | bytes 131072 | tf_op jit(solution)/shard_map/all_to_all | solution.py:358
  55.2 9.3 %all_to_all.16 = bf16[4,128,256]{2,1,0:T(8,128)(2,1)S(1)} all-to-all(bf16[4,128,256]{2,1,0:T(8,128)(2,1)S(1)} %broadcast_in_dim.8), channel_id=1, replica_groups=mesh['row_0'=8,'row_1'=8,'x'=4,'core'=2] {'x'}, dimensions={0} | all-to-all | bytes 524288 | tf_op jit(solution)/shard_map/all_to_all | solution.py:360
  64.6 6.0 %all-gather = bf16[4,256,256]{2,1,0:T(8,128)(2,1)S(1)} all-gather(bf16[4,128,256]{2,1,0:T(8,128)(2,1)S(1)} %all_to_all.16), channel_id=2, replica_groups=mesh['row_0'=8,'row_1'=8,'x'=4,'core'=2] {'core'}, dimensions={1}, use_global_device_ids=true | all-gather | bytes 786432 | tf_op jit(solution)/shard_map/all_gather | solution.py:363
  70.6 0.0 copy-done.16
  70.6 1.0 %convolution_convert_fusion = bf16[256,256]{1,0:T(8,128)(2,1)} fusion(bf16[1024,256]{1,0:T(8,128)(2,1)S(1)} %bitcast.6, bf16[1024,256]{1,0:T(8,128)(2,1)S(1)} %copy-done.16), kind=kOutput, calls=%fused_computation | convolution fusion | flops 134283264 | bytes 1179648 | tf_op jit(solution)/shard_map/ct,cd->td/dot_general | solution.py:365
  (13 shorter events, 0.1 us)
Async XLA Ops:
  0.0 21.1 %copy-start.8 = (f32[2,128,128]{2,1,0:T(8,128)S(1)}, f32[2,128,128]{2,1,0:T(8,128)}, u32[]{:S(2)}) copy-start(f32[2,128,128]{2,1,0:T(8,128)} %constant.20.clone.fine_ref) | copy-start | bytes 393220
  0.0 21.1 %copy-start.12 = (bf16[256,128]{1,0:T(8,128)(2,1)S(1)}, bf16[256,128]{1,0:T(8,128)(2,1)}, u32[]{:S(2)}) copy-start(bf16[256,128]{1,0:T(8,128)(2,1)} %constant.21.clone.in_hi_ref.in_hi) | copy-start | bytes 196612
  0.0 21.1 %copy-start.15 = (f32[4,16,128]{2,1,0:T(8,128)S(1)}, f32[4,16,128]{2,1,0:T(8,128)}, u32[]{:S(2)}) copy-start(f32[4,16,128]{2,1,0:T(8,128)} %constant.29.clone.waves_ref) | copy-start | bytes 98308
  3.7 17.4 %copy-start = (f32[64,2,2,128]{3,2,1,0:T(2,128)S(1)}, f32[64,2,2,128]{3,2,1,0:T(2,128)}, u32[]{:S(2)}) copy-start(f32[64,2,2,128]{3,2,1,0:T(2,128)} %out_ref.1) | copy-start | bytes 393220
  3.7 17.4 %copy-start.1 = (f32[64,64]{1,0:T(8,128)S(1)}, f32[64,64]{1,0:T(8,128)}, u32[]{:S(2)}) copy-start(f32[64,64]{1,0:T(8,128)} %mid_ref.1) | copy-start | bytes 49156
  3.7 17.4 %copy-start.2 = (f32[33,64]{1,0:T(8,128)S(1)}, f32[33,64]{1,0:T(8,128)}, u32[]{:S(2)}) copy-start(f32[33,64]{1,0:T(8,128)} %in_ref.1) | copy-start | bytes 25348
  3.7 17.4 %copy-start.6 = (bf16[256,256]{1,0:T(8,128)(2,1)S(1)}, bf16[256,256]{1,0:T(8,128)(2,1)}, u32[]{:S(2)}) copy-start(bf16[256,256]{1,0:T(8,128)(2,1)} %constant.26.clone.right_lo) | copy-start | bytes 393220
  3.8 17.4 %copy-start.7 = (bf16[256,256]{1,0:T(8,128)(2,1)S(1)}, bf16[256,256]{1,0:T(8,128)(2,1)}, u32[]{:S(2)}) copy-start(bf16[256,256]{1,0:T(8,128)(2,1)} %constant.25.clone.right_hi) | copy-start | bytes 393220
  3.8 17.4 %copy-start.11 = (bf16[256,128]{1,0:T(8,128)(2,1)S(1)}, bf16[256,128]{1,0:T(8,128)(2,1)}, u32[]{:S(2)}) copy-start(bf16[256,128]{1,0:T(8,128)(2,1)} %constant.22.clone.in_lo_ref.in_lo) | copy-start | bytes 196612
  3.8 30.1 %all-to-all-start = ((bf16[64,12,128]{2,1,0:T(8,128)(2,1)}), bf16[64,12,128]{2,1,0:T(8,128)(2,1)S(1)}, u32[]{:S(2)}, u32[]{:S(2)}) async-start(bf16[64,12,128]{2,1,0:T(8,128)(2,1)} %project.1), calls=%async_computation | async-start | bytes 524288 | tf_op jit(solution)/shard_map/all_to_all | solution.py:303
  21.1 0.7 copy-start.5
  21.7 12.2 %copy-start.3 = (f32[3,3,128]{2,1,0:T(4,128)S(1)}, f32[3,3,128]{2,1,0:T(4,128)}, u32[]{:S(2)}) copy-start(f32[3,3,128]{2,1,0:T(4,128)} %taps_ref.1) | copy-start | bytes 13828
  21.7 12.2 %copy-start.9 = (bf16[256,256]{1,0:T(8,128)(2,1)S(1)}, bf16[256,256]{1,0:T(8,128)(2,1)}, u32[]{:S(2)}) copy-start(bf16[256,256]{1,0:T(8,128)(2,1)} %constant.28.clone.back_lo) | copy-start | bytes 393220
  21.7 12.2 %copy-start.10 = (bf16[256,256]{1,0:T(8,128)(2,1)S(1)}, bf16[256,256]{1,0:T(8,128)(2,1)}, u32[]{:S(2)}) copy-start(bf16[256,256]{1,0:T(8,128)(2,1)} %constant.27.clone.back_hi) | copy-start | bytes 393220
  21.7 12.2 %copy-start.13 = (bf16[128,256]{1,0:T(8,128)(2,1)S(1)}, bf16[128,256]{1,0:T(8,128)(2,1)}, u32[]{:S(2)}) copy-start(bf16[128,256]{1,0:T(8,128)(2,1)} %constant.24.clone.out_lo) | copy-start | bytes 196612
  21.7 12.2 %copy-start.14 = (bf16[128,256]{1,0:T(8,128)(2,1)S(1)}, bf16[128,256]{1,0:T(8,128)(2,1)}, u32[]{:S(2)}) copy-start(bf16[128,256]{1,0:T(8,128)(2,1)} %constant.23.clone.out_hi) | copy-start | bytes 196612
  33.9 0.7 copy-start.4
  64.6 6.0 %copy-start.16 = (bf16[1024,256]{1,0:T(8,128)(2,1)S(1)}, bf16[1024,256]{1,0:T(8,128)(2,1)}, u32[]{:S(2)}) copy-start(bf16[1024,256]{1,0:T(8,128)(2,1)} %param.31) | copy-start | bytes 1572868

commit v3 on v2

v3 whole, which is shorter than its diff:
```python
import functools
import math

import jax
import jax.numpy as jnp
import numpy as np
from jax import lax
from jax.experimental import pallas as pl
from jax.experimental.pallas import tpu as pltpu
from jax.sharding import Mesh
from jax.sharding import PartitionSpec as P

ROW = ("row_0", "row_1")
COL = ("x", "core")
SIDE = 128
HALF = SIDE // 2
MAPS_FIRST = 6 * SIDE
BF = jnp.bfloat16
F32 = jnp.float32


def halves(table):
    table = np.asarray(table, np.float32)
    top = table.astype(jnp.bfloat16)
    return top, (table - top.astype(np.float32)).astype(jnp.bfloat16)


@functools.lru_cache(None)
def tables(length, feats):
    bands = (feats - 1) // 2
    freq = np.linspace(0.0001, bands - 1, bands)[:, None] * (2.0 * math.pi / length)
    coarse, near = freq * np.arange(SIDE) * SIDE, freq * np.arange(SIDE)
    waves = np.stack([np.cos(coarse), np.sin(coarse), np.cos(near), np.sin(near)])
    index = np.arange(SIDE)
    turn = 2.0 * math.pi / SIDE * (index[:, None] * index[None, :] % SIDE)
    cos, sin = np.cos(turn), np.sin(turn)
    fine = 2.0 * math.pi / (SIDE * SIDE) * (index[:, None] * index[None, :])
    pair_in = np.block([[cos[:, :HALF], sin[:, :HALF]], [-sin[:, :HALF], cos[:, :HALF]]])
    right = np.block([[cos, -sin], [sin, cos]])
    in_hi, in_lo = halves(pair_in)
    out_hi, out_lo = halves(pair_in.T)
    right_hi, right_lo = halves(right)
    back_hi, back_lo = halves(right.T)
    maps = np.concatenate(
        [right_hi, right_lo, np.concatenate([in_hi, in_lo], axis=1), back_hi, back_lo, out_hi, out_lo]
    )
    angles = np.concatenate([np.cos(fine), np.sin(fine), *waves]).astype(np.float32)
    return angles, maps[:MAPS_FIRST], maps[MAPS_FIRST:]


def hi_lo(value):
    top = value.astype(BF)
    return top, (value - top.astype(F32)).astype(BF)


def mm(a, b, dims=(((1,), (0,)), ((), ()))):
    return lax.dot_general(a, b, dims, preferred_element_type=F32)


def left_const(const_hi, const_lo, value):
    top, low = hi_lo(value)
    return mm(const_hi, top) + mm(const_lo, top) + mm(const_hi, low)


def right_const(value, const_hi, const_lo):
    top, low = hi_lo(value)
    return mm(top, const_hi) + mm(low, const_hi) + mm(top, const_lo)


def sine_of_turns(turns):
    big = 12582912.0
    moved = turns - 0.25
    moved = moved - ((moved + big) - big)
    quarter = 0.25 - jnp.abs(moved)
    square = quarter * quarter
    poly = -70.98993302 * square + 81.34038614
    poly = poly * square - 41.33713041
    poly = poly * square + 6.28316395
    return poly * quarter


def project_kernel(
    steps, tok_hbm, a_hbm, b_hbm, c_hbm, o_ref, tok, weights, sum_ref, flat_ref, wide_ref, sems
):
    depth = tok.shape[1] // steps

    def group_of(step, cut):
        group = []
        for s in range(2):
            group.append((tok_hbm.at[s, :, cut], tok.at[pl.ds(s * SIDE, SIDE), cut]))
        for p, source in enumerate((a_hbm, b_hbm, c_hbm)):
            group.append((source.at[cut, :], weights.at[cut, pl.ds(p * SIDE, SIDE)]))
        return [
            pltpu.make_async_copy(near, far, sems.at[step, k]) for k, (near, far) in enumerate(group)
        ]

    for step in range(steps):
        for copy in group_of(step, pl.ds(step * depth, depth)):
            copy.start()
    sum_ref[...] = jnp.zeros_like(sum_ref)

    @pl.loop(0, steps)
    def _(step):
        cut = pl.ds(pl.multiple_of(step * depth, depth), depth)
        for copy in group_of(step, cut):
            copy.wait()
        sum_ref[...] += mm(tok[:, cut], weights[cut, :])

    @pl.loop(0, 3)
    def _(p):
        cut = pl.ds(pl.multiple_of(p * SIDE, SIDE), SIDE)
        for s in range(2):
            flat_ref[s] = sum_ref[s * SIDE : (s + 1) * SIDE, cut].T
            for c in range(2):
                wide_ref[:, s * 2 + c, :] = flat_ref[s, pl.ds(c, HALF, stride=2), :]
        o_ref[:, :, cut] = wide_ref[...].astype(BF)


def filter_kernel(
    angles_ref, maps_ref, in_ref, mid_ref, out_ref, rate_ref, taps_ref, gain_ref,
    spec_re_ref, spec_im_ref, coef_ref, rows_ref, pad_ref,
):
    length = HALF * SIDE
    device = lax.axis_index("row_0") * lax.axis_size("row_1") + lax.axis_index("row_1")
    lane = lax.broadcasted_iota(jnp.int32, (8, SIDE), 1)
    row = lax.broadcasted_iota(jnp.int32, (8, SIDE), 0)
    mine = lane == 2 * device + row % 2
    last = (((1,), (1,)), ((), ()))
    first = (((0,), (0,)), ((), ()))
    out_hi = jnp.zeros((8, out_ref.shape[0]), F32)
    out_lo = jnp.zeros((8, out_ref.shape[0]), F32)
    for pair in range(4):
        pick = jnp.where(mine & (row // 2 == pair), 1.0, 0.0).astype(BF)
        top, low = hi_lo(out_ref[:, pair // 2, pair % 2, :])
        out_hi += mm(pick, top, last)
        out_lo += mm(pick, low, last)
    out_hi, out_lo = out_hi.astype(BF), out_lo.astype(BF)
    rate = jnp.sum(jnp.where(mine, rate_ref[...], 0.0), axis=1, keepdims=True)
    for c in range(2):
        sources = [(tap, taps_ref[tap], 0) for tap in range(3)] + [(3, gain_ref[...], 1)]
        for at, source, shift in sources:
            count = source.shape[0]
            at_lane = lax.broadcasted_iota(jnp.int32, (count, SIDE), 1) == 2 * device + c
            value = jnp.sum(jnp.where(at_lane, source, 0.0), axis=1, keepdims=True)
            value = jnp.broadcast_to(value, (count, SIDE))
            for k in range(count):
                coef_ref[k + shift, at : at + 1, c * SIDE : (c + 1) * SIDE] = value[k : k + 1]
    scale = 1.0 / (2.0 * math.pi)
    pad_ref[...] = jnp.zeros_like(pad_ref)
    pad_ref[:32, :] = in_ref[1:33, :] * scale
    pad_ref[32:33, :] = in_ref[0:1, :] * scale
    in_hi, in_lo = hi_lo(pad_ref[...])
    in_all = jnp.concatenate([in_hi, in_lo, in_hi], axis=0)
    mid_hi, mid_lo = hi_lo(mid_ref[...] * scale)
    out_all = jnp.concatenate([out_hi, out_lo, out_hi], axis=1)
    mid_all = jnp.concatenate([mid_hi, mid_lo, mid_hi], axis=0)
    chunk = 1024
    blocks = chunk // SIDE
    sign = jnp.where(row < 4, 1.0, -1.0)
    cos_near, sin_near = (
        angles_ref[2 * SIDE + 16 * k : 2 * SIDE + 16 * (k + 1), :] for k in (2, 3)
    )
    top_row = lax.broadcasted_iota(jnp.int32, (16, SIDE), 0) == 0
    wide_lane = lax.broadcasted_iota(jnp.int32, (16, SIDE), 1)

    def one_chunk(step, squares):
        cos_far, sin_far = (
            pltpu.roll(
                angles_ref[2 * SIDE + 16 * k : 2 * SIDE + 16 * (k + 1), :], SIDE - step * blocks, 1
            )
            for k in (0, 1)
        )
        pieces = []
        for piece in range(blocks):
            far_c, far_s = cos_far[:, piece : piece + 1], sin_far[:, piece : piece + 1]
            lag = (wide_lane + (step * blocks + piece) * SIDE).astype(F32)
            pieces.append(
                jnp.concatenate(
                    [
                        far_c * cos_near - far_s * sin_near,
                        -(far_s * cos_near + far_c * sin_near),
                        jnp.where(top_row, lag * (1.0 / (length - 1)), 0.0),
                    ],
                    axis=0,
                )
            )
        top, low = hi_lo(jnp.concatenate(pieces, axis=1))
        turns = mm(in_all, jnp.concatenate([top, top, low], axis=0), first)
        top, low = hi_lo(sine_of_turns(turns))
        turns = mm(mid_all, jnp.concatenate([top, top, low], axis=0), first)
        top, low = hi_lo(sine_of_turns(turns))
        shaped = mm(out_all, jnp.concatenate([top, top, low], axis=0))
        for piece in range(blocks):
            lag = lane + (step * blocks + piece) * SIDE
            part = shaped[:, piece * SIDE : (piece + 1) * SIDE] * jnp.exp(-rate * lag.astype(F32))
            part = jnp.where((row >= 4) & (lag == 0), 0.0, part)
            squares += part * part
            rows_ref[step * blocks + piece] = pltpu.roll(part, 4, 0) + part * sign
        return squares

    squares = lax.fori_loop(0, length // chunk, one_chunk, jnp.zeros((8, SIDE), F32))
    total = jnp.sum(squares + pltpu.roll(squares, 4, 0), axis=1, keepdims=True)
    factor = lax.rsqrt(total + 1e-06) * (1.0 / (SIDE * SIDE))
    grid = jnp.concatenate([rows_ref[:, j, :] * factor[j : j + 1, :] for j in range(8)], axis=1)
    grid = left_const(
        maps_ref[4 * SIDE :, :HALF], maps_ref[4 * SIDE :, SIDE : SIDE + HALF], grid
    )
    cos, sin = angles_ref[:SIDE, :], angles_ref[SIDE : 2 * SIDE, :]

    def turned(j):
        real = grid[:SIDE, j * SIDE : (j + 1) * SIDE]
        imag = grid[SIDE:, j * SIDE : (j + 1) * SIDE]
        return jnp.concatenate([real * cos + imag * sin, imag * cos - real * sin], axis=1)

    for order in range(2):
        for channel in range(2):
            j = order * 2 + channel
            rows = pl.ds(channel * SIDE, SIDE)
            spec_re_ref[order, rows, :] = right_const(
                turned(j), maps_ref[: 2 * SIDE, :SIDE], maps_ref[2 * SIDE : 4 * SIDE, :SIDE]
            )
            spec_im_ref[order, rows, :] = right_const(
                turned(j + 4), maps_ref[: 2 * SIDE, SIDE:], maps_ref[2 * SIDE : 4 * SIDE, SIDE:]
            )


def conv_kernel(
    x_ref, coef_ref, spec_re_ref, spec_im_ref, angles_ref, maps_ref, more_ref,
    o_ref, wide_ref, rows_ref,
):
    wide_ref[...] = x_ref[...].astype(F32)
    row = lax.broadcasted_iota(jnp.int32, (HALF, SIDE), 0)
    lane = lax.broadcasted_iota(jnp.int32, (HALF, SIDE), 1)

    def smoothed(p):
        seqs = []
        cut = pl.ds(pl.multiple_of(p * SIDE, SIDE), SIDE)
        for s in range(2):
            chans = []
            for c in range(2):
                here = wide_ref[:, s * 2 + c, cut]
                moved = pltpu.roll(here, 1, 1)
                prev = jnp.where(lane == 0, pltpu.roll(moved, 1, 0), moved)
                prev = jnp.where((lane == 0) & (row == 0), 0.0, prev)
                moved = pltpu.roll(here, SIDE - 1, 1)
                after = jnp.where(lane == SIDE - 1, pltpu.roll(moved, HALF - 1, 0), moved)
                after = jnp.where((lane == SIDE - 1) & (row == HALF - 1), 0.0, after)
                first, second, third = (
                    coef_ref[p, tap : tap + 1, c * SIDE : (c + 1) * SIDE] for tap in range(3)
                )
                chans.append(first * prev + second * here + third * after)
            seqs.append(jnp.concatenate(chans, axis=1))
        return jnp.concatenate(seqs, axis=0)

    cos, sin = angles_ref[:SIDE, :], angles_ref[SIDE : 2 * SIDE, :]
    cos2, sin2 = jnp.concatenate([cos, cos], axis=1), jnp.concatenate([sin, sin], axis=1)

    def one_order(order, state):
        grid = left_const(maps_ref[4 * SIDE :, :SIDE], maps_ref[4 * SIDE :, SIDE:], state)
        real, imag = grid[:SIDE], grid[SIDE:]
        real, imag = real * cos2 + imag * sin2, imag * cos2 - real * sin2
        grid = jnp.concatenate(
            [
                jnp.concatenate([real[:, :SIDE], imag[:, :SIDE]], axis=1),
                jnp.concatenate([real[:, SIDE:], imag[:, SIDE:]], axis=1),
            ],
            axis=0,
        )
        grid = right_const(grid, maps_ref[: 2 * SIDE, :], maps_ref[2 * SIDE : 4 * SIDE, :])
        real, imag = grid[:, :SIDE], grid[:, SIDE:]
        k_re, k_im = spec_re_ref[order], spec_im_ref[order]
        grid = jnp.concatenate([real * k_re - imag * k_im, real * k_im + imag * k_re], axis=1)
        grid = right_const(grid, more_ref[: 2 * SIDE, :], more_ref[2 * SIDE : 4 * SIDE, :])
        real = jnp.concatenate([grid[:SIDE, :SIDE], grid[SIDE:, :SIDE]], axis=1)
        imag = jnp.concatenate([grid[:SIDE, SIDE:], grid[SIDE:, SIDE:]], axis=1)
        grid = jnp.concatenate([real * cos2 - imag * sin2, real * sin2 + imag * cos2], axis=0)
        reach = left_const(more_ref[4 * SIDE : 5 * SIDE, :], more_ref[5 * SIDE :, :], grid)
        return smoothed(order + 1) * (reach + coef_ref[order + 1, 3:4, :] * state)

    state = lax.fori_loop(0, 2, one_order, smoothed(0))
    for s in range(2):
        for c in range(2):
            rows_ref[:, c, pl.ds(s * SIDE, SIDE)] = state[
                s * HALF : (s + 1) * HALF, c * SIDE : (c + 1) * SIDE
            ]
    o_ref[...] = rows_ref[...].astype(BF)


def on_device(
    tokens,
    w_value,
    w_first,
    w_second,
    short_taps,
    filter_in,
    filter_mid,
    filter_out,
    decay_rate,
    skip_gain,
    w_output,
):
    seqs, tok_rows, _ = tokens.shape
    blocks = lax.axis_size(ROW)
    length = tok_rows * blocks
    feats = filter_in.shape[0]
    angles, maps, more = (jnp.asarray(t) for t in tables(length, feats))
    far = pl.BlockSpec(memory_space=pltpu.HBM)
    vmem = pl.BlockSpec(memory_space=pltpu.VMEM)
    steps = 4
    pieces = pl.pallas_call(
        functools.partial(project_kernel, steps),
        out_shape=jax.ShapeDtypeStruct((blocks, 4, 3 * tok_rows), BF),
        in_specs=[far] * 4,
        out_specs=vmem,
        scratch_shapes=[
            pltpu.VMEM((seqs * tok_rows, tokens.shape[2]), BF),
            pltpu.VMEM((tokens.shape[2], 3 * SIDE), BF),
            pltpu.VMEM((seqs * tok_rows, 3 * SIDE), F32),
            pltpu.VMEM((2, SIDE, SIDE), F32),
            pltpu.VMEM((HALF, 4, SIDE), F32),
            pltpu.SemaphoreType.DMA((steps, 5)),
        ],
        compiler_params=pltpu.CompilerParams(vmem_limit_bytes=66_700_000),
        name="project",
    )(tokens, w_value, w_first, w_second)
    arrived = lax.all_to_all(pieces, ROW, 0, 0, tiled=True)

    spec = jax.ShapeDtypeStruct((2, 2 * SIDE, SIDE), F32)
    spec_re, spec_im, coef = pl.pallas_call(
        filter_kernel,
        out_shape=(spec, spec, jax.ShapeDtypeStruct((3, 8, 2 * SIDE), F32)),
        in_specs=[vmem] * 8,
        out_specs=(vmem, vmem, vmem),
        scratch_shapes=[
            pltpu.VMEM((HALF, 8, SIDE), F32),
            pltpu.VMEM((48, filter_in.shape[1]), F32),
        ],
        compiler_params=pltpu.CompilerParams(vmem_limit_bytes=16 * 2**20),
        cost_estimate=pl.CostEstimate(
            flops=4_000_000_000, bytes_accessed=3_000_000, transcendentals=0
        ),
        name="filter_spectra",
    )(
        angles,
        maps,
        filter_in,
        filter_mid,
        filter_out,
        decay_rate.reshape(1, -1),
        short_taps,
        skip_gain,
    )
    gated = pl.pallas_call(
        conv_kernel,
        out_shape=jax.ShapeDtypeStruct((blocks, 2, seqs * tok_rows), BF),
        in_specs=[vmem] * 7,
        out_specs=vmem,
        scratch_shapes=[
            pltpu.VMEM((HALF, 4, 3 * SIDE), F32),
            pltpu.VMEM((HALF, 2, 2 * SIDE), F32),
        ],
        compiler_params=pltpu.CompilerParams(vmem_limit_bytes=16 * 2**20),
        cost_estimate=pl.CostEstimate(
            flops=4_000_000_000, bytes_accessed=2_000_000, transcendentals=0
        ),
        name="gated_conv",
    )(
        arrived,
        coef,
        spec_re,
        spec_im,
        angles,
        maps,
        more,
    )
    returned = lax.all_to_all(gated, ROW, 0, 0, tiled=True)
    returned = returned.reshape(2 * blocks, seqs * tok_rows)
    everyone = lax.all_to_all(
        jnp.broadcast_to(returned[None], (lax.axis_size("x"), *returned.shape)), "x", 0, 0, tiled=True
    )
    everyone = lax.all_gather(everyone, "core", axis=1)
    everyone = everyone.reshape(-1, seqs * tok_rows)
    result = jnp.einsum("ct,cd->td", everyone, w_output, preferred_element_type=F32)
    return result.astype(BF).reshape(seqs, tok_rows, -1)


def solution(mesh):
    torus = Mesh(mesh.devices.reshape(8, 8, 4, 2), ("row_0", "row_1", "x", "core"))
    in_specs = (
        P(None, ROW, None),
        P(None, COL),
        P(None, COL),
        P(None, COL),
        P(None, None, COL),
        P(),
        P(),
        P(None, None, None, COL),
        P(COL),
        P(None, COL),
        P(None, COL),
    )
    out_specs = P(None, ROW, COL)
    return jax.shard_map(
        on_device, mesh=torus, in_specs=in_specs, out_specs=out_specs, check_vma=False
    )
```

time: 71.9 us -> 74.1 us (1.031)
  blocking collectives: 32.6 us -> 36.9 us
  waiting for transfers between devices: 5.83 us -> 1.55 us
  Pallas kernels: 13.4 us -> 15.2 us
    all_to_all x1, blocking collectives: 17.2 us -> 21.5 us  [on_device(): returned = lax.all_to_all(gated, ROW, 0, 0, tiled=True)]
    all_to_all x1, waiting for transfers between devices: 5.83 us -> 1.55 us  [on_device(): arrived = lax.all_to_all(pieces, ROW, 0, 0, tiled=True)]
    pallas_call x1, Pallas kernels: 6.32 us -> 8.78 us  [on_device(): pl.pallas_call(filter_kernel, out_shape=(spec, spec, jax.ShapeDtypeStruct...]
    pallas_call x1, Pallas kernels: 3.38 us -> 2.57 us  [on_device(): pl.pallas_call(conv_kernel, out_shape=jax.ShapeDtypeStruct((blocks, 2, se...]
    unnamed x34 -> x22, local copies, waits for them, and re-layouts: 1.28 us -> 1.66 us
  transfers between devices with their start and end apart: 1 -> 1, of which waited for: 1 -> 1; matrix products, arithmetic and copies ran while one was open for 0% -> 0% of each run, Pallas kernels for 9% -> 12%
where the time goes in v3:
time: 74.1 us; the launch traced here: 73.7 us
  blocking collectives  36.9 us (50%)
  starting transfers between devices  17.3 us (23%)
  Pallas kernels  15.2 us (21%)
  local copies, waits for them, and re-layouts  1.71 us (2%)
  waiting for transfers between devices  1.55 us (2%)
  matrix products  1 us (1%)
    all_to_all x1, blocking collectives, on_device(): returned = lax.all_to_all(gated, ROW, 0, 0, tiled=True)  21.5 us
    all_to_all x1, starting transfers between devices, on_device(): arrived = lax.all_to_all(pieces, ROW, 0, 0, tiled=True)  17.3 us
    all_to_all x1, blocking collectives, on_device(): lax.all_to_all(jnp.broadcast_to(returned[None], (lax.axis_size('x'), *ret...  9.35 us
    pallas_call x1, Pallas kernels, on_device(): pl.pallas_call(filter_kernel, out_shape=(spec, spec, jax.ShapeDtypeStruct...  8.78 us
    all_gather x1, blocking collectives, on_device(): everyone = lax.all_gather(everyone, 'core', axis=1)  6.03 us
    pallas_call x1, Pallas kernels, on_device(): pl.pallas_call(functools.partial(project_kernel, steps), out_shape=jax.Sh...  3.82 us
    pallas_call x1, Pallas kernels, on_device(): pl.pallas_call(conv_kernel, out_shape=jax.ShapeDtypeStruct((blocks, 2, se...  2.57 us
    unnamed x22, local copies, waits for them, and re-layouts  1.66 us
  transfers between devices with their start and end apart: 1, of which 1 were waited for; matrix products, arithmetic and copies ran while one was open for 0% of the time, Pallas kernels for 12%

profile of v3, /device:TPU:1, one launch (start us, length us, event | category | flops | bytes accessed | tf_op | source)
XLA Modules:
  0.0 73.7 jit_solution(16529380839543058535)
XLA Ops:
  0.0 3.8 %project.1 = bf16[64,4,384]{2,1,0:T(4,128)(2,1)} custom-call(bf16[2,128,2048]{2,1,0:T(8,128)(2,1)} %tok_hbm.1, bf16[2048,128]{1,0:T(8,128)(2,1)} %a_hbm.1, bf16[2048,128]{1,0:T(8,128)(2,1)} %b_hbm.1, bf16[2048,128]{1,0:T(8,128)(2,1)} %c_hbm.1), custom_call_target="tpu_custom_call" | custom-call | tf_op jit(solution)/shard_map/project/pallas_call | solution.py:310
  3.8 0.0 copy-start
  3.8 0.0 copy-start.1
  3.9 0.0 copy-start.2
  3.9 0.0 copy-start.3
  3.9 0.0 copy-start.9
  3.9 17.3 %all-to-all-start = ((bf16[64,4,384]{2,1,0:T(4,128)(2,1)}), bf16[64,4,384]{2,1,0:T(4,128)(2,1)S(1)}, u32[]{:S(2)}, u32[]{:S(2)}) async-start(bf16[64,4,384]{2,1,0:T(4,128)(2,1)} %project.1), calls=%async_computation | async-start | bytes 393216 | tf_op jit(solution)/shard_map/all_to_all | solution.py:326
  21.2 0.0 copy-start.4
  21.2 0.0 copy-start.5
  21.2 0.0 copy-done
  21.2 0.0 copy-done.1
  21.2 0.0 copy-done.2
  21.2 0.0 copy-done.3
  21.2 0.0 copy-done.9
  21.3 0.6 copy-done.4
  21.9 0.0 copy-done.5
  21.9 0.0 copy-start.6
  21.9 1.0 %copy-done.6 = bf16[768,256]{1,0:T(8,128)(2,1)S(1)} copy-done((bf16[768,256]{1,0:T(8,128)(2,1)S(1)}, bf16[768,256]{1,0:T(8,128)(2,1)}, u32[]{:S(2)}) %copy-start.6) | copy-done | bytes 393240
  22.9 0.0 copy-start.7
  22.9 0.0 copy-start.8
  22.9 8.8 %filter_spectra.1 = (f32[2,256,128]{2,1,0:T(8,128)S(1)}, f32[2,256,128]{2,1,0:T(8,128)S(1)}, f32[3,8,256]{2,1,0:T(8,128)S(1)}) custom-call(f32[320,128]{1,0:T(8,128)S(1)} %copy-done.9, bf16[768,256]{1,0:T(8,128)(2,1)S(1)} %copy-done.6, f32[33,64]{1,0:T(8,128)S(1)} %copy-done.2, f32[64,64]{1,0:T(8,128)S(1)} %copy-done.1, f32[64,2,2,128]{3,2,1,0:T(2,128)S(1)} %copy-done, ...), custom_call_target="tpu_custom_call" | custom-call | flops 4000000000 | bytes 3000000 | tf_op jit(solution)/shard_map/filter_spectra/pallas_call | solution.py:329
  31.6 1.5 %all-to-all-done.x_ref = bf16[64,4,384]{2,1,0:T(4,128)(2,1)S(1)} async-done(((bf16[64,4,384]{2,1,0:T(4,128)(2,1)}), bf16[64,4,384]{2,1,0:T(4,128)(2,1)S(1)}, u32[]{:S(2)}, u32[]{:S(2)}) %all-to-all-start) | async-done | bytes 196640 | tf_op jit(solution)/shard_map/all_to_all | solution.py:326
  33.2 0.0 copy-done.7
  33.2 0.0 copy-done.8
  33.2 2.6 %gated_conv.1 = bf16[64,2,256]{2,1,0:T(2,128)(2,1)S(1)} custom-call(bf16[64,4,384]{2,1,0:T(4,128)(2,1)S(1)} %all-to-all-done.x_ref, f32[3,8,256]{2,1,0:T(8,128)S(1)} %get-tuple-element.8.coef_ref, f32[2,256,128]{2,1,0:T(8,128)S(1)} %get-tuple-element.9.spec_re_ref, f32[2,256,128]{2,1,0:T(8,128)S(1)} %get-tuple-element.10.spec_im_ref, ...), custom_call_target="tpu_custom_call" | custom-call | flops 4000000000 | bytes 2000000 | tf_op jit(solution)/shard_map/gated_conv/pallas_call | solution.py:353
  35.8 21.5 %all_to_all.15 = bf16[64,2,256]{2,1,0:T(2,128)(2,1)S(1)} all-to-all(bf16[64,2,256]{2,1,0:T(2,128)(2,1)S(1)} %gated_conv.1), channel_id=1, replica_groups=mesh['row_0'=8,'row_1'=8,'x'=4,'core'=2] {'row_0','row_1'}, dimensions={0} | all-to-all | bytes 131072 | tf_op jit(solution)/shard_map/all_to_all | solution.py:376
  57.3 9.3 %all_to_all.16 = bf16[4,128,256]{2,1,0:T(8,128)(2,1)S(1)} all-to-all(bf16[4,128,256]{2,1,0:T(8,128)(2,1)S(1)} %broadcast_in_dim.8), channel_id=1, replica_groups=mesh['row_0'=8,'row_1'=8,'x'=4,'core'=2] {'x'}, dimensions={0} | all-to-all | bytes 524288 | tf_op jit(solution)/shard_map/all_to_all | solution.py:378
  66.7 0.0 copy-start.10
  66.7 6.0 %all-gather = bf16[4,256,256]{2,1,0:T(8,128)(2,1)S(1)} all-gather(bf16[4,128,256]{2,1,0:T(8,128)(2,1)S(1)} %all_to_all.16), channel_id=2, replica_groups=mesh['row_0'=8,'row_1'=8,'x'=4,'core'=2] {'core'}, dimensions={1}, use_global_device_ids=true | all-gather | bytes 786432 | tf_op jit(solution)/shard_map/all_gather | solution.py:381
  72.7 0.0 copy-done.10
  72.7 1.0 %convolution_convert_fusion = bf16[256,256]{1,0:T(8,128)(2,1)} fusion(bf16[1024,256]{1,0:T(8,128)(2,1)S(1)} %bitcast.6, bf16[1024,256]{1,0:T(8,128)(2,1)S(1)} %copy-done.10), kind=kOutput, calls=%fused_computation | convolution fusion | flops 134283264 | bytes 1179648 | tf_op jit(solution)/shard_map/ct,cd->td/dot_general | solution.py:383
  (2 shorter events, 0.1 us)
Async XLA Ops:
  3.8 17.4 %copy-start = (f32[64,2,2,128]{3,2,1,0:T(2,128)S(1)}, f32[64,2,2,128]{3,2,1,0:T(2,128)}, u32[]{:S(2)}) copy-start(f32[64,2,2,128]{3,2,1,0:T(2,128)} %out_ref.1) | copy-start | bytes 393220
  3.8 17.4 %copy-start.1 = (f32[64,64]{1,0:T(8,128)S(1)}, f32[64,64]{1,0:T(8,128)}, u32[]{:S(2)}) copy-start(f32[64,64]{1,0:T(8,128)} %mid_ref.1) | copy-start | bytes 49156
  3.9 17.4 %copy-start.2 = (f32[33,64]{1,0:T(8,128)S(1)}, f32[33,64]{1,0:T(8,128)}, u32[]{:S(2)}) copy-start(f32[33,64]{1,0:T(8,128)} %in_ref.1) | copy-start | bytes 25348
  3.9 17.4 %copy-start.3 = (f32[3,3,128]{2,1,0:T(4,128)S(1)}, f32[3,3,128]{2,1,0:T(4,128)}, u32[]{:S(2)}) copy-start(f32[3,3,128]{2,1,0:T(4,128)} %taps_ref.1) | copy-start | bytes 13828
  3.9 17.4 %copy-start.9 = (f32[320,128]{1,0:T(8,128)S(1)}, f32[320,128]{1,0:T(8,128)}, u32[]{:S(2)}) copy-start(f32[320,128]{1,0:T(8,128)} %constant.6.clone.angles_ref) | copy-start | bytes 491524
  3.9 29.3 %all-to-all-start = ((bf16[64,4,384]{2,1,0:T(4,128)(2,1)}), bf16[64,4,384]{2,1,0:T(4,128)(2,1)S(1)}, u32[]{:S(2)}, u32[]{:S(2)}) async-start(bf16[64,4,384]{2,1,0:T(4,128)(2,1)} %project.1), calls=%async_computation | async-start | bytes 393216 | tf_op jit(solution)/shard_map/all_to_all | solution.py:326
  21.2 0.7 copy-start.4
  21.2 0.7 copy-start.5
  21.9 1.0 %copy-start.6 = (bf16[768,256]{1,0:T(8,128)(2,1)S(1)}, bf16[768,256]{1,0:T(8,128)(2,1)}, u32[]{:S(2)}) copy-start(bf16[768,256]{1,0:T(8,128)(2,1)} %constant.7.clone.maps_ref) | copy-start | bytes 1179652
  22.9 10.3 %copy-start.7 = (bf16[768,256]{1,0:T(8,128)(2,1)S(1)}, bf16[768,256]{1,0:T(8,128)(2,1)}, u32[]{:S(2)}) copy-start(bf16[768,256]{1,0:T(8,128)(2,1)} %constant.7.clone.maps_ref) | copy-start | bytes 1179652
  22.9 10.3 %copy-start.8 = (bf16[768,256]{1,0:T(8,128)(2,1)S(1)}, bf16[768,256]{1,0:T(8,128)(2,1)}, u32[]{:S(2)}) copy-start(bf16[768,256]{1,0:T(8,128)(2,1)} %constant.8.clone.more_ref) | copy-start | bytes 1179652
  66.7 6.0 %copy-start.10 = (bf16[1024,256]{1,0:T(8,128)(2,1)S(1)}, bf16[1024,256]{1,0:T(8,128)(2,1)}, u32[]{:S(2)}) copy-start(bf16[1024,256]{1,0:T(8,128)(2,1)} %param.24) | copy-start | bytes 1572868

commit v4 on v3

--- a/solution.py
+++ b/solution.py
@@ -14,7 +14,7 @@
 COL = ("x", "core")
 SIDE = 128
 HALF = SIDE // 2
-MAPS_FIRST = 6 * SIDE
+CHUNK = 4096
 BF = jnp.bfloat16
 F32 = jnp.float32
 
@@ -41,11 +41,13 @@
     out_hi, out_lo = halves(pair_in.T)
     right_hi, right_lo = halves(right)
     back_hi, back_lo = halves(right.T)
-    maps = np.concatenate(
-        [right_hi, right_lo, np.concatenate([in_hi, in_lo], axis=1), back_hi, back_lo, out_hi, out_lo]
-    )
-    angles = np.concatenate([np.cos(fine), np.sin(fine), *waves]).astype(np.float32)
-    return angles, maps[:MAPS_FIRST], maps[MAPS_FIRST:]
+    real_hi, real_lo = in_hi[:, :HALF], in_lo[:, :HALF]
+    real_all = np.concatenate([real_hi, real_lo, real_hi, np.zeros_like(real_hi)], axis=1)
+    rights = np.concatenate([right_hi, right_lo])
+    backs = np.concatenate([back_hi, back_lo])
+    ends = np.concatenate([np.concatenate([in_hi, in_lo], axis=1), out_hi, out_lo])
+    turns = np.concatenate([np.cos(fine), np.sin(fine)]).astype(np.float32)
+    return np.concatenate(waves).astype(np.float32), turns, real_all, rights, backs, ends
 
 
 def hi_lo(value):
@@ -67,10 +69,8 @@
     return mm(top, const_hi) + mm(low, const_hi) + mm(top, const_lo)
 
 
-def sine_of_turns(turns):
-    big = 12582912.0
-    moved = turns - 0.25
-    moved = moved - ((moved + big) - big)
+def sine_of_turns(moved):
+    moved = moved - jnp.round(moved)
     quarter = 0.25 - jnp.abs(moved)
     square = quarter * quarter
     poly = -70.98993302 * square + 81.34038614
@@ -116,9 +116,8 @@
         o_ref[:, :, cut] = wide_ref[...].astype(BF)
 
 
-def filter_kernel(
-    angles_ref, maps_ref, in_ref, mid_ref, out_ref, rate_ref, taps_ref, gain_ref,
-    spec_re_ref, spec_im_ref, coef_ref, rows_ref, pad_ref,
+def network_kernel(
+    waves_ref, in_ref, mid_ref, out_ref, rate_ref, rows_ref, factor_ref, side_ref
 ):
     length = HALF * SIDE
     device = lax.axis_index("row_0") * lax.axis_size("row_1") + lax.axis_index("row_1")
@@ -127,17 +126,80 @@
     mine = lane == 2 * device + row % 2
     last = (((1,), (1,)), ((), ()))
     first = (((0,), (0,)), ((), ()))
-    out_hi = jnp.zeros((8, out_ref.shape[0]), F32)
-    out_lo = jnp.zeros((8, out_ref.shape[0]), F32)
+    units = mid_ref.shape[0]
+    out_hi = jnp.zeros((8, units), F32)
+    out_lo = jnp.zeros((8, units), F32)
     for pair in range(4):
         pick = jnp.where(mine & (row // 2 == pair), 1.0, 0.0).astype(BF)
-        top, low = hi_lo(out_ref[:, pair // 2, pair % 2, :])
+        top, low = hi_lo(out_ref[pl.ds(pair, units, stride=4), :])
         out_hi += mm(pick, top, last)
         out_lo += mm(pick, low, last)
-    out_hi, out_lo = out_hi.astype(BF), out_lo.astype(BF)
+    out_all = jnp.concatenate([out_hi.astype(BF), out_lo.astype(BF)], axis=1)
     rate = jnp.sum(jnp.where(mine, rate_ref[...], 0.0), axis=1, keepdims=True)
+    scale = 1.0 / (2.0 * math.pi)
+    side_ref[...] = jnp.zeros_like(side_ref)
+    ramp_hi, ramp_lo = hi_lo(in_ref[0:1, :] * scale)
+    side_ref[0:1, :] = ramp_hi.astype(F32)
+    side_ref[1:2, :] = ramp_lo.astype(F32)
+    side_ref[2:3, :] = ramp_hi.astype(F32)
+    side_ref[3:4, :] = jnp.full((1, units), -0.25, F32)
+    side_ref[16:17, :] = jnp.full((1, units), -0.25, F32)
+    in_hi, in_lo = hi_lo(in_ref[1:33, :] * scale)
+    in_all = jnp.concatenate([in_hi, in_lo, in_hi, side_ref[0:16, :].astype(BF)], axis=0)
+    mid_hi, mid_lo = hi_lo(mid_ref[...] * scale)
+    mid_all = jnp.concatenate([mid_hi, mid_lo, mid_hi, side_ref[16:32, :].astype(BF)], axis=0)
+    chunk = CHUNK
+    cos_far, sin_far, cos_near, sin_near = (
+        waves_ref[16 * k : 16 * (k + 1), :] for k in range(4)
+    )
+    ones = jnp.ones((16, chunk), BF)
+    sign = jnp.where(row < 4, 1.0, -1.0)
+    squares = jnp.zeros((8, SIDE), F32)
+    blocks = chunk // SIDE
+    for start in range(0, HALF, blocks):
+        pieces, sides = [], []
+        for block in range(start, start + blocks):
+            far_c, far_s = cos_far[:, block : block + 1], sin_far[:, block : block + 1]
+            pieces.append(
+                jnp.concatenate(
+                    [
+                        far_c * cos_near - far_s * sin_near,
+                        -(far_s * cos_near + far_c * sin_near),
+                    ],
+                    axis=0,
+                )
+            )
+            ramp = (lane + block * SIDE).astype(F32) * (1.0 / (length - 1))
+            ramp_top = ramp.astype(BF).astype(F32)
+            ramp = jnp.where(row == 2, ramp - ramp_top, jnp.where(row < 2, ramp_top, 1.0))
+            sides.append(jnp.concatenate([ramp, jnp.zeros_like(ramp)], axis=0).astype(BF))
+        top, low = hi_lo(jnp.concatenate(pieces, axis=1))
+        side = jnp.concatenate(sides, axis=1)
+        moved = mm(in_all, jnp.concatenate([top, top, low, side], axis=0), first)
+        top, low = hi_lo(sine_of_turns(moved))
+        moved = mm(mid_all, jnp.concatenate([top, top, low, ones], axis=0), first)
+        top = sine_of_turns(moved).astype(BF)
+        shaped = mm(out_all, jnp.concatenate([top, top], axis=0))
+        for piece in range(blocks):
+            block = start + piece
+            lag = lane + block * SIDE
+            part = shaped[:, piece * SIDE : (piece + 1) * SIDE] * jnp.exp(-rate * lag.astype(F32))
+            if block == 0:
+                part = jnp.where((row >= 4) & (lag == 0), 0.0, part)
+            squares += part * part
+            rows_ref[block * 8 : (block + 1) * 8, :] = pltpu.roll(part, 4, 0) + part * sign
+    total = jnp.sum(squares + pltpu.roll(squares, 4, 0), axis=1, keepdims=True)
+    factor = lax.rsqrt(total + 1e-06) * (1.0 / (SIDE * SIDE))
+    factor_ref[...] = jnp.broadcast_to(factor, factor_ref.shape)
+
+
+def spectra_kernel(
+    rows_ref, factor_ref, turns_ref, real_ref, right_ref, taps_ref, gain_ref,
+    spec_re_ref, spec_im_ref, coef_ref,
+):
+    device = lax.axis_index("row_0") * lax.axis_size("row_1") + lax.axis_index("row_1")
+    sources = [(tap, taps_ref[tap], 0) for tap in range(3)] + [(3, gain_ref[...], 1)]
     for c in range(2):
-        sources = [(tap, taps_ref[tap], 0) for tap in range(3)] + [(3, gain_ref[...], 1)]
         for at, source, shift in sources:
             count = source.shape[0]
             at_lane = lax.broadcasted_iota(jnp.int32, (count, SIDE), 1) == 2 * device + c
@@ -145,87 +207,30 @@
             value = jnp.broadcast_to(value, (count, SIDE))
             for k in range(count):
                 coef_ref[k + shift, at : at + 1, c * SIDE : (c + 1) * SIDE] = value[k : k + 1]
-    scale = 1.0 / (2.0 * math.pi)
-    pad_ref[...] = jnp.zeros_like(pad_ref)
-    pad_ref[:32, :] = in_ref[1:33, :] * scale
-    pad_ref[32:33, :] = in_ref[0:1, :] * scale
-    in_hi, in_lo = hi_lo(pad_ref[...])
-    in_all = jnp.concatenate([in_hi, in_lo, in_hi], axis=0)
-    mid_hi, mid_lo = hi_lo(mid_ref[...] * scale)
-    out_all = jnp.concatenate([out_hi, out_lo, out_hi], axis=1)
-    mid_all = jnp.concatenate([mid_hi, mid_lo, mid_hi], axis=0)
-    chunk = 1024
-    blocks = chunk // SIDE
-    sign = jnp.where(row < 4, 1.0, -1.0)
-    cos_near, sin_near = (
-        angles_ref[2 * SIDE + 16 * k : 2 * SIDE + 16 * (k + 1), :] for k in (2, 3)
-    )
-    top_row = lax.broadcasted_iota(jnp.int32, (16, SIDE), 0) == 0
-    wide_lane = lax.broadcasted_iota(jnp.int32, (16, SIDE), 1)
-
-    def one_chunk(step, squares):
-        cos_far, sin_far = (
-            pltpu.roll(
-                angles_ref[2 * SIDE + 16 * k : 2 * SIDE + 16 * (k + 1), :], SIDE - step * blocks, 1
-            )
-            for k in (0, 1)
-        )
-        pieces = []
-        for piece in range(blocks):
-            far_c, far_s = cos_far[:, piece : piece + 1], sin_far[:, piece : piece + 1]
-            lag = (wide_lane + (step * blocks + piece) * SIDE).astype(F32)
-            pieces.append(
-                jnp.concatenate(
-                    [
-                        far_c * cos_near - far_s * sin_near,
-                        -(far_s * cos_near + far_c * sin_near),
-                        jnp.where(top_row, lag * (1.0 / (length - 1)), 0.0),
-                    ],
-                    axis=0,
-                )
-            )
-        top, low = hi_lo(jnp.concatenate(pieces, axis=1))
-        turns = mm(in_all, jnp.concatenate([top, top, low], axis=0), first)
-        top, low = hi_lo(sine_of_turns(turns))
-        turns = mm(mid_all, jnp.concatenate([top, top, low], axis=0), first)
-        top, low = hi_lo(sine_of_turns(turns))
-        shaped = mm(out_all, jnp.concatenate([top, top, low], axis=0))
-        for piece in range(blocks):
-            lag = lane + (step * blocks + piece) * SIDE
-            part = shaped[:, piece * SIDE : (piece + 1) * SIDE] * jnp.exp(-rate * lag.astype(F32))
-            part = jnp.where((row >= 4) & (lag == 0), 0.0, part)
-            squares += part * part
-            rows_ref[step * blocks + piece] = pltpu.roll(part, 4, 0) + part * sign
-        return squares
-
-    squares = lax.fori_loop(0, length // chunk, one_chunk, jnp.zeros((8, SIDE), F32))
-    total = jnp.sum(squares + pltpu.roll(squares, 4, 0), axis=1, keepdims=True)
-    factor = lax.rsqrt(total + 1e-06) * (1.0 / (SIDE * SIDE))
-    grid = jnp.concatenate([rows_ref[:, j, :] * factor[j : j + 1, :] for j in range(8)], axis=1)
-    grid = left_const(
-        maps_ref[4 * SIDE :, :HALF], maps_ref[4 * SIDE :, SIDE : SIDE + HALF], grid
-    )
-    cos, sin = angles_ref[:SIDE, :], angles_ref[SIDE : 2 * SIDE, :]
+    pieces = []
+    for j in range(8):
+        pieces.append(rows_ref[pl.ds(j, HALF, stride=8), :] * factor_ref[j : j + 1, :])
+    top, low = hi_lo(jnp.concatenate(pieces, axis=1))
+    grid = mm(real_ref[:, : 3 * HALF], jnp.concatenate([top, top, low], axis=0))
+    cos, sin = turns_ref[:SIDE, :], turns_ref[SIDE:, :]
 
     def turned(j):
         real = grid[:SIDE, j * SIDE : (j + 1) * SIDE]
         imag = grid[SIDE:, j * SIDE : (j + 1) * SIDE]
         return jnp.concatenate([real * cos + imag * sin, imag * cos - real * sin], axis=1)
 
-    for order in range(2):
-        for channel in range(2):
-            j = order * 2 + channel
-            rows = pl.ds(channel * SIDE, SIDE)
-            spec_re_ref[order, rows, :] = right_const(
-                turned(j), maps_ref[: 2 * SIDE, :SIDE], maps_ref[2 * SIDE : 4 * SIDE, :SIDE]
-            )
-            spec_im_ref[order, rows, :] = right_const(
-                turned(j + 4), maps_ref[: 2 * SIDE, SIDE:], maps_ref[2 * SIDE : 4 * SIDE, SIDE:]
-            )
+    for j in range(4):
+        rows = pl.ds(j % 2 * SIDE, SIDE)
+        spec_re_ref[j // 2, rows, :] = right_const(
+            turned(j), right_ref[: 2 * SIDE, :SIDE], right_ref[2 * SIDE :, :SIDE]
+        )
+        spec_im_ref[j // 2, rows, :] = right_const(
+            turned(j + 4), right_ref[: 2 * SIDE, SIDE:], right_ref[2 * SIDE :, SIDE:]
+        )
 
 
 def conv_kernel(
-    x_ref, coef_ref, spec_re_ref, spec_im_ref, angles_ref, maps_ref, more_ref,
+    x_ref, coef_ref, spec_re_ref, spec_im_ref, turns_ref, right_ref, back_ref, ends_ref,
     o_ref, wide_ref, rows_ref,
 ):
     wide_ref[...] = x_ref[...].astype(F32)
@@ -252,11 +257,11 @@
             seqs.append(jnp.concatenate(chans, axis=1))
         return jnp.concatenate(seqs, axis=0)
 
-    cos, sin = angles_ref[:SIDE, :], angles_ref[SIDE : 2 * SIDE, :]
+    cos, sin = turns_ref[:SIDE, :], turns_ref[SIDE:, :]
     cos2, sin2 = jnp.concatenate([cos, cos], axis=1), jnp.concatenate([sin, sin], axis=1)
 
     def one_order(order, state):
-        grid = left_const(maps_ref[4 * SIDE :, :SIDE], maps_ref[4 * SIDE :, SIDE:], state)
+        grid = left_const(ends_ref[: 2 * SIDE, :SIDE], ends_ref[: 2 * SIDE, SIDE:], state)
         real, imag = grid[:SIDE], grid[SIDE:]
         real, imag = real * cos2 + imag * sin2, imag * cos2 - real * sin2
         grid = jnp.concatenate(
@@ -266,15 +271,15 @@
             ],
             axis=0,
         )
-        grid = right_const(grid, maps_ref[: 2 * SIDE, :], maps_ref[2 * SIDE : 4 * SIDE, :])
+        grid = right_const(grid, right_ref[: 2 * SIDE, :], right_ref[2 * SIDE :, :])
         real, imag = grid[:, :SIDE], grid[:, SIDE:]
         k_re, k_im = spec_re_ref[order], spec_im_ref[order]
         grid = jnp.concatenate([real * k_re - imag * k_im, real * k_im + imag * k_re], axis=1)
-        grid = right_const(grid, more_ref[: 2 * SIDE, :], more_ref[2 * SIDE : 4 * SIDE, :])
+        grid = right_const(grid, back_ref[: 2 * SIDE, :], back_ref[2 * SIDE :, :])
         real = jnp.concatenate([grid[:SIDE, :SIDE], grid[SIDE:, :SIDE]], axis=1)
         imag = jnp.concatenate([grid[:SIDE, SIDE:], grid[SIDE:, SIDE:]], axis=1)
         grid = jnp.concatenate([real * cos2 - imag * sin2, real * sin2 + imag * cos2], axis=0)
-        reach = left_const(more_ref[4 * SIDE : 5 * SIDE, :], more_ref[5 * SIDE :, :], grid)
+        reach = left_const(ends_ref[2 * SIDE : 3 * SIDE, :], ends_ref[3 * SIDE :, :], grid)
         return smoothed(order + 1) * (reach + coef_ref[order + 1, 3:4, :] * state)
 
     state = lax.fori_loop(0, 2, one_order, smoothed(0))
@@ -303,7 +308,7 @@
     blocks = lax.axis_size(ROW)
     length = tok_rows * blocks
     feats = filter_in.shape[0]
-    angles, maps, more = (jnp.asarray(t) for t in tables(length, feats))
+    waves, turns, real_all, rights, backs, ends = (jnp.asarray(t) for t in tables(length, feats))
     far = pl.BlockSpec(memory_space=pltpu.HBM)
     vmem = pl.BlockSpec(memory_space=pltpu.VMEM)
     steps = 4
@@ -326,34 +331,43 @@
     arrived = lax.all_to_all(pieces, ROW, 0, 0, tiled=True)
 
     spec = jax.ShapeDtypeStruct((2, 2 * SIDE, SIDE), F32)
-    spec_re, spec_im, coef = pl.pallas_call(
-        filter_kernel,
-        out_shape=(spec, spec, jax.ShapeDtypeStruct((3, 8, 2 * SIDE), F32)),
-        in_specs=[vmem] * 8,
-        out_specs=(vmem, vmem, vmem),
-        scratch_shapes=[
-            pltpu.VMEM((HALF, 8, SIDE), F32),
-            pltpu.VMEM((48, filter_in.shape[1]), F32),
-        ],
+    units = filter_in.shape[1]
+    rows, factor = pl.pallas_call(
+        network_kernel,
+        out_shape=(
+            jax.ShapeDtypeStruct((8 * HALF, SIDE), F32),
+            jax.ShapeDtypeStruct((8, SIDE), F32),
+        ),
+        in_specs=[vmem] * 5,
+        out_specs=(vmem, vmem),
+        scratch_shapes=[pltpu.VMEM((32, units), F32)],
         compiler_params=pltpu.CompilerParams(vmem_limit_bytes=16 * 2**20),
         cost_estimate=pl.CostEstimate(
-            flops=4_000_000_000, bytes_accessed=3_000_000, transcendentals=0
+            flops=4_000_000_000, bytes_accessed=1_000_000, transcendentals=0
         ),
-        name="filter_spectra",
+        name="network",
     )(
-        angles,
-        maps,
+        waves,
         filter_in,
         filter_mid,
-        filter_out,
+        filter_out.reshape(4 * units, -1),
         decay_rate.reshape(1, -1),
-        short_taps,
-        skip_gain,
-    )
+    )
+    spec_re, spec_im, coef = pl.pallas_call(
+        spectra_kernel,
+        out_shape=(spec, spec, jax.ShapeDtypeStruct((3, 8, 2 * SIDE), F32)),
+        in_specs=[vmem] * 7,
+        out_specs=(vmem,) * 3,
+        compiler_params=pltpu.CompilerParams(vmem_limit_bytes=16 * 2**20),
+        cost_estimate=pl.CostEstimate(
+            flops=1_000_000_000, bytes_accessed=2_000_000, transcendentals=0
+        ),
+        name="spectra",
+    )(rows, factor, turns, real_all, rights, short_taps, skip_gain)
     gated = pl.pallas_call(
         conv_kernel,
         out_shape=jax.ShapeDtypeStruct((blocks, 2, seqs * tok_rows), BF),
-        in_specs=[vmem] * 7,
+        in_specs=[vmem] * 8,
         out_specs=vmem,
         scratch_shapes=[
             pltpu.VMEM((HALF, 4, 3 * SIDE), F32),
@@ -369,9 +383,10 @@
         coef,
         spec_re,
         spec_im,
-        angles,
-        maps,
-        more,
+        turns,
+        rights,
+        backs,
+        ends,
     )
     returned = lax.all_to_all(gated, ROW, 0, 0, tiled=True)
     returned = returned.reshape(2 * blocks, seqs * tok_rows)

time: 74.1 us -> 68.6 us (0.926)
  waiting for transfers between devices: 1.55 us -> 7.14 us
  blocking collectives: 36.9 us -> 31.4 us
  Pallas kernels: 15.2 us -> 9.91 us
    all_to_all x1, waiting for transfers between devices: 1.55 us -> 7.14 us  [on_device(): arrived = lax.all_to_all(pieces, ROW, 0, 0, tiled=True)]
    all_to_all x1, blocking collectives: 21.5 us -> 16.1 us  [on_device(): returned = lax.all_to_all(gated, ROW, 0, 0, tiled=True)]
    pallas_call x1 -> x2, Pallas kernels: 8.78 us -> 3.5 us  [the longest x1 2.67 us: on_device(): pl.pallas_call(network_kernel, out_shape=(jax.ShapeDtypeStruct((8 * HALF,...]
    unnamed x22 -> x26, local copies, waits for them, and re-layouts: 1.66 us -> 1.32 us
  transfers between devices with their start and end apart: 1 -> 1, of which waited for: 1 -> 1; matrix products, arithmetic and copies ran while one was open for 0% -> 0% of each run, Pallas kernels for 12% -> 5%
where the time goes in v4:
time: 68.6 us; the launch traced here: 68.3 us
  blocking collectives  31.4 us (46%)
  starting transfers between devices  17.3 us (25%)
  Pallas kernels  9.91 us (14%)
  waiting for transfers between devices  7.14 us (10%)
  local copies, waits for them, and re-layouts  1.37 us (2%)
  matrix products  1 us (1%)
    all_to_all x1, starting transfers between devices, on_device(): arrived = lax.all_to_all(pieces, ROW, 0, 0, tiled=True)  17.3 us
    all_to_all x1, blocking collectives, on_device(): returned = lax.all_to_all(gated, ROW, 0, 0, tiled=True)  16.1 us
    all_to_all x1, blocking collectives, on_device(): lax.all_to_all(jnp.broadcast_to(returned[None], (lax.axis_size('x'), *ret...  9.34 us
    all_to_all x1, waiting for transfers between devices, on_device(): arrived = lax.all_to_all(pieces, ROW, 0, 0, tiled=True)  7.14 us
    all_gather x1, blocking collectives, on_device(): everyone = lax.all_gather(everyone, 'core', axis=1)  5.98 us
    pallas_call x1, Pallas kernels, on_device(): pl.pallas_call(functools.partial(project_kernel, steps), out_shape=jax.Sh...  3.82 us
    pallas_call x1, Pallas kernels, on_device(): pl.pallas_call(network_kernel, out_shape=(jax.ShapeDtypeStruct((8 * HALF,...  2.67 us
    pallas_call x1, Pallas kernels, on_device(): pl.pallas_call(conv_kernel, out_shape=jax.ShapeDtypeStruct((blocks, 2, se...  2.58 us
  transfers between devices with their start and end apart: 1, of which 1 were waited for; matrix products, arithmetic and copies ran while one was open for 0% of the time, Pallas kernels for 5%

profile of v4, /device:TPU:1, one launch (start us, length us, event | category | flops | bytes accessed | tf_op | source)
XLA Modules:
  0.0 68.3 jit_solution(4299083353495164076)
XLA Ops:
  0.0 3.8 %project.1 = bf16[64,4,384]{2,1,0:T(4,128)(2,1)} custom-call(bf16[2,128,2048]{2,1,0:T(8,128)(2,1)} %tok_hbm.1, bf16[2048,128]{1,0:T(8,128)(2,1)} %a_hbm.1, bf16[2048,128]{1,0:T(8,128)(2,1)} %b_hbm.1, bf16[2048,128]{1,0:T(8,128)(2,1)} %c_hbm.1), custom_call_target="tpu_custom_call" | custom-call | tf_op jit(solution)/shard_map/project/pallas_call | solution.py:315
  3.8 0.0 copy-start
  3.8 0.0 copy-start.1
  3.9 0.0 copy-start.2
  3.9 0.0 copy-start.11
  3.9 17.3 %all-to-all-start = ((bf16[64,4,384]{2,1,0:T(4,128)(2,1)}), bf16[64,4,384]{2,1,0:T(4,128)(2,1)S(1)}, u32[]{:S(2)}, u32[]{:S(2)}) async-start(bf16[64,4,384]{2,1,0:T(4,128)(2,1)} %project.1), calls=%async_computation | async-start | bytes 393216 | tf_op jit(solution)/shard_map/all_to_all | solution.py:331
  21.2 0.0 copy-start.5
  21.2 0.0 copy-done
  21.2 0.0 copy-done.1
  21.2 0.0 copy-done.2
  21.2 0.0 copy-done.11
  21.2 0.6 copy-done.5
  21.8 0.0 copy-start.3
  21.8 0.0 copy-start.6
  21.8 0.0 copy-start.9
  21.8 0.0 copy-start.10
  21.8 2.7 %network.1 = (f32[512,128]{1,0:T(8,128)S(1)}, f32[8,128]{1,0:T(8,128)S(1)}) custom-call(f32[64,128]{1,0:T(8,128)S(1)} %copy-done.11, f32[33,64]{1,0:T(8,128)S(1)} %copy-done.2, f32[64,64]{1,0:T(8,128)S(1)} %copy-done.1, f32[256,128]{1,0:T(8,128)S(1)} %bitcast.6, f32[1,128]{1,0:T(1,128)S(1)} %bitcast.7), custom_call_target="tpu_custom_call" | custom-call | flops 4000000000 | bytes 1000000 | tf_op jit(solution)/shard_map/network/pallas_call | solution.py:335
  24.5 0.0 copy-done.3
  24.5 0.0 copy-done.6
  24.5 0.0 copy-done.9
  24.5 0.0 copy-done.10
  24.5 0.7 copy-done.4
  25.2 0.8 %spectra.1 = (f32[2,256,128]{2,1,0:T(8,128)S(1)}, f32[2,256,128]{2,1,0:T(8,128)S(1)}, f32[3,8,256]{2,1,0:T(8,128)S(1)}) custom-call(f32[512,128]{1,0:T(8,128)S(1)} %get-tuple-element.10.rows_ref, f32[8,128]{1,0:T(8,128)S(1)} %get-tuple-element.11.factor_ref, f32[256,128]{1,0:T(8,128)S(1)} %copy-done.9, bf16[256,256]{1,0:T(8,128)(2,1)S(1)} %copy-done.10, ...), custom_call_target="tpu_custom_call" | custom-call | flops 1000000000 | bytes 2000000 | tf_op jit(solution)/shard_map/spectra/pallas_call | solution.py:356
  26.0 7.1 %all-to-all-done.x_ref = bf16[64,4,384]{2,1,0:T(4,128)(2,1)S(1)} async-done(((bf16[64,4,384]{2,1,0:T(4,128)(2,1)}), bf16[64,4,384]{2,1,0:T(4,128)(2,1)S(1)}, u32[]{:S(2)}, u32[]{:S(2)}) %all-to-all-start) | async-done | bytes 196640 | tf_op jit(solution)/shard_map/all_to_all | solution.py:331
  33.2 0.0 copy-done.7
  33.2 0.0 copy-done.8
  33.2 2.6 %gated_conv.1 = bf16[64,2,256]{2,1,0:T(2,128)(2,1)S(1)} custom-call(bf16[64,4,384]{2,1,0:T(4,128)(2,1)S(1)} %all-to-all-done.x_ref, f32[3,8,256]{2,1,0:T(8,128)S(1)} %get-tuple-element.12.coef_ref, f32[2,256,128]{2,1,0:T(8,128)S(1)} %get-tuple-element.13.spec_re_ref, f32[2,256,128]{2,1,0:T(8,128)S(1)} %get-tuple-element.14.spec_im_ref, ...), custom_call_target="tpu_custom_call" | custom-call | flops 4000000000 | bytes 2000000 | tf_op jit(solution)/shard_map/gated_conv/pallas_call | solution.py:367
  35.8 16.1 %all_to_all.15 = bf16[64,2,256]{2,1,0:T(2,128)(2,1)S(1)} all-to-all(bf16[64,2,256]{2,1,0:T(2,128)(2,1)S(1)} %gated_conv.1), channel_id=1, replica_groups=mesh['row_0'=8,'row_1'=8,'x'=4,'core'=2] {'row_0','row_1'}, dimensions={0} | all-to-all | bytes 131072 | tf_op jit(solution)/shard_map/all_to_all | solution.py:391
  52.0 9.3 %all_to_all.16 = bf16[4,128,256]{2,1,0:T(8,128)(2,1)S(1)} all-to-all(bf16[4,128,256]{2,1,0:T(8,128)(2,1)S(1)} %broadcast_in_dim.8), channel_id=1, replica_groups=mesh['row_0'=8,'row_1'=8,'x'=4,'core'=2] {'x'}, dimensions={0} | all-to-all | bytes 524288 | tf_op jit(solution)/shard_map/all_to_all | solution.py:393
  61.3 6.0 %all-gather = bf16[4,256,256]{2,1,0:T(8,128)(2,1)S(1)} all-gather(bf16[4,128,256]{2,1,0:T(8,128)(2,1)S(1)} %all_to_all.16), channel_id=2, replica_groups=mesh['row_0'=8,'row_1'=8,'x'=4,'core'=2] {'core'}, dimensions={1}, use_global_device_ids=true | all-gather | bytes 786432 | tf_op jit(solution)/shard_map/all_gather | solution.py:396
  67.3 0.0 copy-done.12
  67.3 1.0 %convolution_convert_fusion = bf16[256,256]{1,0:T(8,128)(2,1)} fusion(bf16[1024,256]{1,0:T(8,128)(2,1)S(1)} %bitcast.8, bf16[1024,256]{1,0:T(8,128)(2,1)S(1)} %copy-done.12), kind=kOutput, calls=%fused_computation | convolution fusion | flops 134283264 | bytes 1179648 | tf_op jit(solution)/shard_map/ct,cd->td/dot_general | solution.py:398
  (6 shorter events, 0.1 us)
Async XLA Ops:
  3.8 17.3 %copy-start = (f32[64,2,2,128]{3,2,1,0:T(2,128)S(1)}, f32[64,2,2,128]{3,2,1,0:T(2,128)}, u32[]{:S(2)}) copy-start(f32[64,2,2,128]{3,2,1,0:T(2,128)} %param.24) | copy-start | bytes 393220
  3.8 17.3 %copy-start.1 = (f32[64,64]{1,0:T(8,128)S(1)}, f32[64,64]{1,0:T(8,128)}, u32[]{:S(2)}) copy-start(f32[64,64]{1,0:T(8,128)} %mid_ref.1) | copy-start | bytes 49156
  3.9 17.3 %copy-start.2 = (f32[33,64]{1,0:T(8,128)S(1)}, f32[33,64]{1,0:T(8,128)}, u32[]{:S(2)}) copy-start(f32[33,64]{1,0:T(8,128)} %in_ref.1) | copy-start | bytes 25348
  3.9 17.3 %copy-start.11 = (f32[64,128]{1,0:T(8,128)S(1)}, f32[64,128]{1,0:T(8,128)}, u32[]{:S(2)}) copy-start(f32[64,128]{1,0:T(8,128)} %constant.12.clone.waves_ref) | copy-start | bytes 98308
  3.9 29.3 %all-to-all-start = ((bf16[64,4,384]{2,1,0:T(4,128)(2,1)}), bf16[64,4,384]{2,1,0:T(4,128)(2,1)S(1)}, u32[]{:S(2)}, u32[]{:S(2)}) async-start(bf16[64,4,384]{2,1,0:T(4,128)(2,1)} %project.1), calls=%async_computation | async-start | bytes 393216 | tf_op jit(solution)/shard_map/all_to_all | solution.py:331
  21.2 0.7 copy-start.5
  21.8 2.7 %copy-start.3 = (f32[3,3,128]{2,1,0:T(4,128)S(1)}, f32[3,3,128]{2,1,0:T(4,128)}, u32[]{:S(2)}) copy-start(f32[3,3,128]{2,1,0:T(4,128)} %taps_ref.1) | copy-start | bytes 13828
  21.8 2.7 %copy-start.6 = (bf16[512,256]{1,0:T(8,128)(2,1)S(1)}, bf16[512,256]{1,0:T(8,128)(2,1)}, u32[]{:S(2)}) copy-start(bf16[512,256]{1,0:T(8,128)(2,1)} %constant.15.clone.right_ref) | copy-start | bytes 786436
  21.8 2.7 %copy-start.9 = (f32[256,128]{1,0:T(8,128)S(1)}, f32[256,128]{1,0:T(8,128)}, u32[]{:S(2)}) copy-start(f32[256,128]{1,0:T(8,128)} %constant.13.clone.turns_ref) | copy-start | bytes 393220
  21.8 2.7 %copy-start.10 = (bf16[256,256]{1,0:T(8,128)(2,1)S(1)}, bf16[256,256]{1,0:T(8,128)(2,1)}, u32[]{:S(2)}) copy-start(bf16[256,256]{1,0:T(8,128)(2,1)} %constant.14.clone.real_ref) | copy-start | bytes 393220
  24.5 0.7 %copy-start.4 = (f32[2,128]{1,0:T(2,128)S(1)}, f32[2,128]{1,0:T(2,128)}, u32[]{:S(2)}) copy-start(f32[2,128]{1,0:T(2,128)} %gain_ref.1) | copy-start | bytes 3076
  25.2 8.0 %copy-start.7 = (bf16[512,256]{1,0:T(8,128)(2,1)S(1)}, bf16[512,256]{1,0:T(8,128)(2,1)}, u32[]{:S(2)}) copy-start(bf16[512,256]{1,0:T(8,128)(2,1)} %constant.16.clone.back_ref) | copy-start | bytes 786436
  25.2 8.0 %copy-start.8 = (bf16[512,256]{1,0:T(8,128)(2,1)S(1)}, bf16[512,256]{1,0:T(8,128)(2,1)}, u32[]{:S(2)}) copy-start(bf16[512,256]{1,0:T(8,128)(2,1)} %constant.17.clone.ends_ref) | copy-start | bytes 786436
  61.3 6.0 %copy-start.12 = (bf16[1024,256]{1,0:T(8,128)(2,1)S(1)}, bf16[1024,256]{1,0:T(8,128)(2,1)}, u32[]{:S(2)}) copy-start(bf16[1024,256]{1,0:T(8,128)(2,1)} %param.27) | copy-start | bytes 1572868

commit v5 on v4

--- a/solution.py
+++ b/solution.py
@@ -80,7 +80,7 @@
 
 
 def project_kernel(
-    steps, tok_hbm, a_hbm, b_hbm, c_hbm, o_ref, tok, weights, sum_ref, flat_ref, wide_ref, sems
+    steps, tok_hbm, a_hbm, b_hbm, c_hbm, o_ref, tok, weights, sum_ref, sems
 ):
     depth = tok.shape[1] // steps
 
@@ -97,23 +97,19 @@
     for step in range(steps):
         for copy in group_of(step, pl.ds(step * depth, depth)):
             copy.start()
-    sum_ref[...] = jnp.zeros_like(sum_ref)
-
-    @pl.loop(0, steps)
-    def _(step):
-        cut = pl.ds(pl.multiple_of(step * depth, depth), depth)
-        for copy in group_of(step, cut):
+    for step in range(steps):
+        for copy in group_of(step, pl.ds(step * depth, depth)):
             copy.wait()
-        sum_ref[...] += mm(tok[:, cut], weights[cut, :])
-
-    @pl.loop(0, 3)
-    def _(p):
-        cut = pl.ds(pl.multiple_of(p * SIDE, SIDE), SIDE)
+        cut = slice(step * depth, (step + 1) * depth)
+        part = mm(tok[:, cut], weights[cut, :])
+        if step < steps - 1:
+            sum_ref[...] = part if step == 0 else sum_ref[...] + part
+    part += sum_ref[...]
+    for p in range(3):
+        cut = slice(p * SIDE, (p + 1) * SIDE)
         for s in range(2):
-            flat_ref[s] = sum_ref[s * SIDE : (s + 1) * SIDE, cut].T
-            for c in range(2):
-                wide_ref[:, s * 2 + c, :] = flat_ref[s, pl.ds(c, HALF, stride=2), :]
-        o_ref[:, :, cut] = wide_ref[...].astype(BF)
+            turned = part[s * SIDE : (s + 1) * SIDE, cut].T
+            o_ref[:, 2 * s : 2 * s + 2, cut] = turned.astype(BF).reshape(HALF, 2, SIDE)
 
 
 def network_kernel(
@@ -134,7 +130,8 @@
         top, low = hi_lo(out_ref[pl.ds(pair, units, stride=4), :])
         out_hi += mm(pick, top, last)
         out_lo += mm(pick, low, last)
-    out_all = jnp.concatenate([out_hi.astype(BF), out_lo.astype(BF)], axis=1)
+    out_hi, out_lo = out_hi.astype(BF), out_lo.astype(BF)
+    out_all = jnp.concatenate([out_hi, out_lo, out_hi], axis=1)
     rate = jnp.sum(jnp.where(mine, rate_ref[...], 0.0), axis=1, keepdims=True)
     scale = 1.0 / (2.0 * math.pi)
     side_ref[...] = jnp.zeros_like(side_ref)
@@ -178,8 +175,8 @@
         moved = mm(in_all, jnp.concatenate([top, top, low, side], axis=0), first)
         top, low = hi_lo(sine_of_turns(moved))
         moved = mm(mid_all, jnp.concatenate([top, top, low, ones], axis=0), first)
-        top = sine_of_turns(moved).astype(BF)
-        shaped = mm(out_all, jnp.concatenate([top, top], axis=0))
+        top, low = hi_lo(sine_of_turns(moved))
+        shaped = mm(out_all, jnp.concatenate([top, top, low], axis=0))
         for piece in range(blocks):
             block = start + piece
             lag = lane + block * SIDE
@@ -231,19 +228,21 @@
 
 def conv_kernel(
     x_ref, coef_ref, spec_re_ref, spec_im_ref, turns_ref, right_ref, back_ref, ends_ref,
-    o_ref, wide_ref, rows_ref,
+    o_ref, rows_ref,
 ):
-    wide_ref[...] = x_ref[...].astype(F32)
+    for p in range(3):
+        for s in range(2):
+            piece = x_ref[:, 2 * s : 2 * s + 2, p * SIDE : (p + 1) * SIDE]
+            rows_ref[2 * p + s] = piece.reshape(SIDE, SIDE).astype(F32)
     row = lax.broadcasted_iota(jnp.int32, (HALF, SIDE), 0)
     lane = lax.broadcasted_iota(jnp.int32, (HALF, SIDE), 1)
 
     def smoothed(p):
         seqs = []
-        cut = pl.ds(pl.multiple_of(p * SIDE, SIDE), SIDE)
         for s in range(2):
             chans = []
             for c in range(2):
-                here = wide_ref[:, s * 2 + c, cut]
+                here = rows_ref[2 * p + s, pl.ds(c, HALF, stride=2), :]
                 moved = pltpu.roll(here, 1, 1)
                 prev = jnp.where(lane == 0, pltpu.roll(moved, 1, 0), moved)
                 prev = jnp.where((lane == 0) & (row == 0), 0.0, prev)
@@ -285,10 +284,10 @@
     state = lax.fori_loop(0, 2, one_order, smoothed(0))
     for s in range(2):
         for c in range(2):
-            rows_ref[:, c, pl.ds(s * SIDE, SIDE)] = state[
+            rows_ref[s, pl.ds(c, HALF, stride=2), :] = state[
                 s * HALF : (s + 1) * HALF, c * SIDE : (c + 1) * SIDE
             ]
-    o_ref[...] = rows_ref[...].astype(BF)
+        o_ref[:, :, s * SIDE : (s + 1) * SIDE] = rows_ref[s].astype(BF).reshape(HALF, 2, SIDE)
 
 
 def on_device(
@@ -311,7 +310,7 @@
     waves, turns, real_all, rights, backs, ends = (jnp.asarray(t) for t in tables(length, feats))
     far = pl.BlockSpec(memory_space=pltpu.HBM)
     vmem = pl.BlockSpec(memory_space=pltpu.VMEM)
-    steps = 4
+    steps = 2
     pieces = pl.pallas_call(
         functools.partial(project_kernel, steps),
         out_shape=jax.ShapeDtypeStruct((blocks, 4, 3 * tok_rows), BF),
@@ -321,8 +320,6 @@
             pltpu.VMEM((seqs * tok_rows, tokens.shape[2]), BF),
             pltpu.VMEM((tokens.shape[2], 3 * SIDE), BF),
             pltpu.VMEM((seqs * tok_rows, 3 * SIDE), F32),
-            pltpu.VMEM((2, SIDE, SIDE), F32),
-            pltpu.VMEM((HALF, 4, SIDE), F32),
             pltpu.SemaphoreType.DMA((steps, 5)),
         ],
         compiler_params=pltpu.CompilerParams(vmem_limit_bytes=66_700_000),
@@ -370,8 +367,7 @@
         in_specs=[vmem] * 8,
         out_specs=vmem,
         scratch_shapes=[
-            pltpu.VMEM((HALF, 4, 3 * SIDE), F32),
-            pltpu.VMEM((HALF, 2, 2 * SIDE), F32),
+            pltpu.VMEM((6, SIDE, SIDE), F32),
         ],
         compiler_params=pltpu.CompilerParams(vmem_limit_bytes=16 * 2**20),
         cost_estimate=pl.CostEstimate(

time: 68.6 us -> 68 us (level)
    pallas_call x1, Pallas kernels: 3.82 us -> 3.07 us  [on_device(): pl.pallas_call(functools.partial(project_kernel, steps), out_shape=jax.Sh...]
where the time goes in v5:
time: 68 us; the launch traced here: 67.7 us
  blocking collectives  31.6 us (46%)
  starting transfers between devices  17.3 us (25%)
  Pallas kernels  9.29 us (14%)
  waiting for transfers between devices  6.95 us (10%)
  local copies, waits for them, and re-layouts  1.38 us (2%)
  matrix products  1 us (1%)
    all_to_all x1, starting transfers between devices, on_device(): arrived = lax.all_to_all(pieces, ROW, 0, 0, tiled=True)  17.3 us
    all_to_all x1, blocking collectives, on_device(): returned = lax.all_to_all(gated, ROW, 0, 0, tiled=True)  16.2 us
    all_to_all x1, blocking collectives, on_device(): lax.all_to_all(jnp.broadcast_to(returned[None], (lax.axis_size('x'), *ret...  9.34 us
    all_to_all x1, waiting for transfers between devices, on_device(): arrived = lax.all_to_all(pieces, ROW, 0, 0, tiled=True)  6.95 us
    all_gather x1, blocking collectives, on_device(): everyone = lax.all_gather(everyone, 'core', axis=1)  6.04 us
    pallas_call x1, Pallas kernels, on_device(): pl.pallas_call(functools.partial(project_kernel, steps), out_shape=jax.Sh...  3.07 us
    pallas_call x1, Pallas kernels, on_device(): pl.pallas_call(network_kernel, out_shape=(jax.ShapeDtypeStruct((8 * HALF,...  2.86 us
    pallas_call x1, Pallas kernels, on_device(): pl.pallas_call(conv_kernel, out_shape=jax.ShapeDtypeStruct((blocks, 2, se...  2.52 us
  transfers between devices with their start and end apart: 1, of which 1 were waited for; matrix products, arithmetic and copies ran while one was open for 0% of the time, Pallas kernels for 5%

profile of v5, /device:TPU:1, one launch (start us, length us, event | category | flops | bytes accessed | tf_op | source)
XLA Modules:
  0.0 67.7 jit_solution(15030583256075065144)
XLA Ops:
  0.0 3.1 %project.1 = bf16[64,4,384]{2,1,0:T(4,128)(2,1)} custom-call(bf16[2,128,2048]{2,1,0:T(8,128)(2,1)} %tok_hbm.1, bf16[2048,128]{1,0:T(8,128)(2,1)} %a_hbm.1, bf16[2048,128]{1,0:T(8,128)(2,1)} %b_hbm.1, bf16[2048,128]{1,0:T(8,128)(2,1)} %c_hbm.1), custom_call_target="tpu_custom_call" | custom-call | tf_op jit(solution)/shard_map/project/pallas_call | solution.py:314
  3.1 0.0 copy-start
  3.1 0.0 copy-start.1
  3.1 0.0 copy-start.2
  3.1 0.0 copy-start.11
  3.1 17.3 %all-to-all-start = ((bf16[64,4,384]{2,1,0:T(4,128)(2,1)}), bf16[64,4,384]{2,1,0:T(4,128)(2,1)S(1)}, u32[]{:S(2)}, u32[]{:S(2)}) async-start(bf16[64,4,384]{2,1,0:T(4,128)(2,1)} %project.1), calls=%async_computation | async-start | bytes 393216 | tf_op jit(solution)/shard_map/all_to_all | solution.py:328
  20.4 0.0 copy-start.5
  20.4 0.0 copy-done
  20.4 0.0 copy-done.1
  20.4 0.0 copy-done.2
  20.5 0.0 copy-done.11
  20.5 0.6 copy-done.5
  21.1 0.0 copy-start.3
  21.1 0.0 copy-start.6
  21.1 0.0 copy-start.9
  21.1 0.0 copy-start.10
  21.1 2.9 %network.1 = (f32[512,128]{1,0:T(8,128)S(1)}, f32[8,128]{1,0:T(8,128)S(1)}) custom-call(f32[64,128]{1,0:T(8,128)S(1)} %copy-done.11, f32[33,64]{1,0:T(8,128)S(1)} %copy-done.2, f32[64,64]{1,0:T(8,128)S(1)} %copy-done.1, f32[256,128]{1,0:T(8,128)S(1)} %bitcast.6, f32[1,128]{1,0:T(1,128)S(1)} %bitcast.7), custom_call_target="tpu_custom_call" | custom-call | flops 4000000000 | bytes 1000000 | tf_op jit(solution)/shard_map/network/pallas_call | solution.py:332
  23.9 0.0 copy-done.3
  23.9 0.0 copy-done.6
  24.0 0.0 copy-done.9
  24.0 0.0 copy-done.10
  24.0 0.7 copy-done.4
  24.6 0.8 %spectra.1 = (f32[2,256,128]{2,1,0:T(8,128)S(1)}, f32[2,256,128]{2,1,0:T(8,128)S(1)}, f32[3,8,256]{2,1,0:T(8,128)S(1)}) custom-call(f32[512,128]{1,0:T(8,128)S(1)} %get-tuple-element.10.rows_ref, f32[8,128]{1,0:T(8,128)S(1)} %get-tuple-element.11.factor_ref, f32[256,128]{1,0:T(8,128)S(1)} %copy-done.9, bf16[256,256]{1,0:T(8,128)(2,1)S(1)} %copy-done.10, ...), custom_call_target="tpu_custom_call" | custom-call | flops 1000000000 | bytes 2000000 | tf_op jit(solution)/shard_map/spectra/pallas_call | solution.py:353
  25.5 6.9 %all-to-all-done.x_ref = bf16[64,4,384]{2,1,0:T(4,128)(2,1)S(1)} async-done(((bf16[64,4,384]{2,1,0:T(4,128)(2,1)}), bf16[64,4,384]{2,1,0:T(4,128)(2,1)S(1)}, u32[]{:S(2)}, u32[]{:S(2)}) %all-to-all-start) | async-done | bytes 196640 | tf_op jit(solution)/shard_map/all_to_all | solution.py:328
  32.4 0.0 copy-done.7
  32.4 0.0 copy-done.8
  32.4 2.5 %gated_conv.1 = bf16[64,2,256]{2,1,0:T(2,128)(2,1)S(1)} custom-call(bf16[64,4,384]{2,1,0:T(4,128)(2,1)S(1)} %all-to-all-done.x_ref, f32[3,8,256]{2,1,0:T(8,128)S(1)} %get-tuple-element.12.coef_ref, f32[2,256,128]{2,1,0:T(8,128)S(1)} %get-tuple-element.13.spec_re_ref, f32[2,256,128]{2,1,0:T(8,128)S(1)} %get-tuple-element.14.spec_im_ref, ...), custom_call_target="tpu_custom_call" | custom-call | flops 4000000000 | bytes 2000000 | tf_op jit(solution)/shard_map/gated_conv/pallas_call | solution.py:364
  35.0 16.2 %all_to_all.15 = bf16[64,2,256]{2,1,0:T(2,128)(2,1)S(1)} all-to-all(bf16[64,2,256]{2,1,0:T(2,128)(2,1)S(1)} %gated_conv.1), channel_id=1, replica_groups=mesh['row_0'=8,'row_1'=8,'x'=4,'core'=2] {'row_0','row_1'}, dimensions={0} | all-to-all | bytes 131072 | tf_op jit(solution)/shard_map/all_to_all | solution.py:387
  51.3 9.3 %all_to_all.16 = bf16[4,128,256]{2,1,0:T(8,128)(2,1)S(1)} all-to-all(bf16[4,128,256]{2,1,0:T(8,128)(2,1)S(1)} %broadcast_in_dim.8), channel_id=1, replica_groups=mesh['row_0'=8,'row_1'=8,'x'=4,'core'=2] {'x'}, dimensions={0} | all-to-all | bytes 524288 | tf_op jit(solution)/shard_map/all_to_all | solution.py:389
  60.6 6.0 %all-gather = bf16[4,256,256]{2,1,0:T(8,128)(2,1)S(1)} all-gather(bf16[4,128,256]{2,1,0:T(8,128)(2,1)S(1)} %all_to_all.16), channel_id=2, replica_groups=mesh['row_0'=8,'row_1'=8,'x'=4,'core'=2] {'core'}, dimensions={1}, use_global_device_ids=true | all-gather | bytes 786432 | tf_op jit(solution)/shard_map/all_gather | solution.py:392
  66.7 0.0 copy-done.12
  66.7 1.0 %convolution_convert_fusion = bf16[256,256]{1,0:T(8,128)(2,1)} fusion(bf16[1024,256]{1,0:T(8,128)(2,1)S(1)} %bitcast.8, bf16[1024,256]{1,0:T(8,128)(2,1)S(1)} %copy-done.12), kind=kOutput, calls=%fused_computation | convolution fusion | flops 134283264 | bytes 1179648 | tf_op jit(solution)/shard_map/ct,cd->td/dot_general | solution.py:394
  (6 shorter events, 0.1 us)
Async XLA Ops:
  3.1 17.3 %copy-start = (f32[64,2,2,128]{3,2,1,0:T(2,128)S(1)}, f32[64,2,2,128]{3,2,1,0:T(2,128)}, u32[]{:S(2)}) copy-start(f32[64,2,2,128]{3,2,1,0:T(2,128)} %param.24) | copy-start | bytes 393220
  3.1 17.3 %copy-start.1 = (f32[64,64]{1,0:T(8,128)S(1)}, f32[64,64]{1,0:T(8,128)}, u32[]{:S(2)}) copy-start(f32[64,64]{1,0:T(8,128)} %mid_ref.1) | copy-start | bytes 49156
  3.1 17.3 %copy-start.2 = (f32[33,64]{1,0:T(8,128)S(1)}, f32[33,64]{1,0:T(8,128)}, u32[]{:S(2)}) copy-start(f32[33,64]{1,0:T(8,128)} %in_ref.1) | copy-start | bytes 25348
  3.1 17.3 %copy-start.11 = (f32[64,128]{1,0:T(8,128)S(1)}, f32[64,128]{1,0:T(8,128)}, u32[]{:S(2)}) copy-start(f32[64,128]{1,0:T(8,128)} %constant.12.clone.waves_ref) | copy-start | bytes 98308
  3.1 29.3 %all-to-all-start = ((bf16[64,4,384]{2,1,0:T(4,128)(2,1)}), bf16[64,4,384]{2,1,0:T(4,128)(2,1)S(1)}, u32[]{:S(2)}, u32[]{:S(2)}) async-start(bf16[64,4,384]{2,1,0:T(4,128)(2,1)} %project.1), calls=%async_computation | async-start | bytes 393216 | tf_op jit(solution)/shard_map/all_to_all | solution.py:328
  20.4 0.7 copy-start.5
  21.1 2.9 %copy-start.3 = (f32[3,3,128]{2,1,0:T(4,128)S(1)}, f32[3,3,128]{2,1,0:T(4,128)}, u32[]{:S(2)}) copy-start(f32[3,3,128]{2,1,0:T(4,128)} %taps_ref.1) | copy-start | bytes 13828
  21.1 2.9 %copy-start.6 = (bf16[512,256]{1,0:T(8,128)(2,1)S(1)}, bf16[512,256]{1,0:T(8,128)(2,1)}, u32[]{:S(2)}) copy-start(bf16[512,256]{1,0:T(8,128)(2,1)} %constant.15.clone.right_ref) | copy-start | bytes 786436
  21.1 2.9 %copy-start.9 = (f32[256,128]{1,0:T(8,128)S(1)}, f32[256,128]{1,0:T(8,128)}, u32[]{:S(2)}) copy-start(f32[256,128]{1,0:T(8,128)} %constant.13.clone.turns_ref) | copy-start | bytes 393220
  21.1 2.9 %copy-start.10 = (bf16[256,256]{1,0:T(8,128)(2,1)S(1)}, bf16[256,256]{1,0:T(8,128)(2,1)}, u32[]{:S(2)}) copy-start(bf16[256,256]{1,0:T(8,128)(2,1)} %constant.14.clone.real_ref) | copy-start | bytes 393220
  23.9 0.7 %copy-start.4 = (f32[2,128]{1,0:T(2,128)S(1)}, f32[2,128]{1,0:T(2,128)}, u32[]{:S(2)}) copy-start(f32[2,128]{1,0:T(2,128)} %gain_ref.1) | copy-start | bytes 3076
  24.6 7.8 %copy-start.7 = (bf16[512,256]{1,0:T(8,128)(2,1)S(1)}, bf16[512,256]{1,0:T(8,128)(2,1)}, u32[]{:S(2)}) copy-start(bf16[512,256]{1,0:T(8,128)(2,1)} %constant.16.clone.back_ref) | copy-start | bytes 786436
  24.6 7.8 %copy-start.8 = (bf16[512,256]{1,0:T(8,128)(2,1)S(1)}, bf16[512,256]{1,0:T(8,128)(2,1)}, u32[]{:S(2)}) copy-start(bf16[512,256]{1,0:T(8,128)(2,1)} %constant.17.clone.ends_ref) | copy-start | bytes 786436
  60.6 6.0 %copy-start.12 = (bf16[1024,256]{1,0:T(8,128)(2,1)S(1)}, bf16[1024,256]{1,0:T(8,128)(2,1)}, u32[]{:S(2)}) copy-start(bf16[1024,256]{1,0:T(8,128)(2,1)} %param.27) | copy-start | bytes 1572868

commit v6 on v5

--- a/solution.py
+++ b/solution.py
@@ -260,28 +260,29 @@
     cos2, sin2 = jnp.concatenate([cos, cos], axis=1), jnp.concatenate([sin, sin], axis=1)
 
     def one_order(order, state):
-        grid = left_const(ends_ref[: 2 * SIDE, :SIDE], ends_ref[: 2 * SIDE, SIDE:], state)
-        real, imag = grid[:SIDE], grid[SIDE:]
-        real, imag = real * cos2 + imag * sin2, imag * cos2 - real * sin2
+        top, low = hi_lo(state)
+        grid = mm(ends_ref[: 2 * SIDE, :], jnp.concatenate([top, top], axis=0))
+        grid += mm(ends_ref[: 2 * SIDE, :SIDE], low)
+        reals, imags = [], []
+        for c in range(2):
+            cut = slice(c * SIDE, (c + 1) * SIDE)
+            real, imag = grid[:SIDE, cut], grid[SIDE:, cut]
+            pair = jnp.concatenate([real * cos + imag * sin, imag * cos - real * sin], axis=1)
+            pair = right_const(pair, right_ref[: 2 * SIDE, :], right_ref[2 * SIDE :, :])
+            real, imag = pair[:, :SIDE], pair[:, SIDE:]
+            k_re, k_im = spec_re_ref[order, cut, :], spec_im_ref[order, cut, :]
+            pair = jnp.concatenate([real * k_re - imag * k_im, real * k_im + imag * k_re], axis=1)
+            pair = right_const(pair, back_ref[: 2 * SIDE, :], back_ref[2 * SIDE :, :])
+            real, imag = pair[:, :SIDE], pair[:, SIDE:]
+            reals.append(real * cos - imag * sin)
+            imags.append(real * sin + imag * cos)
         grid = jnp.concatenate(
-            [
-                jnp.concatenate([real[:, :SIDE], imag[:, :SIDE]], axis=1),
-                jnp.concatenate([real[:, SIDE:], imag[:, SIDE:]], axis=1),
-            ],
-            axis=0,
+            [jnp.concatenate(reals, axis=1), jnp.concatenate(imags, axis=1)], axis=0
         )
-        grid = right_const(grid, right_ref[: 2 * SIDE, :], right_ref[2 * SIDE :, :])
-        real, imag = grid[:, :SIDE], grid[:, SIDE:]
-        k_re, k_im = spec_re_ref[order], spec_im_ref[order]
-        grid = jnp.concatenate([real * k_re - imag * k_im, real * k_im + imag * k_re], axis=1)
-        grid = right_const(grid, back_ref[: 2 * SIDE, :], back_ref[2 * SIDE :, :])
-        real = jnp.concatenate([grid[:SIDE, :SIDE], grid[SIDE:, :SIDE]], axis=1)
-        imag = jnp.concatenate([grid[:SIDE, SIDE:], grid[SIDE:, SIDE:]], axis=1)
-        grid = jnp.concatenate([real * cos2 - imag * sin2, real * sin2 + imag * cos2], axis=0)
         reach = left_const(ends_ref[2 * SIDE : 3 * SIDE, :], ends_ref[3 * SIDE :, :], grid)
         return smoothed(order + 1) * (reach + coef_ref[order + 1, 3:4, :] * state)
 
-    state = lax.fori_loop(0, 2, one_order, smoothed(0))
+    state = one_order(1, one_order(0, smoothed(0)))
     for s in range(2):
         for c in range(2):
             rows_ref[s, pl.ds(c, HALF, stride=2), :] = state[

time: 68 us -> 67.7 us (level)
  no operation moved by 1% of the time
where the time goes in v6:
time: 67.7 us; the launch traced here: 67.4 us
  blocking collectives  31.6 us (47%)
  starting transfers between devices  17.3 us (26%)
  Pallas kernels  9.03 us (13%)
  waiting for transfers between devices  6.95 us (10%)
  local copies, waits for them, and re-layouts  1.38 us (2%)
  matrix products  1 us (1%)
    all_to_all x1, starting transfers between devices, on_device(): arrived = lax.all_to_all(pieces, ROW, 0, 0, tiled=True)  17.3 us
    all_to_all x1, blocking collectives, on_device(): returned = lax.all_to_all(gated, ROW, 0, 0, tiled=True)  16.3 us
    all_to_all x1, blocking collectives, on_device(): lax.all_to_all(jnp.broadcast_to(returned[None], (lax.axis_size('x'), *ret...  9.34 us
    all_to_all x1, waiting for transfers between devices, on_device(): arrived = lax.all_to_all(pieces, ROW, 0, 0, tiled=True)  6.95 us
    all_gather x1, blocking collectives, on_device(): everyone = lax.all_gather(everyone, 'core', axis=1)  6.03 us
    pallas_call x1, Pallas kernels, on_device(): pl.pallas_call(functools.partial(project_kernel, steps), out_shape=jax.Sh...  3.07 us
    pallas_call x1, Pallas kernels, on_device(): pl.pallas_call(network_kernel, out_shape=(jax.ShapeDtypeStruct((8 * HALF,...  2.86 us
    pallas_call x1, Pallas kernels, on_device(): pl.pallas_call(conv_kernel, out_shape=jax.ShapeDtypeStruct((blocks, 2, se...  2.26 us
  transfers between devices with their start and end apart: 1, of which 1 were waited for; matrix products, arithmetic and copies ran while one was open for 0% of the time, Pallas kernels for 5%

profile of v6, /device:TPU:1, one launch (start us, length us, event | category | flops | bytes accessed | tf_op | source)
XLA Modules:
  0.0 67.4 jit_solution(14678064687339592559)
XLA Ops:
  0.0 3.1 %project.1 = bf16[64,4,384]{2,1,0:T(4,128)(2,1)} custom-call(bf16[2,128,2048]{2,1,0:T(8,128)(2,1)} %tok_hbm.1, bf16[2048,128]{1,0:T(8,128)(2,1)} %a_hbm.1, bf16[2048,128]{1,0:T(8,128)(2,1)} %b_hbm.1, bf16[2048,128]{1,0:T(8,128)(2,1)} %c_hbm.1), custom_call_target="tpu_custom_call" | custom-call | tf_op jit(solution)/shard_map/project/pallas_call | solution.py:315
  3.1 0.0 copy-start
  3.1 0.0 copy-start.1
  3.1 0.0 copy-start.2
  3.1 0.0 copy-start.11
  3.1 17.3 %all-to-all-start = ((bf16[64,4,384]{2,1,0:T(4,128)(2,1)}), bf16[64,4,384]{2,1,0:T(4,128)(2,1)S(1)}, u32[]{:S(2)}, u32[]{:S(2)}) async-start(bf16[64,4,384]{2,1,0:T(4,128)(2,1)} %project.1), calls=%async_computation | async-start | bytes 393216 | tf_op jit(solution)/shard_map/all_to_all | solution.py:329
  20.4 0.0 copy-start.5
  20.4 0.0 copy-done
  20.4 0.0 copy-done.1
  20.4 0.0 copy-done.2
  20.5 0.0 copy-done.11
  20.5 0.6 copy-done.5
  21.1 0.0 copy-start.3
  21.1 0.0 copy-start.6
  21.1 0.0 copy-start.9
  21.1 0.0 copy-start.10
  21.1 2.9 %network.1 = (f32[512,128]{1,0:T(8,128)S(1)}, f32[8,128]{1,0:T(8,128)S(1)}) custom-call(f32[64,128]{1,0:T(8,128)S(1)} %copy-done.11, f32[33,64]{1,0:T(8,128)S(1)} %copy-done.2, f32[64,64]{1,0:T(8,128)S(1)} %copy-done.1, f32[256,128]{1,0:T(8,128)S(1)} %bitcast.6, f32[1,128]{1,0:T(1,128)S(1)} %bitcast.7), custom_call_target="tpu_custom_call" | custom-call | flops 4000000000 | bytes 1000000 | tf_op jit(solution)/shard_map/network/pallas_call | solution.py:333
  23.9 0.0 copy-done.3
  23.9 0.0 copy-done.6
  24.0 0.0 copy-done.9
  24.0 0.0 copy-done.10
  24.0 0.7 copy-done.4
  24.6 0.8 %spectra.1 = (f32[2,256,128]{2,1,0:T(8,128)S(1)}, f32[2,256,128]{2,1,0:T(8,128)S(1)}, f32[3,8,256]{2,1,0:T(8,128)S(1)}) custom-call(f32[512,128]{1,0:T(8,128)S(1)} %get-tuple-element.10.rows_ref, f32[8,128]{1,0:T(8,128)S(1)} %get-tuple-element.11.factor_ref, f32[256,128]{1,0:T(8,128)S(1)} %copy-done.9, bf16[256,256]{1,0:T(8,128)(2,1)S(1)} %copy-done.10, ...), custom_call_target="tpu_custom_call" | custom-call | flops 1000000000 | bytes 2000000 | tf_op jit(solution)/shard_map/spectra/pallas_call | solution.py:354
  25.5 6.9 %all-to-all-done.x_ref = bf16[64,4,384]{2,1,0:T(4,128)(2,1)S(1)} async-done(((bf16[64,4,384]{2,1,0:T(4,128)(2,1)}), bf16[64,4,384]{2,1,0:T(4,128)(2,1)S(1)}, u32[]{:S(2)}, u32[]{:S(2)}) %all-to-all-start) | async-done | bytes 196640 | tf_op jit(solution)/shard_map/all_to_all | solution.py:329
  32.4 0.0 copy-done.7
  32.4 0.0 copy-done.8
  32.4 2.3 %gated_conv.1 = bf16[64,2,256]{2,1,0:T(2,128)(2,1)S(1)} custom-call(bf16[64,4,384]{2,1,0:T(4,128)(2,1)S(1)} %all-to-all-done.x_ref, f32[3,8,256]{2,1,0:T(8,128)S(1)} %get-tuple-element.12.coef_ref, f32[2,256,128]{2,1,0:T(8,128)S(1)} %get-tuple-element.13.spec_re_ref, f32[2,256,128]{2,1,0:T(8,128)S(1)} %get-tuple-element.14.spec_im_ref, ...), custom_call_target="tpu_custom_call" | custom-call | flops 4000000000 | bytes 2000000 | tf_op jit(solution)/shard_map/gated_conv/pallas_call | solution.py:365
  34.7 16.3 %all_to_all.15 = bf16[64,2,256]{2,1,0:T(2,128)(2,1)S(1)} all-to-all(bf16[64,2,256]{2,1,0:T(2,128)(2,1)S(1)} %gated_conv.1), channel_id=1, replica_groups=mesh['row_0'=8,'row_1'=8,'x'=4,'core'=2] {'row_0','row_1'}, dimensions={0} | all-to-all | bytes 131072 | tf_op jit(solution)/shard_map/all_to_all | solution.py:388
  51.0 9.3 %all_to_all.16 = bf16[4,128,256]{2,1,0:T(8,128)(2,1)S(1)} all-to-all(bf16[4,128,256]{2,1,0:T(8,128)(2,1)S(1)} %broadcast_in_dim.8), channel_id=1, replica_groups=mesh['row_0'=8,'row_1'=8,'x'=4,'core'=2] {'x'}, dimensions={0} | all-to-all | bytes 524288 | tf_op jit(solution)/shard_map/all_to_all | solution.py:390
  60.4 6.0 %all-gather = bf16[4,256,256]{2,1,0:T(8,128)(2,1)S(1)} all-gather(bf16[4,128,256]{2,1,0:T(8,128)(2,1)S(1)} %all_to_all.16), channel_id=2, replica_groups=mesh['row_0'=8,'row_1'=8,'x'=4,'core'=2] {'core'}, dimensions={1}, use_global_device_ids=true | all-gather | bytes 786432 | tf_op jit(solution)/shard_map/all_gather | solution.py:393
  66.4 0.0 copy-done.12
  66.4 1.0 %convolution_convert_fusion = bf16[256,256]{1,0:T(8,128)(2,1)} fusion(bf16[1024,256]{1,0:T(8,128)(2,1)S(1)} %bitcast.8, bf16[1024,256]{1,0:T(8,128)(2,1)S(1)} %copy-done.12), kind=kOutput, calls=%fused_computation | convolution fusion | flops 134283264 | bytes 1179648 | tf_op jit(solution)/shard_map/ct,cd->td/dot_general | solution.py:395
  (6 shorter events, 0.1 us)
Async XLA Ops:
  3.1 17.3 %copy-start = (f32[64,2,2,128]{3,2,1,0:T(2,128)S(1)}, f32[64,2,2,128]{3,2,1,0:T(2,128)}, u32[]{:S(2)}) copy-start(f32[64,2,2,128]{3,2,1,0:T(2,128)} %param.24) | copy-start | bytes 393220
  3.1 17.3 %copy-start.1 = (f32[64,64]{1,0:T(8,128)S(1)}, f32[64,64]{1,0:T(8,128)}, u32[]{:S(2)}) copy-start(f32[64,64]{1,0:T(8,128)} %mid_ref.1) | copy-start | bytes 49156
  3.1 17.3 %copy-start.2 = (f32[33,64]{1,0:T(8,128)S(1)}, f32[33,64]{1,0:T(8,128)}, u32[]{:S(2)}) copy-start(f32[33,64]{1,0:T(8,128)} %in_ref.1) | copy-start | bytes 25348
  3.1 17.3 %copy-start.11 = (f32[64,128]{1,0:T(8,128)S(1)}, f32[64,128]{1,0:T(8,128)}, u32[]{:S(2)}) copy-start(f32[64,128]{1,0:T(8,128)} %constant.12.clone.waves_ref) | copy-start | bytes 98308
  3.1 29.3 %all-to-all-start = ((bf16[64,4,384]{2,1,0:T(4,128)(2,1)}), bf16[64,4,384]{2,1,0:T(4,128)(2,1)S(1)}, u32[]{:S(2)}, u32[]{:S(2)}) async-start(bf16[64,4,384]{2,1,0:T(4,128)(2,1)} %project.1), calls=%async_computation | async-start | bytes 393216 | tf_op jit(solution)/shard_map/all_to_all | solution.py:329
  20.4 0.7 copy-start.5
  21.1 2.9 %copy-start.3 = (f32[3,3,128]{2,1,0:T(4,128)S(1)}, f32[3,3,128]{2,1,0:T(4,128)}, u32[]{:S(2)}) copy-start(f32[3,3,128]{2,1,0:T(4,128)} %taps_ref.1) | copy-start | bytes 13828
  21.1 2.9 %copy-start.6 = (bf16[512,256]{1,0:T(8,128)(2,1)S(1)}, bf16[512,256]{1,0:T(8,128)(2,1)}, u32[]{:S(2)}) copy-start(bf16[512,256]{1,0:T(8,128)(2,1)} %constant.15.clone.right_ref) | copy-start | bytes 786436
  21.1 2.9 %copy-start.9 = (f32[256,128]{1,0:T(8,128)S(1)}, f32[256,128]{1,0:T(8,128)}, u32[]{:S(2)}) copy-start(f32[256,128]{1,0:T(8,128)} %constant.13.clone.turns_ref) | copy-start | bytes 393220
  21.1 2.9 %copy-start.10 = (bf16[256,256]{1,0:T(8,128)(2,1)S(1)}, bf16[256,256]{1,0:T(8,128)(2,1)}, u32[]{:S(2)}) copy-start(bf16[256,256]{1,0:T(8,128)(2,1)} %constant.14.clone.real_ref) | copy-start | bytes 393220
  23.9 0.7 %copy-start.4 = (f32[2,128]{1,0:T(2,128)S(1)}, f32[2,128]{1,0:T(2,128)}, u32[]{:S(2)}) copy-start(f32[2,128]{1,0:T(2,128)} %gain_ref.1) | copy-start | bytes 3076
  24.6 7.8 %copy-start.7 = (bf16[512,256]{1,0:T(8,128)(2,1)S(1)}, bf16[512,256]{1,0:T(8,128)(2,1)}, u32[]{:S(2)}) copy-start(bf16[512,256]{1,0:T(8,128)(2,1)} %constant.16.clone.back_ref) | copy-start | bytes 786436
  24.6 7.8 %copy-start.8 = (bf16[512,256]{1,0:T(8,128)(2,1)S(1)}, bf16[512,256]{1,0:T(8,128)(2,1)}, u32[]{:S(2)}) copy-start(bf16[512,256]{1,0:T(8,128)(2,1)} %constant.17.clone.ends_ref) | copy-start | bytes 786436
  60.4 6.0 %copy-start.12 = (bf16[1024,256]{1,0:T(8,128)(2,1)S(1)}, bf16[1024,256]{1,0:T(8,128)(2,1)}, u32[]{:S(2)}) copy-start(bf16[1024,256]{1,0:T(8,128)(2,1)} %param.27) | copy-start | bytes 1572868

commit v7 on v6

--- a/solution.py
+++ b/solution.py
@@ -15,6 +15,7 @@
 SIDE = 128
 HALF = SIDE // 2
 CHUNK = 4096
+ROOT = 44
 BF = jnp.bfloat16
 F32 = jnp.float32
 
@@ -117,6 +118,7 @@
 ):
     length = HALF * SIDE
     device = lax.axis_index("row_0") * lax.axis_size("row_1") + lax.axis_index("row_1")
+    device = (device + (HALF - ROOT)) % HALF
     lane = lax.broadcasted_iota(jnp.int32, (8, SIDE), 1)
     row = lax.broadcasted_iota(jnp.int32, (8, SIDE), 0)
     mine = lane == 2 * device + row % 2
@@ -195,6 +197,7 @@
     spec_re_ref, spec_im_ref, coef_ref,
 ):
     device = lax.axis_index("row_0") * lax.axis_size("row_1") + lax.axis_index("row_1")
+    device = (device + (HALF - ROOT)) % HALF
     sources = [(tap, taps_ref[tap], 0) for tap in range(3)] + [(3, gain_ref[...], 1)]
     for c in range(2):
         for at, source, shift in sources:
@@ -233,6 +236,7 @@
     for p in range(3):
         for s in range(2):
             piece = x_ref[:, 2 * s : 2 * s + 2, p * SIDE : (p + 1) * SIDE]
+            piece = jnp.concatenate([piece[HALF - ROOT :], piece[: HALF - ROOT]], axis=0)
             rows_ref[2 * p + s] = piece.reshape(SIDE, SIDE).astype(F32)
     row = lax.broadcasted_iota(jnp.int32, (HALF, SIDE), 0)
     lane = lax.broadcasted_iota(jnp.int32, (HALF, SIDE), 1)
@@ -288,7 +292,9 @@
             rows_ref[s, pl.ds(c, HALF, stride=2), :] = state[
                 s * HALF : (s + 1) * HALF, c * SIDE : (c + 1) * SIDE
             ]
-        o_ref[:, :, s * SIDE : (s + 1) * SIDE] = rows_ref[s].astype(BF).reshape(HALF, 2, SIDE)
+        piece = rows_ref[s].astype(BF).reshape(HALF, 2, SIDE)
+        piece = jnp.concatenate([piece[ROOT:], piece[:ROOT]], axis=0)
+        o_ref[:, :, s * SIDE : (s + 1) * SIDE] = piece
 
 
 def on_device(
@@ -326,7 +332,8 @@
         compiler_params=pltpu.CompilerParams(vmem_limit_bytes=66_700_000),
         name="project",
     )(tokens, w_value, w_first, w_second)
-    arrived = lax.all_to_all(pieces, ROW, 0, 0, tiled=True)
+    members = [[(i + ROOT) % blocks for i in range(blocks)]]
+    arrived = lax.all_to_all(pieces, ROW, 0, 0, tiled=True, axis_index_groups=members)
 
     spec = jax.ShapeDtypeStruct((2, 2 * SIDE, SIDE), F32)
     units = filter_in.shape[1]
@@ -385,7 +392,7 @@
         backs,
         ends,
     )
-    returned = lax.all_to_all(gated, ROW, 0, 0, tiled=True)
+    returned = lax.all_to_all(gated, ROW, 0, 0, tiled=True, axis_index_groups=members)
     returned = returned.reshape(2 * blocks, seqs * tok_rows)
     everyone = lax.all_to_all(
         jnp.broadcast_to(returned[None], (lax.axis_size("x"), *returned.shape)), "x", 0, 0, tiled=True

time: 67.7 us -> 61.4 us (0.907)
  waiting for transfers between devices: 6.95 us -> 0.45 us
  starting transfers between devices: 17.3 us -> 19.3 us
  blocking collectives: 31.6 us -> 29.9 us
    all_to_all x1, waiting for transfers between devices: 6.95 us -> 0.45 us  [on_device(): lax.all_to_all(pieces, ROW, 0, 0, tiled=True, axis_index_groups=members)]
    all_to_all x1, starting transfers between devices: 17.3 us -> 19.3 us  [on_device(): lax.all_to_all(pieces, ROW, 0, 0, tiled=True, axis_index_groups=members)]
    all_to_all x1, blocking collectives: 16.3 us -> 14.8 us  [on_device(): lax.all_to_all(gated, ROW, 0, 0, tiled=True, axis_index_groups=members)]
  transfers between devices with their start and end apart: 1 -> 1, of which waited for: 1 -> 1; matrix products, arithmetic and copies ran while one was open for 0% -> 0% of each run, Pallas kernels for 5% -> 6%
where the time goes in v7:
time: 61.4 us; the launch traced here: 61.1 us
  blocking collectives  29.9 us (49%)
  starting transfers between devices  19.3 us (31%)
  Pallas kernels  9.04 us (15%)
  local copies, waits for them, and re-layouts  1.38 us (2%)
  matrix products  1 us (2%)
    all_to_all x1, starting transfers between devices, on_device(): lax.all_to_all(pieces, ROW, 0, 0, tiled=True, axis_index_groups=members)  19.3 us
    all_to_all x1, blocking collectives, on_device(): lax.all_to_all(gated, ROW, 0, 0, tiled=True, axis_index_groups=members)  14.8 us
    all_to_all x1, blocking collectives, on_device(): lax.all_to_all(jnp.broadcast_to(returned[None], (lax.axis_size('x'), *ret...  9.34 us
    all_gather x1, blocking collectives, on_device(): everyone = lax.all_gather(everyone, 'core', axis=1)  5.73 us
    pallas_call x1, Pallas kernels, on_device(): pl.pallas_call(functools.partial(project_kernel, steps), out_shape=jax.Sh...  3.07 us
    pallas_call x1, Pallas kernels, on_device(): pl.pallas_call(network_kernel, out_shape=(jax.ShapeDtypeStruct((8 * HALF,...  2.87 us
    pallas_call x1, Pallas kernels, on_device(): pl.pallas_call(conv_kernel, out_shape=jax.ShapeDtypeStruct((blocks, 2, se...  2.26 us
    unnamed x26, local copies, waits for them, and re-layouts  1.33 us
  transfers between devices with their start and end apart: 1, of which 1 were waited for; matrix products, arithmetic and copies ran while one was open for 0% of the time, Pallas kernels for 6%

profile of v7, /device:TPU:1, one launch (start us, length us, event | category | flops | bytes accessed | tf_op | source)
XLA Modules:
  0.0 61.1 jit_solution(3362278144018112945)
XLA Ops:
  0.0 3.1 %project.1 = bf16[64,4,384]{2,1,0:T(4,128)(2,1)} custom-call(bf16[2,128,2048]{2,1,0:T(8,128)(2,1)} %tok_hbm.1, bf16[2048,128]{1,0:T(8,128)(2,1)} %a_hbm.1, bf16[2048,128]{1,0:T(8,128)(2,1)} %b_hbm.1, bf16[2048,128]{1,0:T(8,128)(2,1)} %c_hbm.1), custom_call_target="tpu_custom_call" | custom-call | tf_op jit(solution)/shard_map/project/pallas_call | solution.py:321
  3.1 0.0 copy-start
  3.1 0.0 copy-start.1
  3.1 0.0 copy-start.2
  3.1 0.0 copy-start.11
  3.1 19.3 %all-to-all-start = ((bf16[64,4,384]{2,1,0:T(4,128)(2,1)}), bf16[64,4,384]{2,1,0:T(4,128)(2,1)S(1)}, u32[]{:S(2)}, u32[]{:S(2)}) async-start(bf16[64,4,384]{2,1,0:T(4,128)(2,1)} %project.1), calls=%async_computation | async-start | bytes 393216 | tf_op jit(solution)/shard_map/all_to_all | solution.py:336
  22.4 0.0 copy-start.5
  22.4 0.0 copy-done
  22.4 0.0 copy-done.1
  22.4 0.0 copy-done.2
  22.4 0.0 copy-done.11
  22.4 0.6 copy-done.5
  23.1 0.0 copy-start.3
  23.1 0.0 copy-start.6
  23.1 0.0 copy-start.9
  23.1 2.9 %network.1 = (f32[512,128]{1,0:T(8,128)S(1)}, f32[8,128]{1,0:T(8,128)S(1)}) custom-call(f32[64,128]{1,0:T(8,128)S(1)} %copy-done.11, f32[33,64]{1,0:T(8,128)S(1)} %copy-done.2, f32[64,64]{1,0:T(8,128)S(1)} %copy-done.1, f32[256,128]{1,0:T(8,128)S(1)} %bitcast.6, f32[1,128]{1,0:T(1,128)S(1)} %bitcast.7), custom_call_target="tpu_custom_call" | custom-call | flops 4000000000 | bytes 1000000 | tf_op jit(solution)/shard_map/network/pallas_call | solution.py:340
  25.9 0.0 copy-start.4
  25.9 0.0 copy-done.3
  25.9 0.0 copy-done.6
  26.0 0.0 copy-done.9
  26.0 0.0 copy-done.10
  26.0 0.7 %copy-done.4 = f32[2,128]{1,0:T(2,128)S(1)} copy-done((f32[2,128]{1,0:T(2,128)S(1)}, f32[2,128]{1,0:T(2,128)}, u32[]{:S(2)}) %copy-start.4) | copy-done | bytes 1048
  26.6 0.8 %spectra.1 = (f32[2,256,128]{2,1,0:T(8,128)S(1)}, f32[2,256,128]{2,1,0:T(8,128)S(1)}, f32[3,8,256]{2,1,0:T(8,128)S(1)}) custom-call(f32[512,128]{1,0:T(8,128)S(1)} %get-tuple-element.10.rows_ref, f32[8,128]{1,0:T(8,128)S(1)} %get-tuple-element.11.factor_ref, f32[256,128]{1,0:T(8,128)S(1)} %copy-done.9, bf16[256,256]{1,0:T(8,128)(2,1)S(1)} %copy-done.10, ...), custom_call_target="tpu_custom_call" | custom-call | flops 1000000000 | bytes 2000000 | tf_op jit(solution)/shard_map/spectra/pallas_call | solution.py:361
  27.5 0.5 all-to-all-done.x_ref
  27.9 0.0 copy-done.7
  27.9 0.0 copy-done.8
  27.9 2.3 %gated_conv.1 = bf16[64,2,256]{2,1,0:T(2,128)(2,1)S(1)} custom-call(bf16[64,4,384]{2,1,0:T(4,128)(2,1)S(1)} %all-to-all-done.x_ref, f32[3,8,256]{2,1,0:T(8,128)S(1)} %get-tuple-element.12.coef_ref, f32[2,256,128]{2,1,0:T(8,128)S(1)} %get-tuple-element.13.spec_re_ref, f32[2,256,128]{2,1,0:T(8,128)S(1)} %get-tuple-element.14.spec_im_ref, ...), custom_call_target="tpu_custom_call" | custom-call | flops 4000000000 | bytes 2000000 | tf_op jit(solution)/shard_map/gated_conv/pallas_call | solution.py:372
  30.2 14.8 %all_to_all.15 = bf16[64,2,256]{2,1,0:T(2,128)(2,1)S(1)} all-to-all(bf16[64,2,256]{2,1,0:T(2,128)(2,1)S(1)} %gated_conv.1), channel_id=1, replica_groups={{352,360,368,376,384,392,400,408,416,424,432,440,448,456,464,472,480,48..., dimensions={0} | all-to-all | bytes 131072 | tf_op jit(solution)/shard_map/all_to_all | solution.py:395
  45.0 9.3 %all_to_all.16 = bf16[4,128,256]{2,1,0:T(8,128)(2,1)S(1)} all-to-all(bf16[4,128,256]{2,1,0:T(8,128)(2,1)S(1)} %broadcast_in_dim.8), channel_id=1, replica_groups=mesh['row_0'=8,'row_1'=8,'x'=4,'core'=2] {'x'}, dimensions={0} | all-to-all | bytes 524288 | tf_op jit(solution)/shard_map/all_to_all | solution.py:397
  54.4 5.7 %all-gather = bf16[4,256,256]{2,1,0:T(8,128)(2,1)S(1)} all-gather(bf16[4,128,256]{2,1,0:T(8,128)(2,1)S(1)} %all_to_all.16), channel_id=2, replica_groups=mesh['row_0'=8,'row_1'=8,'x'=4,'core'=2] {'core'}, dimensions={1}, use_global_device_ids=true | all-gather | bytes 786432 | tf_op jit(solution)/shard_map/all_gather | solution.py:400
  60.1 0.0 copy-done.12
  60.1 1.0 %convolution_convert_fusion = bf16[256,256]{1,0:T(8,128)(2,1)} fusion(bf16[1024,256]{1,0:T(8,128)(2,1)S(1)} %bitcast.8, bf16[1024,256]{1,0:T(8,128)(2,1)S(1)} %copy-done.12), kind=kOutput, calls=%fused_computation | convolution fusion | flops 134283264 | bytes 1179648 | tf_op jit(solution)/shard_map/ct,cd->td/dot_general | solution.py:402
  (6 shorter events, 0.1 us)
Async XLA Ops:
  3.1 19.3 %copy-start = (f32[64,2,2,128]{3,2,1,0:T(2,128)S(1)}, f32[64,2,2,128]{3,2,1,0:T(2,128)}, u32[]{:S(2)}) copy-start(f32[64,2,2,128]{3,2,1,0:T(2,128)} %param.24) | copy-start | bytes 393220
  3.1 19.3 %copy-start.1 = (f32[64,64]{1,0:T(8,128)S(1)}, f32[64,64]{1,0:T(8,128)}, u32[]{:S(2)}) copy-start(f32[64,64]{1,0:T(8,128)} %mid_ref.1) | copy-start | bytes 49156
  3.1 19.3 %copy-start.2 = (f32[33,64]{1,0:T(8,128)S(1)}, f32[33,64]{1,0:T(8,128)}, u32[]{:S(2)}) copy-start(f32[33,64]{1,0:T(8,128)} %in_ref.1) | copy-start | bytes 25348
  3.1 19.3 %copy-start.11 = (f32[64,128]{1,0:T(8,128)S(1)}, f32[64,128]{1,0:T(8,128)}, u32[]{:S(2)}) copy-start(f32[64,128]{1,0:T(8,128)} %constant.12.clone.waves_ref) | copy-start | bytes 98308
  3.1 24.8 %all-to-all-start = ((bf16[64,4,384]{2,1,0:T(4,128)(2,1)}), bf16[64,4,384]{2,1,0:T(4,128)(2,1)S(1)}, u32[]{:S(2)}, u32[]{:S(2)}) async-start(bf16[64,4,384]{2,1,0:T(4,128)(2,1)} %project.1), calls=%async_computation | async-start | bytes 393216 | tf_op jit(solution)/shard_map/all_to_all | solution.py:336
  22.4 0.7 %copy-start.5 = (f32[128]{0:T(128)S(1)}, f32[128]{0:T(128)}, u32[]{:S(2)}) copy-start(f32[128]{0:T(128)} %param.25) | copy-start | bytes 1540
  23.1 2.9 %copy-start.3 = (f32[3,3,128]{2,1,0:T(4,128)S(1)}, f32[3,3,128]{2,1,0:T(4,128)}, u32[]{:S(2)}) copy-start(f32[3,3,128]{2,1,0:T(4,128)} %taps_ref.1) | copy-start | bytes 13828
  23.1 2.9 %copy-start.6 = (bf16[512,256]{1,0:T(8,128)(2,1)S(1)}, bf16[512,256]{1,0:T(8,128)(2,1)}, u32[]{:S(2)}) copy-start(bf16[512,256]{1,0:T(8,128)(2,1)} %constant.15.clone.right_ref) | copy-start | bytes 786436
  23.1 2.9 %copy-start.9 = (f32[256,128]{1,0:T(8,128)S(1)}, f32[256,128]{1,0:T(8,128)}, u32[]{:S(2)}) copy-start(f32[256,128]{1,0:T(8,128)} %constant.13.clone.turns_ref) | copy-start | bytes 393220
  23.1 2.9 %copy-start.10 = (bf16[256,256]{1,0:T(8,128)(2,1)S(1)}, bf16[256,256]{1,0:T(8,128)(2,1)}, u32[]{:S(2)}) copy-start(bf16[256,256]{1,0:T(8,128)(2,1)} %constant.14.clone.real_ref) | copy-start | bytes 393220
  25.9 0.7 %copy-start.4 = (f32[2,128]{1,0:T(2,128)S(1)}, f32[2,128]{1,0:T(2,128)}, u32[]{:S(2)}) copy-start(f32[2,128]{1,0:T(2,128)} %gain_ref.1) | copy-start | bytes 3076
  26.6 1.3 %copy-start.7 = (bf16[512,256]{1,0:T(8,128)(2,1)S(1)}, bf16[512,256]{1,0:T(8,128)(2,1)}, u32[]{:S(2)}) copy-start(bf16[512,256]{1,0:T(8,128)(2,1)} %constant.16.clone.back_ref) | copy-start | bytes 786436
  26.6 1.3 %copy-start.8 = (bf16[512,256]{1,0:T(8,128)(2,1)S(1)}, bf16[512,256]{1,0:T(8,128)(2,1)}, u32[]{:S(2)}) copy-start(bf16[512,256]{1,0:T(8,128)(2,1)} %constant.17.clone.ends_ref) | copy-start | bytes 786436
  54.4 5.7 %copy-start.12 = (bf16[1024,256]{1,0:T(8,128)(2,1)S(1)}, bf16[1024,256]{1,0:T(8,128)(2,1)}, u32[]{:S(2)}) copy-start(bf16[1024,256]{1,0:T(8,128)(2,1)} %param.27) | copy-start | bytes 1572868

commit v8 on v7

--- a/solution.py
+++ b/solution.py
@@ -15,6 +15,7 @@
 SIDE = 128
 HALF = SIDE // 2
 CHUNK = 4096
+PLANE = 2
 ROOT = 44
 BF = jnp.bfloat16
 F32 = jnp.float32
@@ -369,6 +370,10 @@
         ),
         name="spectra",
     )(rows, factor, turns, real_all, rights, short_taps, skip_gain)
+    planes = lax.axis_size("x")
+    cut = PLANE * (w_output.shape[0] // planes)
+    w_turned = jnp.concatenate([w_output[cut:], w_output[:cut]], axis=0)
+    coef, w_turned = lax.optimization_barrier((coef, w_turned))
     gated = pl.pallas_call(
         conv_kernel,
         out_shape=jax.ShapeDtypeStruct((blocks, 2, seqs * tok_rows), BF),
@@ -394,12 +399,14 @@
     )
     returned = lax.all_to_all(gated, ROW, 0, 0, tiled=True, axis_index_groups=members)
     returned = returned.reshape(2 * blocks, seqs * tok_rows)
+    turned = [[(i + PLANE) % planes for i in range(planes)]]
     everyone = lax.all_to_all(
-        jnp.broadcast_to(returned[None], (lax.axis_size("x"), *returned.shape)), "x", 0, 0, tiled=True
+        jnp.broadcast_to(returned[None], (planes, *returned.shape)),
+        "x", 0, 0, tiled=True, axis_index_groups=turned,
     )
     everyone = lax.all_gather(everyone, "core", axis=1)
     everyone = everyone.reshape(-1, seqs * tok_rows)
-    result = jnp.einsum("ct,cd->td", everyone, w_output, preferred_element_type=F32)
+    result = jnp.einsum("ct,cd->td", everyone, w_turned, preferred_element_type=F32)
     return result.astype(BF).reshape(seqs, tok_rows, -1)
 
 

time: 61.4 us -> 60.6 us (0.987)
  blocking collectives: 29.9 us -> 28.2 us
  local copies, waits for them, and re-layouts: 1.38 us -> 2.43 us
    all_to_all x1, blocking collectives: 9.34 us -> 7.97 us  [on_device(): lax.all_to_all(jnp.broadcast_to(returned[None], (planes, *returned.shape)...]
    unnamed x26, local copies, waits for them, and re-layouts: 1.33 us -> 2.34 us
where the time goes in v8:
time: 60.6 us; the launch traced here: 60.2 us
  blocking collectives  28.2 us (47%)
  starting transfers between devices  19.3 us (32%)
  Pallas kernels  9.05 us (15%)
  local copies, waits for them, and re-layouts  2.43 us (4%)
  matrix products  1 us (2%)
    all_to_all x1, starting transfers between devices, on_device(): lax.all_to_all(pieces, ROW, 0, 0, tiled=True, axis_index_groups=members)  19.3 us
    all_to_all x1, blocking collectives, on_device(): lax.all_to_all(gated, ROW, 0, 0, tiled=True, axis_index_groups=members)  15.1 us
    all_to_all x1, blocking collectives, on_device(): lax.all_to_all(jnp.broadcast_to(returned[None], (planes, *returned.shape)...  7.97 us
    all_gather x1, blocking collectives, on_device(): everyone = lax.all_gather(everyone, 'core', axis=1)  5.12 us
    pallas_call x1, Pallas kernels, on_device(): pl.pallas_call(functools.partial(project_kernel, steps), out_shape=jax.Sh...  3.07 us
    pallas_call x1, Pallas kernels, on_device(): pl.pallas_call(network_kernel, out_shape=(jax.ShapeDtypeStruct((8 * HALF,...  2.87 us
    unnamed x26, local copies, waits for them, and re-layouts  2.34 us
    pallas_call x1, Pallas kernels, on_device(): pl.pallas_call(conv_kernel, out_shape=jax.ShapeDtypeStruct((blocks, 2, se...  2.28 us
  transfers between devices with their start and end apart: 1, of which 1 were waited for; matrix products, arithmetic and copies ran while one was open for 0% of the time, Pallas kernels for 6%

profile of v8, /device:TPU:1, one launch (start us, length us, event | category | flops | bytes accessed | tf_op | source)
XLA Modules:
  0.0 60.2 jit_solution(2783856870853543140)
XLA Ops:
  0.0 3.1 %project.1 = bf16[64,4,384]{2,1,0:T(4,128)(2,1)} custom-call(bf16[2,128,2048]{2,1,0:T(8,128)(2,1)} %tok_hbm.1, bf16[2048,128]{1,0:T(8,128)(2,1)} %a_hbm.1, bf16[2048,128]{1,0:T(8,128)(2,1)} %b_hbm.1, bf16[2048,128]{1,0:T(8,128)(2,1)} %c_hbm.1), custom_call_target="tpu_custom_call" | custom-call | tf_op jit(solution)/shard_map/project/pallas_call | solution.py:322
  3.1 0.0 copy-start
  3.1 0.0 copy-start.1
  3.1 0.0 copy-start.2
  3.1 0.0 copy-start.11
  3.1 19.3 %all-to-all-start = ((bf16[64,4,384]{2,1,0:T(4,128)(2,1)}), bf16[64,4,384]{2,1,0:T(4,128)(2,1)S(1)}, u32[]{:S(2)}, u32[]{:S(2)}) async-start(bf16[64,4,384]{2,1,0:T(4,128)(2,1)} %project.1), calls=%async_computation | async-start | bytes 393216 | tf_op jit(solution)/shard_map/all_to_all | solution.py:337
  22.4 0.0 copy-start.5
  22.4 0.0 copy-done
  22.4 0.0 copy-done.1
  22.4 0.0 copy-done.2
  22.4 0.0 copy-done.11
  22.4 0.6 %copy-done.5 = f32[128]{0:T(128)S(1)} copy-done((f32[128]{0:T(128)S(1)}, f32[128]{0:T(128)}, u32[]{:S(2)}) %copy-start.5) | copy-done | bytes 536
  23.0 0.0 copy-start.3
  23.1 0.0 copy-start.6
  23.1 2.9 %network.1 = (f32[512,128]{1,0:T(8,128)S(1)}, f32[8,128]{1,0:T(8,128)S(1)}) custom-call(f32[64,128]{1,0:T(8,128)S(1)} %copy-done.11, f32[33,64]{1,0:T(8,128)S(1)} %copy-done.2, f32[64,64]{1,0:T(8,128)S(1)} %copy-done.1, f32[256,128]{1,0:T(8,128)S(1)} %bitcast.6, f32[1,128]{1,0:T(1,128)S(1)} %bitcast.7), custom_call_target="tpu_custom_call" | custom-call | flops 4000000000 | bytes 1000000 | tf_op jit(solution)/shard_map/network/pallas_call | solution.py:341
  25.9 0.0 copy-done.3
  25.9 0.0 copy-done.6
  25.9 0.0 copy-done.9
  26.0 0.0 copy-done.10
  26.0 0.7 %copy-done.4 = f32[2,128]{1,0:T(2,128)S(1)} copy-done((f32[2,128]{1,0:T(2,128)S(1)}, f32[2,128]{1,0:T(2,128)}, u32[]{:S(2)}) %copy-start.4) | copy-done | bytes 1048
  26.6 0.8 %spectra.1 = (f32[2,256,128]{2,1,0:T(8,128)S(1)}, f32[2,256,128]{2,1,0:T(8,128)S(1)}, f32[3,8,256]{2,1,0:T(8,128)S(1)}) custom-call(f32[512,128]{1,0:T(8,128)S(1)} %get-tuple-element.12.rows_ref, f32[8,128]{1,0:T(8,128)S(1)} %get-tuple-element.13.factor_ref, f32[256,128]{1,0:T(8,128)S(1)} %copy-done.9, bf16[256,256]{1,0:T(8,128)(2,1)S(1)} %copy-done.10, ...), custom_call_target="tpu_custom_call" | custom-call | flops 1000000000 | bytes 2000000 | tf_op jit(solution)/shard_map/spectra/pallas_call | solution.py:362
  27.5 0.2 copy-done.12
  27.7 0.0 copy-start.7
  27.7 0.0 copy-start.8
  27.8 0.1 all-to-all-done.x_ref
  27.9 0.7 %copy-done.7 = bf16[512,256]{1,0:T(8,128)(2,1)S(1)} copy-done((bf16[512,256]{1,0:T(8,128)(2,1)S(1)}, bf16[512,256]{1,0:T(8,128)(2,1)}, u32[]{:S(2)}) %copy-start.7) | copy-done | bytes 262168
  28.7 0.1 copy-done.8
  28.7 2.3 %gated_conv.1 = bf16[64,2,256]{2,1,0:T(2,128)(2,1)S(1)} custom-call(bf16[64,4,384]{2,1,0:T(4,128)(2,1)S(1)} %all-to-all-done.x_ref, f32[3,8,256]{2,1,0:T(8,128)S(1)} %get-tuple-element.15.coef_ref, f32[2,256,128]{2,1,0:T(8,128)S(1)} %get-tuple-element.16.spec_re_ref, f32[2,256,128]{2,1,0:T(8,128)S(1)} %get-tuple-element.17.spec_im_ref, ...), custom_call_target="tpu_custom_call" | custom-call | flops 4000000000 | bytes 2000000 | tf_op jit(solution)/shard_map/gated_conv/pallas_call | solution.py:377
  31.0 15.1 %all_to_all.15 = bf16[64,2,256]{2,1,0:T(2,128)(2,1)S(1)} all-to-all(bf16[64,2,256]{2,1,0:T(2,128)(2,1)S(1)} %gated_conv.1), channel_id=1, replica_groups={{352,360,368,376,384,392,400,408,416,424,432,440,448,456,464,472,480,48..., dimensions={0} | all-to-all | bytes 131072 | tf_op jit(solution)/shard_map/all_to_all | solution.py:400
  46.1 8.0 %all_to_all.16 = bf16[4,128,256]{2,1,0:T(8,128)(2,1)S(1)} all-to-all(bf16[4,128,256]{2,1,0:T(8,128)(2,1)S(1)} %broadcast_in_dim.8), channel_id=1, replica_groups={{4,6,0,2},{5,7,1,3},{12,14,8,10},{13,15,9,11},{20,22,16,18},{21,23,17,1..., dimensions={0} | all-to-all | bytes 524288 | tf_op jit(solution)/shard_map/all_to_all | solution.py:403
  54.1 5.1 %all-gather = bf16[4,256,256]{2,1,0:T(8,128)(2,1)S(1)} all-gather(bf16[4,128,256]{2,1,0:T(8,128)(2,1)S(1)} %all_to_all.16), channel_id=2, replica_groups=mesh['row_0'=8,'row_1'=8,'x'=4,'core'=2] {'core'}, dimensions={1}, use_global_device_ids=true | all-gather | bytes 786432 | tf_op jit(solution)/shard_map/all_gather | solution.py:407
  59.2 1.0 %convolution_convert_fusion = bf16[256,256]{1,0:T(8,128)(2,1)} fusion(bf16[1024,256]{1,0:T(8,128)(2,1)S(1)} %bitcast.8, bf16[1024,256]{1,0:T(8,128)(2,1)S(1)} %pad_maximum_fusion), kind=kOutput, calls=%fused_computation | convolution fusion | flops 134283264 | bytes 1179648 | tf_op jit(solution)/shard_map/ct,cd->td/dot_general | solution.py:409
  (8 shorter events, 0.1 us)
Async XLA Ops:
  3.1 19.3 %copy-start = (f32[64,2,2,128]{3,2,1,0:T(2,128)S(1)}, f32[64,2,2,128]{3,2,1,0:T(2,128)}, u32[]{:S(2)}) copy-start(f32[64,2,2,128]{3,2,1,0:T(2,128)} %param.24) | copy-start | bytes 393220
  3.1 19.3 %copy-start.1 = (f32[64,64]{1,0:T(8,128)S(1)}, f32[64,64]{1,0:T(8,128)}, u32[]{:S(2)}) copy-start(f32[64,64]{1,0:T(8,128)} %mid_ref.1) | copy-start | bytes 49156
  3.1 19.3 %copy-start.2 = (f32[33,64]{1,0:T(8,128)S(1)}, f32[33,64]{1,0:T(8,128)}, u32[]{:S(2)}) copy-start(f32[33,64]{1,0:T(8,128)} %in_ref.1) | copy-start | bytes 25348
  3.1 19.3 %copy-start.11 = (f32[64,128]{1,0:T(8,128)S(1)}, f32[64,128]{1,0:T(8,128)}, u32[]{:S(2)}) copy-start(f32[64,128]{1,0:T(8,128)} %constant.12.clone.waves_ref) | copy-start | bytes 98308
  3.1 24.8 %all-to-all-start = ((bf16[64,4,384]{2,1,0:T(4,128)(2,1)}), bf16[64,4,384]{2,1,0:T(4,128)(2,1)S(1)}, u32[]{:S(2)}, u32[]{:S(2)}) async-start(bf16[64,4,384]{2,1,0:T(4,128)(2,1)} %project.1), calls=%async_computation | async-start | bytes 393216 | tf_op jit(solution)/shard_map/all_to_all | solution.py:337
  22.4 0.7 %copy-start.5 = (f32[128]{0:T(128)S(1)}, f32[128]{0:T(128)}, u32[]{:S(2)}) copy-start(f32[128]{0:T(128)} %param.25) | copy-start | bytes 1540
  23.0 2.9 %copy-start.3 = (f32[3,3,128]{2,1,0:T(4,128)S(1)}, f32[3,3,128]{2,1,0:T(4,128)}, u32[]{:S(2)}) copy-start(f32[3,3,128]{2,1,0:T(4,128)} %taps_ref.1) | copy-start | bytes 13828
  23.1 2.9 %copy-start.6 = (bf16[512,256]{1,0:T(8,128)(2,1)S(1)}, bf16[512,256]{1,0:T(8,128)(2,1)}, u32[]{:S(2)}) copy-start(bf16[512,256]{1,0:T(8,128)(2,1)} %constant.15.clone.right_ref) | copy-start | bytes 786436
  23.1 2.9 %copy-start.9 = (f32[256,128]{1,0:T(8,128)S(1)}, f32[256,128]{1,0:T(8,128)}, u32[]{:S(2)}) copy-start(f32[256,128]{1,0:T(8,128)} %constant.13.clone.turns_ref) | copy-start | bytes 393220
  23.1 2.9 %copy-start.10 = (bf16[256,256]{1,0:T(8,128)(2,1)S(1)}, bf16[256,256]{1,0:T(8,128)(2,1)}, u32[]{:S(2)}) copy-start(bf16[256,256]{1,0:T(8,128)(2,1)} %constant.14.clone.real_ref) | copy-start | bytes 393220
  25.9 0.7 %copy-start.4 = (f32[2,128]{1,0:T(2,128)S(1)}, f32[2,128]{1,0:T(2,128)}, u32[]{:S(2)}) copy-start(f32[2,128]{1,0:T(2,128)} %gain_ref.1) | copy-start | bytes 3076
  26.6 1.0 %copy-start.12 = (bf16[1024,256]{1,0:T(8,128)(2,1)S(1)}, bf16[1024,256]{1,0:T(8,128)(2,1)}, u32[]{:S(2)}) copy-start(bf16[1024,256]{1,0:T(8,128)(2,1)} %param.27) | copy-start | bytes 1572868
  27.7 1.0 %copy-start.7 = (bf16[512,256]{1,0:T(8,128)(2,1)S(1)}, bf16[512,256]{1,0:T(8,128)(2,1)}, u32[]{:S(2)}) copy-start(bf16[512,256]{1,0:T(8,128)(2,1)} %constant.16.clone.back_ref) | copy-start | bytes 786436
  27.7 1.0 %copy-start.8 = (bf16[512,256]{1,0:T(8,128)(2,1)S(1)}, bf16[512,256]{1,0:T(8,128)(2,1)}, u32[]{:S(2)}) copy-start(bf16[512,256]{1,0:T(8,128)(2,1)} %constant.17.clone.ends_ref) | copy-start | bytes 786436

commit v9 on v8

--- a/solution.py
+++ b/solution.py
@@ -298,6 +298,15 @@
         o_ref[:, :, s * SIDE : (s + 1) * SIDE] = piece
 
 
+def output_kernel(all_ref, w_ref, o_ref):
+    rows = all_ref.shape[0]
+    cut = PLANE * (rows // 4)
+    first = (((0,), (0,)), ((), ()))
+    total = mm(all_ref[: rows - cut, :], w_ref[cut:, :], first)
+    total += mm(all_ref[rows - cut :, :], w_ref[:cut, :], first)
+    o_ref[...] = total.astype(BF)
+
+
 def on_device(
     tokens,
     w_value,
@@ -371,9 +380,6 @@
         name="spectra",
     )(rows, factor, turns, real_all, rights, short_taps, skip_gain)
     planes = lax.axis_size("x")
-    cut = PLANE * (w_output.shape[0] // planes)
-    w_turned = jnp.concatenate([w_output[cut:], w_output[:cut]], axis=0)
-    coef, w_turned = lax.optimization_barrier((coef, w_turned))
     gated = pl.pallas_call(
         conv_kernel,
         out_shape=jax.ShapeDtypeStruct((blocks, 2, seqs * tok_rows), BF),
@@ -406,8 +412,18 @@
     )
     everyone = lax.all_gather(everyone, "core", axis=1)
     everyone = everyone.reshape(-1, seqs * tok_rows)
-    result = jnp.einsum("ct,cd->td", everyone, w_turned, preferred_element_type=F32)
-    return result.astype(BF).reshape(seqs, tok_rows, -1)
+    result = pl.pallas_call(
+        output_kernel,
+        out_shape=jax.ShapeDtypeStruct((seqs * tok_rows, w_output.shape[1]), BF),
+        in_specs=[vmem] * 2,
+        out_specs=vmem,
+        compiler_params=pltpu.CompilerParams(vmem_limit_bytes=16 * 2**20),
+        cost_estimate=pl.CostEstimate(
+            flops=134_217_728, bytes_accessed=1_200_000, transcendentals=0
+        ),
+        name="output_map",
+    )(everyone, w_output)
+    return result.reshape(seqs, tok_rows, -1)
 
 
 def solution(mesh):

time: 60.6 us -> 59.6 us (0.983)
  local copies, waits for them, and re-layouts: 2.43 us -> 1.38 us
  matrix products: 1 us -> 0 us
  Pallas kernels: 9.05 us -> 10 us
    unnamed x26, local copies, waits for them, and re-layouts: 2.34 us -> 1.33 us
    dot_general x1 -> x0, matrix products: 1 us -> none  [on_device(): jnp.einsum('ct,cd->td', everyone, w_turned, preferred_element_type=F32)]
    pallas_call x0 -> x1, Pallas kernels: none -> 1 us  [on_device(): pl.pallas_call(output_kernel, out_shape=jax.ShapeDtypeStruct((seqs * tok_...]
where the time goes in v9:
time: 59.6 us; the launch traced here: 59.3 us
  blocking collectives  28 us (47%)
  starting transfers between devices  19.3 us (32%)
  Pallas kernels  10 us (17%)
  local copies, waits for them, and re-layouts  1.38 us (2%)
    all_to_all x1, starting transfers between devices, on_device(): lax.all_to_all(pieces, ROW, 0, 0, tiled=True, axis_index_groups=members)  19.3 us
    all_to_all x1, blocking collectives, on_device(): lax.all_to_all(gated, ROW, 0, 0, tiled=True, axis_index_groups=members)  14.8 us
    all_to_all x1, blocking collectives, on_device(): lax.all_to_all(jnp.broadcast_to(returned[None], (planes, *returned.shape)...  7.97 us
    all_gather x1, blocking collectives, on_device(): everyone = lax.all_gather(everyone, 'core', axis=1)  5.26 us
    pallas_call x1, Pallas kernels, on_device(): pl.pallas_call(functools.partial(project_kernel, steps), out_shape=jax.Sh...  3.07 us
    pallas_call x1, Pallas kernels, on_device(): pl.pallas_call(network_kernel, out_shape=(jax.ShapeDtypeStruct((8 * HALF,...  2.87 us
    pallas_call x1, Pallas kernels, on_device(): pl.pallas_call(conv_kernel, out_shape=jax.ShapeDtypeStruct((blocks, 2, se...  2.26 us
    unnamed x26, local copies, waits for them, and re-layouts  1.33 us
  transfers between devices with their start and end apart: 1, of which 1 were waited for; matrix products, arithmetic and copies ran while one was open for 0% of the time, Pallas kernels for 6%

profile of v9, /device:TPU:1, one launch (start us, length us, event | category | flops | bytes accessed | tf_op | source)
XLA Modules:
  0.0 59.3 jit_solution(6818359449546298282)
XLA Ops:
  0.0 3.1 %project.1 = bf16[64,4,384]{2,1,0:T(4,128)(2,1)} custom-call(bf16[2,128,2048]{2,1,0:T(8,128)(2,1)} %tok_hbm.1, bf16[2048,128]{1,0:T(8,128)(2,1)} %a_hbm.1, bf16[2048,128]{1,0:T(8,128)(2,1)} %b_hbm.1, bf16[2048,128]{1,0:T(8,128)(2,1)} %c_hbm.1), custom_call_target="tpu_custom_call" | custom-call | tf_op jit(solution)/shard_map/project/pallas_call | solution.py:331
  3.1 0.0 copy-start.1
  3.1 0.0 copy-start.2
  3.1 0.0 copy-start.3
  3.1 0.0 copy-start.12
  3.1 19.3 %all-to-all-start = ((bf16[64,4,384]{2,1,0:T(4,128)(2,1)}), bf16[64,4,384]{2,1,0:T(4,128)(2,1)S(1)}, u32[]{:S(2)}, u32[]{:S(2)}) async-start(bf16[64,4,384]{2,1,0:T(4,128)(2,1)} %project.1), calls=%async_computation | async-start | bytes 393216 | tf_op jit(solution)/shard_map/all_to_all | solution.py:346
  22.4 0.0 copy-start.6
  22.4 0.0 copy-done.1
  22.4 0.0 copy-done.2
  22.4 0.0 copy-done.3
  22.4 0.0 copy-done.12
  22.4 0.6 %copy-done.6 = f32[128]{0:T(128)S(1)} copy-done((f32[128]{0:T(128)S(1)}, f32[128]{0:T(128)}, u32[]{:S(2)}) %copy-start.6) | copy-done | bytes 536
  23.1 0.0 copy-start.4
  23.1 0.0 copy-start.7
  23.1 0.0 copy-start.10
  23.1 0.0 copy-start.11
  23.1 2.9 %network.1 = (f32[512,128]{1,0:T(8,128)S(1)}, f32[8,128]{1,0:T(8,128)S(1)}) custom-call(f32[64,128]{1,0:T(8,128)S(1)} %copy-done.12, f32[33,64]{1,0:T(8,128)S(1)} %copy-done.3, f32[64,64]{1,0:T(8,128)S(1)} %copy-done.2, f32[256,128]{1,0:T(8,128)S(1)} %bitcast.5, f32[1,128]{1,0:T(1,128)S(1)} %bitcast.6), custom_call_target="tpu_custom_call" | custom-call | flops 4000000000 | bytes 1000000 | tf_op jit(solution)/shard_map/network/pallas_call | solution.py:350
  25.9 0.0 copy-done.4
  25.9 0.0 copy-done.7
  26.0 0.0 copy-done.10
  26.0 0.0 copy-done.11
  26.0 0.7 %copy-done.5 = f32[2,128]{1,0:T(2,128)S(1)} copy-done((f32[2,128]{1,0:T(2,128)S(1)}, f32[2,128]{1,0:T(2,128)}, u32[]{:S(2)}) %copy-start.5) | copy-done | bytes 1048
  26.6 0.8 %spectra.1 = (f32[2,256,128]{2,1,0:T(8,128)S(1)}, f32[2,256,128]{2,1,0:T(8,128)S(1)}, f32[3,8,256]{2,1,0:T(8,128)S(1)}) custom-call(f32[512,128]{1,0:T(8,128)S(1)} %get-tuple-element.10.rows_ref, f32[8,128]{1,0:T(8,128)S(1)} %get-tuple-element.11.factor_ref, f32[256,128]{1,0:T(8,128)S(1)} %copy-done.10, bf16[256,256]{1,0:T(8,128)(2,1)S(1)} %copy-done.11, ...), custom_call_target="tpu_custom_call" | custom-call | flops 1000000000 | bytes 2000000 | tf_op jit(solution)/shard_map/spectra/pallas_call | solution.py:371
  27.5 0.5 all-to-all-done.x_ref
  27.9 0.0 copy-done.8
  27.9 0.0 copy-done.9
  27.9 2.3 %gated_conv.1 = bf16[64,2,256]{2,1,0:T(2,128)(2,1)S(1)} custom-call(bf16[64,4,384]{2,1,0:T(4,128)(2,1)S(1)} %all-to-all-done.x_ref, f32[3,8,256]{2,1,0:T(8,128)S(1)} %get-tuple-element.12.coef_ref, f32[2,256,128]{2,1,0:T(8,128)S(1)} %get-tuple-element.13.spec_re_ref, f32[2,256,128]{2,1,0:T(8,128)S(1)} %get-tuple-element.14.spec_im_ref, ...), custom_call_target="tpu_custom_call" | custom-call | flops 4000000000 | bytes 2000000 | tf_op jit(solution)/shard_map/gated_conv/pallas_call | solution.py:383
  30.2 14.8 %all_to_all.15 = bf16[64,2,256]{2,1,0:T(2,128)(2,1)S(1)} all-to-all(bf16[64,2,256]{2,1,0:T(2,128)(2,1)S(1)} %gated_conv.1), channel_id=1, replica_groups={{352,360,368,376,384,392,400,408,416,424,432,440,448,456,464,472,480,48..., dimensions={0} | all-to-all | bytes 131072 | tf_op jit(solution)/shard_map/all_to_all | solution.py:406
  45.0 8.0 %all_to_all.16 = bf16[4,128,256]{2,1,0:T(8,128)(2,1)S(1)} all-to-all(bf16[4,128,256]{2,1,0:T(8,128)(2,1)S(1)} %broadcast_in_dim.8), channel_id=1, replica_groups={{4,6,0,2},{5,7,1,3},{12,14,8,10},{13,15,9,11},{20,22,16,18},{21,23,17,1..., dimensions={0} | all-to-all | bytes 524288 | tf_op jit(solution)/shard_map/all_to_all | solution.py:409
  53.0 5.3 %all-gather = bf16[4,256,256]{2,1,0:T(8,128)(2,1)S(1)} all-gather(bf16[4,128,256]{2,1,0:T(8,128)(2,1)S(1)} %all_to_all.16), channel_id=2, replica_groups=mesh['row_0'=8,'row_1'=8,'x'=4,'core'=2] {'core'}, dimensions={1}, use_global_device_ids=true | all-gather | bytes 786432 | tf_op jit(solution)/shard_map/all_gather | solution.py:413
  58.3 0.0 copy-done
  58.3 1.0 %output_map.1 = bf16[256,256]{1,0:T(8,128)(2,1)} custom-call(bf16[1024,256]{1,0:T(8,128)(2,1)S(1)} %bitcast.4, bf16[1024,256]{1,0:T(8,128)(2,1)S(1)} %copy-done), custom_call_target="tpu_custom_call" | custom-call | flops 134217728 | bytes 1200000 | tf_op jit(solution)/shard_map/output_map/pallas_call | solution.py:415
  (6 shorter events, 0.1 us)
Async XLA Ops:
  3.1 19.3 %copy-start.1 = (f32[64,2,2,128]{3,2,1,0:T(2,128)S(1)}, f32[64,2,2,128]{3,2,1,0:T(2,128)}, u32[]{:S(2)}) copy-start(f32[64,2,2,128]{3,2,1,0:T(2,128)} %param.24) | copy-start | bytes 393220
  3.1 19.3 %copy-start.2 = (f32[64,64]{1,0:T(8,128)S(1)}, f32[64,64]{1,0:T(8,128)}, u32[]{:S(2)}) copy-start(f32[64,64]{1,0:T(8,128)} %mid_ref.1) | copy-start | bytes 49156
  3.1 19.3 %copy-start.3 = (f32[33,64]{1,0:T(8,128)S(1)}, f32[33,64]{1,0:T(8,128)}, u32[]{:S(2)}) copy-start(f32[33,64]{1,0:T(8,128)} %in_ref.1) | copy-start | bytes 25348
  3.1 19.3 %copy-start.12 = (f32[64,128]{1,0:T(8,128)S(1)}, f32[64,128]{1,0:T(8,128)}, u32[]{:S(2)}) copy-start(f32[64,128]{1,0:T(8,128)} %constant.12.clone.waves_ref) | copy-start | bytes 98308
  3.1 24.8 %all-to-all-start = ((bf16[64,4,384]{2,1,0:T(4,128)(2,1)}), bf16[64,4,384]{2,1,0:T(4,128)(2,1)S(1)}, u32[]{:S(2)}, u32[]{:S(2)}) async-start(bf16[64,4,384]{2,1,0:T(4,128)(2,1)} %project.1), calls=%async_computation | async-start | bytes 393216 | tf_op jit(solution)/shard_map/all_to_all | solution.py:346
  22.4 0.7 %copy-start.6 = (f32[128]{0:T(128)S(1)}, f32[128]{0:T(128)}, u32[]{:S(2)}) copy-start(f32[128]{0:T(128)} %param.25) | copy-start | bytes 1540
  23.1 2.9 %copy-start.4 = (f32[3,3,128]{2,1,0:T(4,128)S(1)}, f32[3,3,128]{2,1,0:T(4,128)}, u32[]{:S(2)}) copy-start(f32[3,3,128]{2,1,0:T(4,128)} %taps_ref.1) | copy-start | bytes 13828
  23.1 2.9 %copy-start.7 = (bf16[512,256]{1,0:T(8,128)(2,1)S(1)}, bf16[512,256]{1,0:T(8,128)(2,1)}, u32[]{:S(2)}) copy-start(bf16[512,256]{1,0:T(8,128)(2,1)} %constant.15.clone.right_ref) | copy-start | bytes 786436
  23.1 2.9 %copy-start.10 = (f32[256,128]{1,0:T(8,128)S(1)}, f32[256,128]{1,0:T(8,128)}, u32[]{:S(2)}) copy-start(f32[256,128]{1,0:T(8,128)} %constant.13.clone.turns_ref) | copy-start | bytes 393220
  23.1 2.9 %copy-start.11 = (bf16[256,256]{1,0:T(8,128)(2,1)S(1)}, bf16[256,256]{1,0:T(8,128)(2,1)}, u32[]{:S(2)}) copy-start(bf16[256,256]{1,0:T(8,128)(2,1)} %constant.14.clone.real_ref) | copy-start | bytes 393220
  25.9 0.7 %copy-start.5 = (f32[2,128]{1,0:T(2,128)S(1)}, f32[2,128]{1,0:T(2,128)}, u32[]{:S(2)}) copy-start(f32[2,128]{1,0:T(2,128)} %gain_ref.1) | copy-start | bytes 3076
  26.6 1.3 %copy-start.8 = (bf16[512,256]{1,0:T(8,128)(2,1)S(1)}, bf16[512,256]{1,0:T(8,128)(2,1)}, u32[]{:S(2)}) copy-start(bf16[512,256]{1,0:T(8,128)(2,1)} %constant.16.clone.back_ref) | copy-start | bytes 786436
  26.6 1.3 %copy-start.9 = (bf16[512,256]{1,0:T(8,128)(2,1)S(1)}, bf16[512,256]{1,0:T(8,128)(2,1)}, u32[]{:S(2)}) copy-start(bf16[512,256]{1,0:T(8,128)(2,1)} %constant.17.clone.ends_ref) | copy-start | bytes 786436
  53.0 5.3 %copy-start = (bf16[1024,256]{1,0:T(8,128)(2,1)S(1)}, bf16[1024,256]{1,0:T(8,128)(2,1)}, u32[]{:S(2)}) copy-start(bf16[1024,256]{1,0:T(8,128)(2,1)} %w_ref.1) | copy-start | bytes 1572868

commit v10 on v9

--- a/solution.py
+++ b/solution.py
@@ -295,7 +295,8 @@
             ]
         piece = rows_ref[s].astype(BF).reshape(HALF, 2, SIDE)
         piece = jnp.concatenate([piece[ROOT:], piece[:ROOT]], axis=0)
-        o_ref[:, :, s * SIDE : (s + 1) * SIDE] = piece
+        for plane in range(o_ref.shape[0]):
+            o_ref[plane, :, :, s * SIDE : (s + 1) * SIDE] = piece
 
 
 def output_kernel(all_ref, w_ref, o_ref):
@@ -382,7 +383,7 @@
     planes = lax.axis_size("x")
     gated = pl.pallas_call(
         conv_kernel,
-        out_shape=jax.ShapeDtypeStruct((blocks, 2, seqs * tok_rows), BF),
+        out_shape=jax.ShapeDtypeStruct((planes, blocks, 2, seqs * tok_rows), BF),
         in_specs=[vmem] * 8,
         out_specs=vmem,
         scratch_shapes=[
@@ -403,13 +404,14 @@
         backs,
         ends,
     )
-    returned = lax.all_to_all(gated, ROW, 0, 0, tiled=True, axis_index_groups=members)
-    returned = returned.reshape(2 * blocks, seqs * tok_rows)
-    turned = [[(i + PLANE) % planes for i in range(planes)]]
+    turned = [
+        [((i // blocks + PLANE) % planes) * blocks + (i + ROOT) % blocks for i in range(planes * blocks)]
+    ]
     everyone = lax.all_to_all(
-        jnp.broadcast_to(returned[None], (planes, *returned.shape)),
-        "x", 0, 0, tiled=True, axis_index_groups=turned,
-    )
+        gated.reshape(planes * blocks, *gated.shape[2:]),
+        ("x", *ROW), 0, 0, tiled=True, axis_index_groups=turned,
+    )
+    everyone = everyone.reshape(planes, 2 * blocks, seqs * tok_rows)
     everyone = lax.all_gather(everyone, "core", axis=1)
     everyone = everyone.reshape(-1, seqs * tok_rows)
     result = pl.pallas_call(

time: 59.6 us -> 58.4 us (0.980)
  blocking collectives: 28 us -> 26.7 us
    all_gather x1, blocking collectives: 5.26 us -> 3.91 us  [on_device(): everyone = lax.all_gather(everyone, 'core', axis=1)]
    all_to_all x2 -> x1, blocking collectives: 22.8 us -> 22.8 us  [on_device(): lax.all_to_all(gated.reshape(planes * blocks, *gated.shape[2:]), ('x', *R...]
where the time goes in v10:
time: 58.4 us; the launch traced here: 58.1 us
  blocking collectives  26.7 us (46%)
  starting transfers between devices  19.3 us (33%)
  Pallas kernels  10.1 us (17%)
  local copies, waits for them, and re-layouts  1.43 us (2%)
    all_to_all x1, blocking collectives, on_device(): lax.all_to_all(gated.reshape(planes * blocks, *gated.shape[2:]), ('x', *R...  22.8 us
    all_to_all x1, starting transfers between devices, on_device(): lax.all_to_all(pieces, ROW, 0, 0, tiled=True, axis_index_groups=members)  19.3 us
    all_gather x1, blocking collectives, on_device(): everyone = lax.all_gather(everyone, 'core', axis=1)  3.91 us
    pallas_call x1, Pallas kernels, on_device(): pl.pallas_call(functools.partial(project_kernel, steps), out_shape=jax.Sh...  3.07 us
    pallas_call x1, Pallas kernels, on_device(): pl.pallas_call(network_kernel, out_shape=(jax.ShapeDtypeStruct((8 * HALF,...  2.87 us
    pallas_call x1, Pallas kernels, on_device(): pl.pallas_call(conv_kernel, out_shape=jax.ShapeDtypeStruct((planes, block...  2.34 us
    unnamed x26, local copies, waits for them, and re-layouts  1.33 us
  transfers between devices with their start and end apart: 1, of which 1 were waited for; matrix products, arithmetic and copies ran while one was open for 0% of the time, Pallas kernels for 6%

profile of v10, /device:TPU:1, one launch (start us, length us, event | category | flops | bytes accessed | tf_op | source)
XLA Modules:
  0.0 58.1 jit_solution(11714097904383233001)
XLA Ops:
  0.0 3.1 %project.1 = bf16[64,4,384]{2,1,0:T(4,128)(2,1)} custom-call(bf16[2,128,2048]{2,1,0:T(8,128)(2,1)} %tok_hbm.1, bf16[2048,128]{1,0:T(8,128)(2,1)} %a_hbm.1, bf16[2048,128]{1,0:T(8,128)(2,1)} %b_hbm.1, bf16[2048,128]{1,0:T(8,128)(2,1)} %c_hbm.1), custom_call_target="tpu_custom_call" | custom-call | tf_op jit(solution)/shard_map/project/pallas_call | solution.py:332
  3.1 0.0 copy-start.1
  3.1 0.0 copy-start.2
  3.1 0.0 copy-start.3
  3.1 0.0 copy-start.12
  3.1 19.3 %all-to-all-start = ((bf16[64,4,384]{2,1,0:T(4,128)(2,1)}), bf16[64,4,384]{2,1,0:T(4,128)(2,1)S(1)}, u32[]{:S(2)}, u32[]{:S(2)}) async-start(bf16[64,4,384]{2,1,0:T(4,128)(2,1)} %project.1), calls=%async_computation | async-start | bytes 393216 | tf_op jit(solution)/shard_map/all_to_all | solution.py:347
  22.4 0.0 copy-start.6
  22.4 0.0 copy-done.1
  22.4 0.0 copy-done.2
  22.4 0.0 copy-done.3
  22.4 0.0 copy-done.12
  22.4 0.6 %copy-done.6 = f32[128]{0:T(128)S(1)} copy-done((f32[128]{0:T(128)S(1)}, f32[128]{0:T(128)}, u32[]{:S(2)}) %copy-start.6) | copy-done | bytes 536
  23.1 0.0 copy-start.4
  23.1 0.0 copy-start.7
  23.1 0.0 copy-start.10
  23.1 2.9 %network.1 = (f32[512,128]{1,0:T(8,128)S(1)}, f32[8,128]{1,0:T(8,128)S(1)}) custom-call(f32[64,128]{1,0:T(8,128)S(1)} %copy-done.12, f32[33,64]{1,0:T(8,128)S(1)} %copy-done.3, f32[64,64]{1,0:T(8,128)S(1)} %copy-done.2, f32[256,128]{1,0:T(8,128)S(1)} %bitcast.7, f32[1,128]{1,0:T(1,128)S(1)} %bitcast.8), custom_call_target="tpu_custom_call" | custom-call | flops 4000000000 | bytes 1000000 | tf_op jit(solution)/shard_map/network/pallas_call | solution.py:351
  25.9 0.0 copy-done.4
  25.9 0.0 copy-done.7
  26.0 0.0 copy-done.10
  26.0 0.0 copy-done.11
  26.0 0.7 %copy-done.5 = f32[2,128]{1,0:T(2,128)S(1)} copy-done((f32[2,128]{1,0:T(2,128)S(1)}, f32[2,128]{1,0:T(2,128)}, u32[]{:S(2)}) %copy-start.5) | copy-done | bytes 1048
  26.6 0.8 %spectra.1 = (f32[2,256,128]{2,1,0:T(8,128)S(1)}, f32[2,256,128]{2,1,0:T(8,128)S(1)}, f32[3,8,256]{2,1,0:T(8,128)S(1)}) custom-call(f32[512,128]{1,0:T(8,128)S(1)} %get-tuple-element.10.rows_ref, f32[8,128]{1,0:T(8,128)S(1)} %get-tuple-element.11.factor_ref, f32[256,128]{1,0:T(8,128)S(1)} %copy-done.10, bf16[256,256]{1,0:T(8,128)(2,1)S(1)} %copy-done.11, ...), custom_call_target="tpu_custom_call" | custom-call | flops 1000000000 | bytes 2000000 | tf_op jit(solution)/shard_map/spectra/pallas_call | solution.py:372
  27.5 0.5 all-to-all-done.x_ref
  27.9 0.0 copy-done.8
  27.9 0.0 copy-done.9
  27.9 2.3 %gated_conv.1 = bf16[4,64,2,256]{3,2,1,0:T(2,128)(2,1)S(1)} custom-call(bf16[64,4,384]{2,1,0:T(4,128)(2,1)S(1)} %all-to-all-done.x_ref, f32[3,8,256]{2,1,0:T(8,128)S(1)} %get-tuple-element.12.coef_ref, f32[2,256,128]{2,1,0:T(8,128)S(1)} %get-tuple-element.13.spec_re_ref, f32[2,256,128]{2,1,0:T(8,128)S(1)} %get-tuple-element.14.spec_im_ref, ...), custom_call_target="tpu_custom_call" | custom-call | flops 4000000000 | bytes 2000000 | tf_op jit(solution)/shard_map/gated_conv/pallas_call | solution.py:384
  30.3 22.8 %all_to_all.10 = bf16[256,2,256]{2,1,0:T(2,128)(2,1)S(1)} all-to-all(bf16[256,2,256]{2,1,0:T(2,128)(2,1)S(1)} %bitcast.6), channel_id=1, replica_groups={{356,364,372,380,388,396,404,412,420,428,436,444,452,460,468,476,484,49..., dimensions={0} | all-to-all | bytes 524288 | tf_op jit(solution)/shard_map/all_to_all | solution.py:410
  53.1 0.1 all_gather_reshape.3
  53.2 0.0 copy-start
  53.2 3.9 %all_gather.3 = bf16[4,2,128,256]{3,2,1,0:T(8,128)(2,1)S(1)} all-gather(bf16[4,1,128,256]{3,2,1,0:T(8,128)(2,1)S(1)} %all_gather_reshape.3), channel_id=1, replica_groups=mesh['row_0'=8,'row_1'=8,'x'=4,'core'=2] {'core'}, dimensions={1}, use_global_device_ids=true | all-gather | bytes 786432 | tf_op jit(solution)/shard_map/all_gather | solution.py:415
  57.1 0.0 copy-done
  57.1 1.0 %output_map.1 = bf16[256,256]{1,0:T(8,128)(2,1)} custom-call(bf16[1024,256]{1,0:T(8,128)(2,1)S(1)} %bitcast.5, bf16[1024,256]{1,0:T(8,128)(2,1)S(1)} %copy-done), custom_call_target="tpu_custom_call" | custom-call | flops 134217728 | bytes 1200000 | tf_op jit(solution)/shard_map/output_map/pallas_call | solution.py:417
  (4 shorter events, 0.0 us)
Async XLA Ops:
  3.1 19.3 %copy-start.1 = (f32[64,2,2,128]{3,2,1,0:T(2,128)S(1)}, f32[64,2,2,128]{3,2,1,0:T(2,128)}, u32[]{:S(2)}) copy-start(f32[64,2,2,128]{3,2,1,0:T(2,128)} %param.24) | copy-start | bytes 393220
  3.1 19.3 %copy-start.2 = (f32[64,64]{1,0:T(8,128)S(1)}, f32[64,64]{1,0:T(8,128)}, u32[]{:S(2)}) copy-start(f32[64,64]{1,0:T(8,128)} %mid_ref.1) | copy-start | bytes 49156
  3.1 19.3 %copy-start.3 = (f32[33,64]{1,0:T(8,128)S(1)}, f32[33,64]{1,0:T(8,128)}, u32[]{:S(2)}) copy-start(f32[33,64]{1,0:T(8,128)} %in_ref.1) | copy-start | bytes 25348
  3.1 19.3 %copy-start.12 = (f32[64,128]{1,0:T(8,128)S(1)}, f32[64,128]{1,0:T(8,128)}, u32[]{:S(2)}) copy-start(f32[64,128]{1,0:T(8,128)} %constant.12.clone.waves_ref) | copy-start | bytes 98308
  3.1 24.8 %all-to-all-start = ((bf16[64,4,384]{2,1,0:T(4,128)(2,1)}), bf16[64,4,384]{2,1,0:T(4,128)(2,1)S(1)}, u32[]{:S(2)}, u32[]{:S(2)}) async-start(bf16[64,4,384]{2,1,0:T(4,128)(2,1)} %project.1), calls=%async_computation | async-start | bytes 393216 | tf_op jit(solution)/shard_map/all_to_all | solution.py:347
  22.4 0.7 %copy-start.6 = (f32[128]{0:T(128)S(1)}, f32[128]{0:T(128)}, u32[]{:S(2)}) copy-start(f32[128]{0:T(128)} %param.25) | copy-start | bytes 1540
  23.1 2.9 %copy-start.4 = (f32[3,3,128]{2,1,0:T(4,128)S(1)}, f32[3,3,128]{2,1,0:T(4,128)}, u32[]{:S(2)}) copy-start(f32[3,3,128]{2,1,0:T(4,128)} %taps_ref.1) | copy-start | bytes 13828
  23.1 2.9 %copy-start.7 = (bf16[512,256]{1,0:T(8,128)(2,1)S(1)}, bf16[512,256]{1,0:T(8,128)(2,1)}, u32[]{:S(2)}) copy-start(bf16[512,256]{1,0:T(8,128)(2,1)} %constant.15.clone.right_ref) | copy-start | bytes 786436
  23.1 2.9 %copy-start.10 = (f32[256,128]{1,0:T(8,128)S(1)}, f32[256,128]{1,0:T(8,128)}, u32[]{:S(2)}) copy-start(f32[256,128]{1,0:T(8,128)} %constant.13.clone.turns_ref) | copy-start | bytes 393220
  23.1 2.9 %copy-start.11 = (bf16[256,256]{1,0:T(8,128)(2,1)S(1)}, bf16[256,256]{1,0:T(8,128)(2,1)}, u32[]{:S(2)}) copy-start(bf16[256,256]{1,0:T(8,128)(2,1)} %constant.14.clone.real_ref) | copy-start | bytes 393220
  25.9 0.7 %copy-start.5 = (f32[2,128]{1,0:T(2,128)S(1)}, f32[2,128]{1,0:T(2,128)}, u32[]{:S(2)}) copy-start(f32[2,128]{1,0:T(2,128)} %gain_ref.1) | copy-start | bytes 3076
  26.6 1.3 %copy-start.8 = (bf16[512,256]{1,0:T(8,128)(2,1)S(1)}, bf16[512,256]{1,0:T(8,128)(2,1)}, u32[]{:S(2)}) copy-start(bf16[512,256]{1,0:T(8,128)(2,1)} %constant.16.clone.back_ref) | copy-start | bytes 786436
  26.6 1.3 %copy-start.9 = (bf16[512,256]{1,0:T(8,128)(2,1)S(1)}, bf16[512,256]{1,0:T(8,128)(2,1)}, u32[]{:S(2)}) copy-start(bf16[512,256]{1,0:T(8,128)(2,1)} %constant.17.clone.ends_ref) | copy-start | bytes 786436
  53.2 3.9 %copy-start = (bf16[1024,256]{1,0:T(8,128)(2,1)S(1)}, bf16[1024,256]{1,0:T(8,128)(2,1)}, u32[]{:S(2)}) copy-start(bf16[1024,256]{1,0:T(8,128)(2,1)} %w_ref.1) | copy-start | bytes 1572868

commit v11 on v10

--- a/solution.py
+++ b/solution.py
@@ -55,6 +55,13 @@
 def hi_lo(value):
     top = value.astype(BF)
     return top, (value - top.astype(F32)).astype(BF)
+
+
+def three_parts(value):
+    top = value.astype(BF)
+    rest = value - top.astype(F32)
+    low = rest.astype(BF)
+    return top, low, (rest - low.astype(F32)).astype(BF)
 
 
 def mm(a, b, dims=(((1,), (0,)), ((), ()))):
@@ -144,8 +151,10 @@
     side_ref[2:3, :] = ramp_hi.astype(F32)
     side_ref[3:4, :] = jnp.full((1, units), -0.25, F32)
     side_ref[16:17, :] = jnp.full((1, units), -0.25, F32)
-    in_hi, in_lo = hi_lo(in_ref[1:33, :] * scale)
-    in_all = jnp.concatenate([in_hi, in_lo, in_hi, side_ref[0:16, :].astype(BF)], axis=0)
+    in_hi, in_lo, in_end = three_parts(in_ref[1:33, :] * scale)
+    in_all = jnp.concatenate(
+        [in_hi, in_lo, in_hi, in_lo, in_hi, in_end, side_ref[0:16, :].astype(BF)], axis=0
+    )
     mid_hi, mid_lo = hi_lo(mid_ref[...] * scale)
     mid_all = jnp.concatenate([mid_hi, mid_lo, mid_hi, side_ref[16:32, :].astype(BF)], axis=0)
     chunk = CHUNK
@@ -173,9 +182,9 @@
             ramp_top = ramp.astype(BF).astype(F32)
             ramp = jnp.where(row == 2, ramp - ramp_top, jnp.where(row < 2, ramp_top, 1.0))
             sides.append(jnp.concatenate([ramp, jnp.zeros_like(ramp)], axis=0).astype(BF))
-        top, low = hi_lo(jnp.concatenate(pieces, axis=1))
+        top, low, end = three_parts(jnp.concatenate(pieces, axis=1))
         side = jnp.concatenate(sides, axis=1)
-        moved = mm(in_all, jnp.concatenate([top, top, low, side], axis=0), first)
+        moved = mm(in_all, jnp.concatenate([top, top, low, low, end, top, side], axis=0), first)
         top, low = hi_lo(sine_of_turns(moved))
         moved = mm(mid_all, jnp.concatenate([top, top, low, ones], axis=0), first)
         top, low = hi_lo(sine_of_turns(moved))

time: 58.4 us -> 58.5 us (level)
  transfers between devices with their start and end apart: 1 -> 1, of which waited for: 1 -> 1; matrix products, arithmetic and copies ran while one was open for 0% -> 0% of each run, Pallas kernels for 6% -> 7%
where the time goes in v11:
time: 58.5 us; the launch traced here: 58.2 us
  blocking collectives  26.8 us (46%)
  starting transfers between devices  19.3 us (33%)
  Pallas kernels  10.2 us (17%)
  local copies, waits for them, and re-layouts  1.43 us (2%)
    all_to_all x1, blocking collectives, on_device(): lax.all_to_all(gated.reshape(planes * blocks, *gated.shape[2:]), ('x', *R...  22.9 us
    all_to_all x1, starting transfers between devices, on_device(): lax.all_to_all(pieces, ROW, 0, 0, tiled=True, axis_index_groups=members)  19.3 us
    all_gather x1, blocking collectives, on_device(): everyone = lax.all_gather(everyone, 'core', axis=1)  3.93 us
    pallas_call x1, Pallas kernels, on_device(): pl.pallas_call(functools.partial(project_kernel, steps), out_shape=jax.Sh...  3.07 us
    pallas_call x1, Pallas kernels, on_device(): pl.pallas_call(network_kernel, out_shape=(jax.ShapeDtypeStruct((8 * HALF,...  2.95 us
    pallas_call x1, Pallas kernels, on_device(): pl.pallas_call(conv_kernel, out_shape=jax.ShapeDtypeStruct((planes, block...  2.34 us
    unnamed x26, local copies, waits for them, and re-layouts  1.33 us
  transfers between devices with their start and end apart: 1, of which 1 were waited for; matrix products, arithmetic and copies ran while one was open for 0% of the time, Pallas kernels for 7%

profile of v11, /device:TPU:1, one launch (start us, length us, event | category | flops | bytes accessed | tf_op | source)
XLA Modules:
  0.0 58.2 jit_solution(13591437021043172029)
XLA Ops:
  0.0 3.1 %project.1 = bf16[64,4,384]{2,1,0:T(4,128)(2,1)} custom-call(bf16[2,128,2048]{2,1,0:T(8,128)(2,1)} %tok_hbm.1, bf16[2048,128]{1,0:T(8,128)(2,1)} %a_hbm.1, bf16[2048,128]{1,0:T(8,128)(2,1)} %b_hbm.1, bf16[2048,128]{1,0:T(8,128)(2,1)} %c_hbm.1), custom_call_target="tpu_custom_call" | custom-call | tf_op jit(solution)/shard_map/project/pallas_call | solution.py:341
  3.1 0.0 copy-start.1
  3.1 0.0 copy-start.2
  3.1 0.0 copy-start.3
  3.1 0.0 copy-start.12
  3.1 19.3 %all-to-all-start = ((bf16[64,4,384]{2,1,0:T(4,128)(2,1)}), bf16[64,4,384]{2,1,0:T(4,128)(2,1)S(1)}, u32[]{:S(2)}, u32[]{:S(2)}) async-start(bf16[64,4,384]{2,1,0:T(4,128)(2,1)} %project.1), calls=%async_computation | async-start | bytes 393216 | tf_op jit(solution)/shard_map/all_to_all | solution.py:356
  22.4 0.0 copy-start.6
  22.4 0.0 copy-done.1
  22.4 0.0 copy-done.2
  22.4 0.0 copy-done.3
  22.4 0.0 copy-done.12
  22.4 0.6 %copy-done.6 = f32[128]{0:T(128)S(1)} copy-done((f32[128]{0:T(128)S(1)}, f32[128]{0:T(128)}, u32[]{:S(2)}) %copy-start.6) | copy-done | bytes 536
  23.1 0.0 copy-start.4
  23.1 0.0 copy-start.7
  23.1 0.0 copy-start.10
  23.1 3.0 %network.1 = (f32[512,128]{1,0:T(8,128)S(1)}, f32[8,128]{1,0:T(8,128)S(1)}) custom-call(f32[64,128]{1,0:T(8,128)S(1)} %copy-done.12, f32[33,64]{1,0:T(8,128)S(1)} %copy-done.3, f32[64,64]{1,0:T(8,128)S(1)} %copy-done.2, f32[256,128]{1,0:T(8,128)S(1)} %bitcast.7, f32[1,128]{1,0:T(1,128)S(1)} %bitcast.8), custom_call_target="tpu_custom_call" | custom-call | flops 4000000000 | bytes 1000000 | tf_op jit(solution)/shard_map/network/pallas_call | solution.py:360
  26.0 0.0 copy-done.4
  26.0 0.0 copy-done.7
  26.0 0.0 copy-done.10
  26.0 0.0 copy-done.11
  26.1 0.7 %copy-done.5 = f32[2,128]{1,0:T(2,128)S(1)} copy-done((f32[2,128]{1,0:T(2,128)S(1)}, f32[2,128]{1,0:T(2,128)}, u32[]{:S(2)}) %copy-start.5) | copy-done | bytes 1048
  26.7 0.8 %spectra.1 = (f32[2,256,128]{2,1,0:T(8,128)S(1)}, f32[2,256,128]{2,1,0:T(8,128)S(1)}, f32[3,8,256]{2,1,0:T(8,128)S(1)}) custom-call(f32[512,128]{1,0:T(8,128)S(1)} %get-tuple-element.10.rows_ref, f32[8,128]{1,0:T(8,128)S(1)} %get-tuple-element.11.factor_ref, f32[256,128]{1,0:T(8,128)S(1)} %copy-done.10, bf16[256,256]{1,0:T(8,128)(2,1)S(1)} %copy-done.11, ...), custom_call_target="tpu_custom_call" | custom-call | flops 1000000000 | bytes 2000000 | tf_op jit(solution)/shard_map/spectra/pallas_call | solution.py:381
  27.6 0.4 all-to-all-done.x_ref
  27.9 0.0 copy-done.8
  27.9 0.0 copy-done.9
  27.9 2.3 %gated_conv.1 = bf16[4,64,2,256]{3,2,1,0:T(2,128)(2,1)S(1)} custom-call(bf16[64,4,384]{2,1,0:T(4,128)(2,1)S(1)} %all-to-all-done.x_ref, f32[3,8,256]{2,1,0:T(8,128)S(1)} %get-tuple-element.12.coef_ref, f32[2,256,128]{2,1,0:T(8,128)S(1)} %get-tuple-element.13.spec_re_ref, f32[2,256,128]{2,1,0:T(8,128)S(1)} %get-tuple-element.14.spec_im_ref, ...), custom_call_target="tpu_custom_call" | custom-call | flops 4000000000 | bytes 2000000 | tf_op jit(solution)/shard_map/gated_conv/pallas_call | solution.py:393
  30.3 22.9 %all_to_all.10 = bf16[256,2,256]{2,1,0:T(2,128)(2,1)S(1)} all-to-all(bf16[256,2,256]{2,1,0:T(2,128)(2,1)S(1)} %bitcast.6), channel_id=1, replica_groups={{356,364,372,380,388,396,404,412,420,428,436,444,452,460,468,476,484,49..., dimensions={0} | all-to-all | bytes 524288 | tf_op jit(solution)/shard_map/all_to_all | solution.py:419
  53.2 0.1 all_gather_reshape.3
  53.3 0.0 copy-start
  53.3 3.9 %all_gather.3 = bf16[4,2,128,256]{3,2,1,0:T(8,128)(2,1)S(1)} all-gather(bf16[4,1,128,256]{3,2,1,0:T(8,128)(2,1)S(1)} %all_gather_reshape.3), channel_id=1, replica_groups=mesh['row_0'=8,'row_1'=8,'x'=4,'core'=2] {'core'}, dimensions={1}, use_global_device_ids=true | all-gather | bytes 786432 | tf_op jit(solution)/shard_map/all_gather | solution.py:424
  57.2 0.0 copy-done
  57.2 1.0 %output_map.1 = bf16[256,256]{1,0:T(8,128)(2,1)} custom-call(bf16[1024,256]{1,0:T(8,128)(2,1)S(1)} %bitcast.5, bf16[1024,256]{1,0:T(8,128)(2,1)S(1)} %copy-done), custom_call_target="tpu_custom_call" | custom-call | flops 134217728 | bytes 1200000 | tf_op jit(solution)/shard_map/output_map/pallas_call | solution.py:426
  (4 shorter events, 0.0 us)
Async XLA Ops:
  3.1 19.3 %copy-start.1 = (f32[64,2,2,128]{3,2,1,0:T(2,128)S(1)}, f32[64,2,2,128]{3,2,1,0:T(2,128)}, u32[]{:S(2)}) copy-start(f32[64,2,2,128]{3,2,1,0:T(2,128)} %param.24) | copy-start | bytes 393220
  3.1 19.3 %copy-start.2 = (f32[64,64]{1,0:T(8,128)S(1)}, f32[64,64]{1,0:T(8,128)}, u32[]{:S(2)}) copy-start(f32[64,64]{1,0:T(8,128)} %mid_ref.1) | copy-start | bytes 49156
  3.1 19.3 %copy-start.3 = (f32[33,64]{1,0:T(8,128)S(1)}, f32[33,64]{1,0:T(8,128)}, u32[]{:S(2)}) copy-start(f32[33,64]{1,0:T(8,128)} %in_ref.1) | copy-start | bytes 25348
  3.1 19.3 %copy-start.12 = (f32[64,128]{1,0:T(8,128)S(1)}, f32[64,128]{1,0:T(8,128)}, u32[]{:S(2)}) copy-start(f32[64,128]{1,0:T(8,128)} %constant.12.clone.waves_ref) | copy-start | bytes 98308
  3.1 24.8 %all-to-all-start = ((bf16[64,4,384]{2,1,0:T(4,128)(2,1)}), bf16[64,4,384]{2,1,0:T(4,128)(2,1)S(1)}, u32[]{:S(2)}, u32[]{:S(2)}) async-start(bf16[64,4,384]{2,1,0:T(4,128)(2,1)} %project.1), calls=%async_computation | async-start | bytes 393216 | tf_op jit(solution)/shard_map/all_to_all | solution.py:356
  22.4 0.7 %copy-start.6 = (f32[128]{0:T(128)S(1)}, f32[128]{0:T(128)}, u32[]{:S(2)}) copy-start(f32[128]{0:T(128)} %param.25) | copy-start | bytes 1540
  23.1 3.0 %copy-start.4 = (f32[3,3,128]{2,1,0:T(4,128)S(1)}, f32[3,3,128]{2,1,0:T(4,128)}, u32[]{:S(2)}) copy-start(f32[3,3,128]{2,1,0:T(4,128)} %taps_ref.1) | copy-start | bytes 13828
  23.1 3.0 %copy-start.7 = (bf16[512,256]{1,0:T(8,128)(2,1)S(1)}, bf16[512,256]{1,0:T(8,128)(2,1)}, u32[]{:S(2)}) copy-start(bf16[512,256]{1,0:T(8,128)(2,1)} %constant.15.clone.right_ref) | copy-start | bytes 786436
  23.1 3.0 %copy-start.10 = (f32[256,128]{1,0:T(8,128)S(1)}, f32[256,128]{1,0:T(8,128)}, u32[]{:S(2)}) copy-start(f32[256,128]{1,0:T(8,128)} %constant.13.clone.turns_ref) | copy-start | bytes 393220
  23.1 3.0 %copy-start.11 = (bf16[256,256]{1,0:T(8,128)(2,1)S(1)}, bf16[256,256]{1,0:T(8,128)(2,1)}, u32[]{:S(2)}) copy-start(bf16[256,256]{1,0:T(8,128)(2,1)} %constant.14.clone.real_ref) | copy-start | bytes 393220
  26.0 0.7 %copy-start.5 = (f32[2,128]{1,0:T(2,128)S(1)}, f32[2,128]{1,0:T(2,128)}, u32[]{:S(2)}) copy-start(f32[2,128]{1,0:T(2,128)} %gain_ref.1) | copy-start | bytes 3076
  26.7 1.2 %copy-start.8 = (bf16[512,256]{1,0:T(8,128)(2,1)S(1)}, bf16[512,256]{1,0:T(8,128)(2,1)}, u32[]{:S(2)}) copy-start(bf16[512,256]{1,0:T(8,128)(2,1)} %constant.16.clone.back_ref) | copy-start | bytes 786436
  26.7 1.2 %copy-start.9 = (bf16[512,256]{1,0:T(8,128)(2,1)S(1)}, bf16[512,256]{1,0:T(8,128)(2,1)}, u32[]{:S(2)}) copy-start(bf16[512,256]{1,0:T(8,128)(2,1)} %constant.17.clone.ends_ref) | copy-start | bytes 786436
  53.3 3.9 %copy-start = (bf16[1024,256]{1,0:T(8,128)(2,1)S(1)}, bf16[1024,256]{1,0:T(8,128)(2,1)}, u32[]{:S(2)}) copy-start(bf16[1024,256]{1,0:T(8,128)(2,1)} %w_ref.1) | copy-start | bytes 1572868

commit v12 on v11

--- a/solution.py
+++ b/solution.py
@@ -308,13 +308,22 @@
             o_ref[plane, :, :, s * SIDE : (s + 1) * SIDE] = piece
 
 
-def output_kernel(all_ref, w_ref, o_ref):
+def output_kernel(all_ref, w_ref, o_hbm, o_ref, sems):
     rows = all_ref.shape[0]
     cut = PLANE * (rows // 4)
     first = (((0,), (0,)), ((), ()))
-    total = mm(all_ref[: rows - cut, :], w_ref[cut:, :], first)
-    total += mm(all_ref[rows - cut :, :], w_ref[:cut, :], first)
-    o_ref[...] = total.astype(BF)
+    copies = []
+    for s in range(2):
+        part = slice(s * SIDE, (s + 1) * SIDE)
+        total = mm(all_ref[: rows - cut, part], w_ref[cut:, :], first)
+        total += mm(all_ref[rows - cut :, part], w_ref[:cut, :], first)
+        o_ref[part, :] = total.astype(BF)
+        span = pl.ds(s * SIDE, SIDE)
+        copy = pltpu.make_async_copy(o_ref.at[span, :], o_hbm.at[span, :], sems.at[s])
+        copy.start()
+        copies.append(copy)
+    for copy in copies:
+        copy.wait()
 
 
 def on_device(
@@ -427,7 +436,11 @@
         output_kernel,
         out_shape=jax.ShapeDtypeStruct((seqs * tok_rows, w_output.shape[1]), BF),
         in_specs=[vmem] * 2,
-        out_specs=vmem,
+        out_specs=far,
+        scratch_shapes=[
+            pltpu.VMEM((seqs * tok_rows, w_output.shape[1]), BF),
+            pltpu.SemaphoreType.DMA((2,)),
+        ],
         compiler_params=pltpu.CompilerParams(vmem_limit_bytes=16 * 2**20),
         cost_estimate=pl.CostEstimate(
             flops=134_217_728, bytes_accessed=1_200_000, transcendentals=0

time: 58.5 us -> 58.5 us (level)
  no operation moved by 1% of the time
where the time goes in v12:
time: 58.5 us; the launch traced here: 58.2 us
  blocking collectives  26.8 us (46%)
  starting transfers between devices  19.3 us (33%)
  Pallas kernels  10.2 us (17%)
  local copies, waits for them, and re-layouts  1.43 us (2%)
    all_to_all x1, blocking collectives, on_device(): lax.all_to_all(gated.reshape(planes * blocks, *gated.shape[2:]), ('x', *R...  22.9 us
    all_to_all x1, starting transfers between devices, on_device(): lax.all_to_all(pieces, ROW, 0, 0, tiled=True, axis_index_groups=members)  19.3 us
    all_gather x1, blocking collectives, on_device(): everyone = lax.all_gather(everyone, 'core', axis=1)  3.93 us
    pallas_call x1, Pallas kernels, on_device(): pl.pallas_call(functools.partial(project_kernel, steps), out_shape=jax.Sh...  3.07 us
    pallas_call x1, Pallas kernels, on_device(): pl.pallas_call(network_kernel, out_shape=(jax.ShapeDtypeStruct((8 * HALF,...  2.95 us
    pallas_call x1, Pallas kernels, on_device(): pl.pallas_call(conv_kernel, out_shape=jax.ShapeDtypeStruct((planes, block...  2.34 us
    unnamed x26, local copies, waits for them, and re-layouts  1.33 us
  transfers between devices with their start and end apart: 1, of which 1 were waited for; matrix products, arithmetic and copies ran while one was open for 0% of the time, Pallas kernels for 7%

profile of v12, /device:TPU:1, one launch (start us, length us, event | category | flops | bytes accessed | tf_op | source)
XLA Modules:
  0.0 58.2 jit_solution(5033124732034557520)
XLA Ops:
  0.0 3.1 %project.1 = bf16[64,4,384]{2,1,0:T(4,128)(2,1)} custom-call(bf16[2,128,2048]{2,1,0:T(8,128)(2,1)} %tok_hbm.1, bf16[2048,128]{1,0:T(8,128)(2,1)} %a_hbm.1, bf16[2048,128]{1,0:T(8,128)(2,1)} %b_hbm.1, bf16[2048,128]{1,0:T(8,128)(2,1)} %c_hbm.1), custom_call_target="tpu_custom_call" | custom-call | tf_op jit(solution)/shard_map/project/pallas_call | solution.py:350
  3.1 0.0 copy-start.1
  3.1 0.0 copy-start.2
  3.1 0.0 copy-start.3
  3.1 0.0 copy-start.12
  3.1 19.3 %all-to-all-start = ((bf16[64,4,384]{2,1,0:T(4,128)(2,1)}), bf16[64,4,384]{2,1,0:T(4,128)(2,1)S(1)}, u32[]{:S(2)}, u32[]{:S(2)}) async-start(bf16[64,4,384]{2,1,0:T(4,128)(2,1)} %project.1), calls=%async_computation | async-start | bytes 393216 | tf_op jit(solution)/shard_map/all_to_all | solution.py:365
  22.4 0.0 copy-start.6
  22.4 0.0 copy-done.1
  22.4 0.0 copy-done.2
  22.4 0.0 copy-done.3
  22.4 0.0 copy-done.12
  22.4 0.6 %copy-done.6 = f32[128]{0:T(128)S(1)} copy-done((f32[128]{0:T(128)S(1)}, f32[128]{0:T(128)}, u32[]{:S(2)}) %copy-start.6) | copy-done | bytes 536
  23.1 0.0 copy-start.4
  23.1 0.0 copy-start.7
  23.1 0.0 copy-start.10
  23.1 3.0 %network.1 = (f32[512,128]{1,0:T(8,128)S(1)}, f32[8,128]{1,0:T(8,128)S(1)}) custom-call(f32[64,128]{1,0:T(8,128)S(1)} %copy-done.12, f32[33,64]{1,0:T(8,128)S(1)} %copy-done.3, f32[64,64]{1,0:T(8,128)S(1)} %copy-done.2, f32[256,128]{1,0:T(8,128)S(1)} %bitcast.7, f32[1,128]{1,0:T(1,128)S(1)} %bitcast.8), custom_call_target="tpu_custom_call" | custom-call | flops 4000000000 | bytes 1000000 | tf_op jit(solution)/shard_map/network/pallas_call | solution.py:369
  26.0 0.0 copy-done.4
  26.0 0.0 copy-done.7
  26.0 0.0 copy-done.10
  26.0 0.0 copy-done.11
  26.1 0.7 %copy-done.5 = f32[2,128]{1,0:T(2,128)S(1)} copy-done((f32[2,128]{1,0:T(2,128)S(1)}, f32[2,128]{1,0:T(2,128)}, u32[]{:S(2)}) %copy-start.5) | copy-done | bytes 1048
  26.7 0.8 %spectra.1 = (f32[2,256,128]{2,1,0:T(8,128)S(1)}, f32[2,256,128]{2,1,0:T(8,128)S(1)}, f32[3,8,256]{2,1,0:T(8,128)S(1)}) custom-call(f32[512,128]{1,0:T(8,128)S(1)} %get-tuple-element.10.rows_ref, f32[8,128]{1,0:T(8,128)S(1)} %get-tuple-element.11.factor_ref, f32[256,128]{1,0:T(8,128)S(1)} %copy-done.10, bf16[256,256]{1,0:T(8,128)(2,1)S(1)} %copy-done.11, ...), custom_call_target="tpu_custom_call" | custom-call | flops 1000000000 | bytes 2000000 | tf_op jit(solution)/shard_map/spectra/pallas_call | solution.py:390
  27.6 0.4 all-to-all-done.x_ref
  27.9 0.0 copy-done.8
  27.9 0.0 copy-done.9
  27.9 2.3 %gated_conv.1 = bf16[4,64,2,256]{3,2,1,0:T(2,128)(2,1)S(1)} custom-call(bf16[64,4,384]{2,1,0:T(4,128)(2,1)S(1)} %all-to-all-done.x_ref, f32[3,8,256]{2,1,0:T(8,128)S(1)} %get-tuple-element.12.coef_ref, f32[2,256,128]{2,1,0:T(8,128)S(1)} %get-tuple-element.13.spec_re_ref, f32[2,256,128]{2,1,0:T(8,128)S(1)} %get-tuple-element.14.spec_im_ref, ...), custom_call_target="tpu_custom_call" | custom-call | flops 4000000000 | bytes 2000000 | tf_op jit(solution)/shard_map/gated_conv/pallas_call | solution.py:402
  30.3 22.9 %all_to_all.10 = bf16[256,2,256]{2,1,0:T(2,128)(2,1)S(1)} all-to-all(bf16[256,2,256]{2,1,0:T(2,128)(2,1)S(1)} %bitcast.6), channel_id=1, replica_groups={{356,364,372,380,388,396,404,412,420,428,436,444,452,460,468,476,484,49..., dimensions={0} | all-to-all | bytes 524288 | tf_op jit(solution)/shard_map/all_to_all | solution.py:428
  53.2 0.1 all_gather_reshape.3
  53.3 0.0 copy-start
  53.3 3.9 %all_gather.3 = bf16[4,2,128,256]{3,2,1,0:T(8,128)(2,1)S(1)} all-gather(bf16[4,1,128,256]{3,2,1,0:T(8,128)(2,1)S(1)} %all_gather_reshape.3), channel_id=1, replica_groups=mesh['row_0'=8,'row_1'=8,'x'=4,'core'=2] {'core'}, dimensions={1}, use_global_device_ids=true | all-gather | bytes 786432 | tf_op jit(solution)/shard_map/all_gather | solution.py:433
  57.2 0.0 copy-done
  57.2 1.0 %output_map.1 = bf16[256,256]{1,0:T(8,128)(2,1)} custom-call(bf16[1024,256]{1,0:T(8,128)(2,1)S(1)} %bitcast.5, bf16[1024,256]{1,0:T(8,128)(2,1)S(1)} %copy-done), custom_call_target="tpu_custom_call" | custom-call | flops 134217728 | bytes 1200000 | tf_op jit(solution)/shard_map/output_map/pallas_call | solution.py:435
  (4 shorter events, 0.0 us)
Async XLA Ops:
  3.1 19.3 %copy-start.1 = (f32[64,2,2,128]{3,2,1,0:T(2,128)S(1)}, f32[64,2,2,128]{3,2,1,0:T(2,128)}, u32[]{:S(2)}) copy-start(f32[64,2,2,128]{3,2,1,0:T(2,128)} %param.24) | copy-start | bytes 393220
  3.1 19.3 %copy-start.2 = (f32[64,64]{1,0:T(8,128)S(1)}, f32[64,64]{1,0:T(8,128)}, u32[]{:S(2)}) copy-start(f32[64,64]{1,0:T(8,128)} %mid_ref.1) | copy-start | bytes 49156
  3.1 19.3 %copy-start.3 = (f32[33,64]{1,0:T(8,128)S(1)}, f32[33,64]{1,0:T(8,128)}, u32[]{:S(2)}) copy-start(f32[33,64]{1,0:T(8,128)} %in_ref.1) | copy-start | bytes 25348
  3.1 19.3 %copy-start.12 = (f32[64,128]{1,0:T(8,128)S(1)}, f32[64,128]{1,0:T(8,128)}, u32[]{:S(2)}) copy-start(f32[64,128]{1,0:T(8,128)} %constant.12.clone.waves_ref) | copy-start | bytes 98308
  3.1 24.8 %all-to-all-start = ((bf16[64,4,384]{2,1,0:T(4,128)(2,1)}), bf16[64,4,384]{2,1,0:T(4,128)(2,1)S(1)}, u32[]{:S(2)}, u32[]{:S(2)}) async-start(bf16[64,4,384]{2,1,0:T(4,128)(2,1)} %project.1), calls=%async_computation | async-start | bytes 393216 | tf_op jit(solution)/shard_map/all_to_all | solution.py:365
  22.4 0.7 %copy-start.6 = (f32[128]{0:T(128)S(1)}, f32[128]{0:T(128)}, u32[]{:S(2)}) copy-start(f32[128]{0:T(128)} %param.25) | copy-start | bytes 1540
  23.1 3.0 %copy-start.4 = (f32[3,3,128]{2,1,0:T(4,128)S(1)}, f32[3,3,128]{2,1,0:T(4,128)}, u32[]{:S(2)}) copy-start(f32[3,3,128]{2,1,0:T(4,128)} %taps_ref.1) | copy-start | bytes 13828
  23.1 3.0 %copy-start.7 = (bf16[512,256]{1,0:T(8,128)(2,1)S(1)}, bf16[512,256]{1,0:T(8,128)(2,1)}, u32[]{:S(2)}) copy-start(bf16[512,256]{1,0:T(8,128)(2,1)} %constant.15.clone.right_ref) | copy-start | bytes 786436
  23.1 3.0 %copy-start.10 = (f32[256,128]{1,0:T(8,128)S(1)}, f32[256,128]{1,0:T(8,128)}, u32[]{:S(2)}) copy-start(f32[256,128]{1,0:T(8,128)} %constant.13.clone.turns_ref) | copy-start | bytes 393220
  23.1 3.0 %copy-start.11 = (bf16[256,256]{1,0:T(8,128)(2,1)S(1)}, bf16[256,256]{1,0:T(8,128)(2,1)}, u32[]{:S(2)}) copy-start(bf16[256,256]{1,0:T(8,128)(2,1)} %constant.14.clone.real_ref) | copy-start | bytes 393220
  26.0 0.7 %copy-start.5 = (f32[2,128]{1,0:T(2,128)S(1)}, f32[2,128]{1,0:T(2,128)}, u32[]{:S(2)}) copy-start(f32[2,128]{1,0:T(2,128)} %gain_ref.1) | copy-start | bytes 3076
  26.7 1.2 %copy-start.8 = (bf16[512,256]{1,0:T(8,128)(2,1)S(1)}, bf16[512,256]{1,0:T(8,128)(2,1)}, u32[]{:S(2)}) copy-start(bf16[512,256]{1,0:T(8,128)(2,1)} %constant.16.clone.back_ref) | copy-start | bytes 786436
  26.7 1.2 %copy-start.9 = (bf16[512,256]{1,0:T(8,128)(2,1)S(1)}, bf16[512,256]{1,0:T(8,128)(2,1)}, u32[]{:S(2)}) copy-start(bf16[512,256]{1,0:T(8,128)(2,1)} %constant.17.clone.ends_ref) | copy-start | bytes 786436
  53.3 3.9 %copy-start = (bf16[1024,256]{1,0:T(8,128)(2,1)S(1)}, bf16[1024,256]{1,0:T(8,128)(2,1)}, u32[]{:S(2)}) copy-start(bf16[1024,256]{1,0:T(8,128)(2,1)} %w_ref.1) | copy-start | bytes 1572868

commit v13 on v11

--- a/solution.py
+++ b/solution.py
@@ -16,7 +16,7 @@
 HALF = SIDE // 2
 CHUNK = 4096
 PLANE = 2
-ROOT = 44
+ROOT = 36
 BF = jnp.bfloat16
 F32 = jnp.float32
 

time: 58.5 us -> 58.5 us (level)
  starting transfers between devices: 19.3 us -> 20.2 us
  blocking collectives: 26.8 us -> 26.1 us
    all_to_all x1, starting transfers between devices: 19.3 us -> 20.2 us  [on_device(): lax.all_to_all(pieces, ROW, 0, 0, tiled=True, axis_index_groups=members)]
  transfers between devices with their start and end apart: 1 -> 1, of which waited for: 1 -> 0; matrix products, arithmetic and copies ran while one was open for 0% -> 0% of each run, Pallas kernels for 7% -> 7%
where the time goes in v13:
time: 58.5 us; the launch traced here: 58.2 us
  blocking collectives  26.1 us (45%)
  starting transfers between devices  20.2 us (35%)
  Pallas kernels  10.2 us (17%)
  local copies, waits for them, and re-layouts  1.6 us (3%)
    all_to_all x1, blocking collectives, on_device(): lax.all_to_all(gated.reshape(planes * blocks, *gated.shape[2:]), ('x', *R...  22.4 us
    all_to_all x1, starting transfers between devices, on_device(): lax.all_to_all(pieces, ROW, 0, 0, tiled=True, axis_index_groups=members)  20.2 us
    all_gather x1, blocking collectives, on_device(): everyone = lax.all_gather(everyone, 'core', axis=1)  3.7 us
    pallas_call x1, Pallas kernels, on_device(): pl.pallas_call(functools.partial(project_kernel, steps), out_shape=jax.Sh...  3.07 us
    pallas_call x1, Pallas kernels, on_device(): pl.pallas_call(network_kernel, out_shape=(jax.ShapeDtypeStruct((8 * HALF,...  2.95 us
    pallas_call x1, Pallas kernels, on_device(): pl.pallas_call(conv_kernel, out_shape=jax.ShapeDtypeStruct((planes, block...  2.34 us
    unnamed x26, local copies, waits for them, and re-layouts  1.49 us
  transfers between devices with their start and end apart: 1, of which 0 were waited for; matrix products, arithmetic and copies ran while one was open for 0% of the time, Pallas kernels for 7%

profile of v13, /device:TPU:1, one launch (start us, length us, event | category | flops | bytes accessed | tf_op | source)
XLA Modules:
  0.0 58.2 jit_solution(1754331230797680329)
XLA Ops:
  0.0 3.1 %project.1 = bf16[64,4,384]{2,1,0:T(4,128)(2,1)} custom-call(bf16[2,128,2048]{2,1,0:T(8,128)(2,1)} %tok_hbm.1, bf16[2048,128]{1,0:T(8,128)(2,1)} %a_hbm.1, bf16[2048,128]{1,0:T(8,128)(2,1)} %b_hbm.1, bf16[2048,128]{1,0:T(8,128)(2,1)} %c_hbm.1), custom_call_target="tpu_custom_call" | custom-call | tf_op jit(solution)/shard_map/project/pallas_call | solution.py:341
  3.1 0.0 copy-start.1
  3.1 0.0 copy-start.2
  3.1 0.0 copy-start.3
  3.1 0.0 copy-start.12
  3.1 20.2 %all-to-all-start = ((bf16[64,4,384]{2,1,0:T(4,128)(2,1)}), bf16[64,4,384]{2,1,0:T(4,128)(2,1)S(1)}, u32[]{:S(2)}, u32[]{:S(2)}) async-start(bf16[64,4,384]{2,1,0:T(4,128)(2,1)} %project.1), calls=%async_computation | async-start | bytes 393216 | tf_op jit(solution)/shard_map/all_to_all | solution.py:356
  23.3 0.0 copy-start.6
  23.4 0.0 copy-done.1
  23.4 0.0 copy-done.2
  23.4 0.0 copy-done.3
  23.4 0.0 copy-done.12
  23.4 0.6 %copy-done.6 = f32[128]{0:T(128)S(1)} copy-done((f32[128]{0:T(128)S(1)}, f32[128]{0:T(128)}, u32[]{:S(2)}) %copy-start.6) | copy-done | bytes 536
  24.0 0.0 copy-start.4
  24.0 0.0 copy-start.7
  24.0 0.0 copy-start.10
  24.0 3.0 %network.1 = (f32[512,128]{1,0:T(8,128)S(1)}, f32[8,128]{1,0:T(8,128)S(1)}) custom-call(f32[64,128]{1,0:T(8,128)S(1)} %copy-done.12, f32[33,64]{1,0:T(8,128)S(1)} %copy-done.3, f32[64,64]{1,0:T(8,128)S(1)} %copy-done.2, f32[256,128]{1,0:T(8,128)S(1)} %bitcast.7, f32[1,128]{1,0:T(1,128)S(1)} %bitcast.8), custom_call_target="tpu_custom_call" | custom-call | flops 4000000000 | bytes 1000000 | tf_op jit(solution)/shard_map/network/pallas_call | solution.py:360
  27.0 0.0 copy-done.4
  27.0 0.0 copy-done.7
  27.0 0.0 copy-done.10
  27.0 0.0 copy-done.11
  27.0 0.7 %copy-done.5 = f32[2,128]{1,0:T(2,128)S(1)} copy-done((f32[2,128]{1,0:T(2,128)S(1)}, f32[2,128]{1,0:T(2,128)}, u32[]{:S(2)}) %copy-start.5) | copy-done | bytes 1048
  27.7 0.8 %spectra.1 = (f32[2,256,128]{2,1,0:T(8,128)S(1)}, f32[2,256,128]{2,1,0:T(8,128)S(1)}, f32[3,8,256]{2,1,0:T(8,128)S(1)}) custom-call(f32[512,128]{1,0:T(8,128)S(1)} %get-tuple-element.10.rows_ref, f32[8,128]{1,0:T(8,128)S(1)} %get-tuple-element.11.factor_ref, f32[256,128]{1,0:T(8,128)S(1)} %copy-done.10, bf16[256,256]{1,0:T(8,128)(2,1)S(1)} %copy-done.11, ...), custom_call_target="tpu_custom_call" | custom-call | flops 1000000000 | bytes 2000000 | tf_op jit(solution)/shard_map/spectra/pallas_call | solution.py:381
  28.5 0.0 all-to-all-done.x_ref
  28.5 0.1 copy-done.8
  28.6 0.1 copy-done.9
  28.7 2.3 %gated_conv.1 = bf16[4,64,2,256]{3,2,1,0:T(2,128)(2,1)S(1)} custom-call(bf16[64,4,384]{2,1,0:T(4,128)(2,1)S(1)} %all-to-all-done.x_ref, f32[3,8,256]{2,1,0:T(8,128)S(1)} %get-tuple-element.12.coef_ref, f32[2,256,128]{2,1,0:T(8,128)S(1)} %get-tuple-element.13.spec_re_ref, f32[2,256,128]{2,1,0:T(8,128)S(1)} %get-tuple-element.14.spec_im_ref, ...), custom_call_target="tpu_custom_call" | custom-call | flops 4000000000 | bytes 2000000 | tf_op jit(solution)/shard_map/gated_conv/pallas_call | solution.py:393
  31.0 22.4 %all_to_all.10 = bf16[256,2,256]{2,1,0:T(2,128)(2,1)S(1)} all-to-all(bf16[256,2,256]{2,1,0:T(2,128)(2,1)S(1)} %bitcast.6), channel_id=1, replica_groups={{292,300,308,316,324,332,340,348,356,364,372,380,388,396,404,412,420,42..., dimensions={0} | all-to-all | bytes 524288 | tf_op jit(solution)/shard_map/all_to_all | solution.py:419
  53.4 0.1 all_gather_reshape.3
  53.5 0.0 copy-start
  53.5 3.7 %all_gather.3 = bf16[4,2,128,256]{3,2,1,0:T(8,128)(2,1)S(1)} all-gather(bf16[4,1,128,256]{3,2,1,0:T(8,128)(2,1)S(1)} %all_gather_reshape.3), channel_id=1, replica_groups=mesh['row_0'=8,'row_1'=8,'x'=4,'core'=2] {'core'}, dimensions={1}, use_global_device_ids=true | all-gather | bytes 786432 | tf_op jit(solution)/shard_map/all_gather | solution.py:424
  57.2 0.0 copy-done
  57.2 1.0 %output_map.1 = bf16[256,256]{1,0:T(8,128)(2,1)} custom-call(bf16[1024,256]{1,0:T(8,128)(2,1)S(1)} %bitcast.5, bf16[1024,256]{1,0:T(8,128)(2,1)S(1)} %copy-done), custom_call_target="tpu_custom_call" | custom-call | flops 134217728 | bytes 1200000 | tf_op jit(solution)/shard_map/output_map/pallas_call | solution.py:426
  (4 shorter events, 0.0 us)
Async XLA Ops:
  3.1 20.3 %copy-start.1 = (f32[64,2,2,128]{3,2,1,0:T(2,128)S(1)}, f32[64,2,2,128]{3,2,1,0:T(2,128)}, u32[]{:S(2)}) copy-start(f32[64,2,2,128]{3,2,1,0:T(2,128)} %param.24) | copy-start | bytes 393220
  3.1 20.3 %copy-start.2 = (f32[64,64]{1,0:T(8,128)S(1)}, f32[64,64]{1,0:T(8,128)}, u32[]{:S(2)}) copy-start(f32[64,64]{1,0:T(8,128)} %mid_ref.1) | copy-start | bytes 49156
  3.1 20.3 %copy-start.3 = (f32[33,64]{1,0:T(8,128)S(1)}, f32[33,64]{1,0:T(8,128)}, u32[]{:S(2)}) copy-start(f32[33,64]{1,0:T(8,128)} %in_ref.1) | copy-start | bytes 25348
  3.1 20.3 %copy-start.12 = (f32[64,128]{1,0:T(8,128)S(1)}, f32[64,128]{1,0:T(8,128)}, u32[]{:S(2)}) copy-start(f32[64,128]{1,0:T(8,128)} %constant.12.clone.waves_ref) | copy-start | bytes 98308
  3.1 25.4 %all-to-all-start = ((bf16[64,4,384]{2,1,0:T(4,128)(2,1)}), bf16[64,4,384]{2,1,0:T(4,128)(2,1)S(1)}, u32[]{:S(2)}, u32[]{:S(2)}) async-start(bf16[64,4,384]{2,1,0:T(4,128)(2,1)} %project.1), calls=%async_computation | async-start | bytes 393216 | tf_op jit(solution)/shard_map/all_to_all | solution.py:356
  23.3 0.7 %copy-start.6 = (f32[128]{0:T(128)S(1)}, f32[128]{0:T(128)}, u32[]{:S(2)}) copy-start(f32[128]{0:T(128)} %param.25) | copy-start | bytes 1540
  24.0 3.0 %copy-start.4 = (f32[3,3,128]{2,1,0:T(4,128)S(1)}, f32[3,3,128]{2,1,0:T(4,128)}, u32[]{:S(2)}) copy-start(f32[3,3,128]{2,1,0:T(4,128)} %taps_ref.1) | copy-start | bytes 13828
  24.0 3.0 %copy-start.7 = (bf16[512,256]{1,0:T(8,128)(2,1)S(1)}, bf16[512,256]{1,0:T(8,128)(2,1)}, u32[]{:S(2)}) copy-start(bf16[512,256]{1,0:T(8,128)(2,1)} %constant.15.clone.right_ref) | copy-start | bytes 786436
  24.0 3.0 %copy-start.10 = (f32[256,128]{1,0:T(8,128)S(1)}, f32[256,128]{1,0:T(8,128)}, u32[]{:S(2)}) copy-start(f32[256,128]{1,0:T(8,128)} %constant.13.clone.turns_ref) | copy-start | bytes 393220
  24.0 3.0 %copy-start.11 = (bf16[256,256]{1,0:T(8,128)(2,1)S(1)}, bf16[256,256]{1,0:T(8,128)(2,1)}, u32[]{:S(2)}) copy-start(bf16[256,256]{1,0:T(8,128)(2,1)} %constant.14.clone.real_ref) | copy-start | bytes 393220
  27.0 0.7 %copy-start.5 = (f32[2,128]{1,0:T(2,128)S(1)}, f32[2,128]{1,0:T(2,128)}, u32[]{:S(2)}) copy-start(f32[2,128]{1,0:T(2,128)} %gain_ref.1) | copy-start | bytes 3076
  27.7 0.9 %copy-start.8 = (bf16[512,256]{1,0:T(8,128)(2,1)S(1)}, bf16[512,256]{1,0:T(8,128)(2,1)}, u32[]{:S(2)}) copy-start(bf16[512,256]{1,0:T(8,128)(2,1)} %constant.16.clone.back_ref) | copy-start | bytes 786436
  27.7 1.0 %copy-start.9 = (bf16[512,256]{1,0:T(8,128)(2,1)S(1)}, bf16[512,256]{1,0:T(8,128)(2,1)}, u32[]{:S(2)}) copy-start(bf16[512,256]{1,0:T(8,128)(2,1)} %constant.17.clone.ends_ref) | copy-start | bytes 786436
  53.5 3.7 %copy-start = (bf16[1024,256]{1,0:T(8,128)(2,1)S(1)}, bf16[1024,256]{1,0:T(8,128)(2,1)}, u32[]{:S(2)}) copy-start(bf16[1024,256]{1,0:T(8,128)(2,1)} %w_ref.1) | copy-start | bytes 1572868
